TPU v7x, 512 devices: a whole 4x4x16 slice. The times are simulated.
512 devices in a mesh: ep: 32 (over z, core), tp: 16 (over y, x).
Axes of the slice: x: 4, y: 4, z: 16, core: 2. Of those that a mesh axis runs over, the one named last changes fastest.
Arguments:
- tokens: bfloat16 [8192, 2048], P('ep', 'tp'), may hold values from -800 to 800
- norm_gain: bfloat16 [2048], P('tp'), may hold values from 0.099609375 to 1.8984375
- w_gate: bfloat16 [32, 2048, 6144], P('ep', None, 'tp'), may hold values from -0.125 to 0.125
- w_up: bfloat16 [32, 2048, 6144], P('ep', None, 'tp'), may hold values from -0.125 to 0.125
- w_down: bfloat16 [32, 6144, 2048], P('ep', 'tp'), may hold values from -1.2757759 to 1.2757759
- routes: int32 [8192, 2], P('ep'), may hold values from 0 to 31, all different within a row; in each aligned block of 256 rows (0 to 255, 256 to 511, ...) at most 32 rows name the same one
- route_weights: float32 [8192, 2], P('ep'), may hold values from 0.1 to 1
- final_gain: bfloat16 [2048], P('tp'), may hold values from 0.099609375 to 1.8984375
Outputs:
- mixed_out: bfloat16 [8192, 2048], P('ep', 'tp')
Inputs may be any that keep to these rules, and one draw needn't show every extreme that they name: `routes`: A token's 2 experts differ. Among the tokens of one index of ep (aligned blocks of 256 rows), no expert is named by more than 32 tokens, a bound that some block reaches.
All inputs are finite; a program needn't handle non-finite values.
Results may differ from a plain program's by a relative error of at most 0.017.
Values may be sent and summed in bfloat16 or wider, within the bound.
No kernel may reach another device: no remote copies, remote signals or barrier semaphores. Data moves between devices by JAX's collectives and lax.ppermute only.
A program may use at most 64 MiB of HBM per device.

v0:
```python
import functools

import jax
import jax.numpy as jnp
from jax import lax
from jax.experimental import pallas as pl
from jax.experimental.pallas import tpu as pltpu
from jax.sharding import Mesh, PartitionSpec as P


EPS = 1e-06
F32 = jnp.float32
BF16 = jnp.bfloat16
GAIN_ROWS = 16


def pack_kernel(pos, routes, weights, tokens, near, far, table):
    tok = tokens.shape[0]
    half = near.shape[0]
    experts = 2 * lax.axis_size("z")
    cap = half // (experts // 2)
    e0 = routes[0:1, :]
    e1 = routes[1:2, :]
    lanes = lax.broadcasted_iota(jnp.int32, (experts, tok), 0)
    hot0 = lanes == e0
    hot1 = lanes == e1
    hot = (hot0 | hot1).astype(F32).astype(BF16)
    row = lax.broadcasted_iota(jnp.int32, (tok, tok), 0)
    col = lax.broadcasted_iota(jnp.int32, (tok, tok), 1)
    earlier = (row < col).astype(F32).astype(BF16)
    before = jnp.dot(hot, earlier, preferred_element_type=F32)

    def place(e, mine):
        slot = jnp.sum(jnp.where(mine, before, 0.0), axis=0, keepdims=True)
        other = jnp.bitwise_xor(jnp.bitwise_and(e, 1), pos[0])
        return other * half + (e >> 1) * cap + slot.astype(jnp.int32)

    t0 = place(e0, hot0)
    t1 = place(e1, hot1)
    for at, out in ((0, near), (half, far)):
        rows = lax.broadcasted_iota(jnp.int32, (half, tok), 0) + at
        put = ((rows == t0) | (rows == t1)).astype(F32).astype(BF16)
        out[...] = jnp.dot(put, tokens[...], preferred_element_type=F32).astype(BF16)
    stack = jnp.concatenate(
        [t0.astype(F32), t1.astype(F32), weights[...], jnp.zeros((4, tok), F32)], axis=0
    )
    table[...] = stack.T


def pack(c, routes, weights, tokens):
    tok, share = tokens.shape
    half = lax.axis_size("z") * 32
    vmem = pl.BlockSpec(memory_space=pltpu.VMEM)
    return pl.pallas_call(
        pack_kernel,
        out_shape=(
            jax.ShapeDtypeStruct((half, share), BF16),
            jax.ShapeDtypeStruct((half, share), BF16),
            jax.ShapeDtypeStruct((tok, 8), F32),
        ),
        in_specs=[pl.BlockSpec(memory_space=pltpu.SMEM), vmem, vmem, vmem],
        out_specs=(vmem, vmem, vmem),
        name="pack",
    )(c, routes, weights, tokens)


def expert_kernel(first, rows, *refs):
    if first:
        xs, wg, wu, wd, out, gain_out = refs[:6]
        refs = refs[6:]
    else:
        pos = refs[0]
        xs = refs[1:5]
        wg, wu, wd, gain_in = refs[5:9]
        outs = refs[9:13]
        refs = refs[13:]
    raw, gain_s, xn, g_s, u_s, d_s, stage, sems, osems = refs

    def fetch(n, src, dst):
        cp = pltpu.make_async_copy(src, dst, sems.at[n])
        cp.start()
        return cp

    if first:
        gain_cp = fetch(0, xs.at[:, :, pl.ds(rows, GAIN_ROWS), :], gain_s)
        x_cp = [fetch(1, xs.at[:, :, pl.ds(0, rows), :], raw)]
    else:
        gain_cp = fetch(0, gain_in, gain_s)
        x_cp = [fetch(1 + s, xs[s], raw.at[lax.rem(pos[0] + s, 4)]) for s in range(4)]
    g_cp = fetch(5, wg, g_s)
    u_cp = fetch(6, wu, u_s)
    d_cp = fetch(7, wd, d_s)
    gain_cp.wait()
    copies = []
    if first:
        cp = pltpu.make_async_copy(gain_s, gain_out, osems.at[4])
        cp.start()
        copies.append(cp)
    width = xn.shape[1]
    step = 32
    for cp in x_cp:
        cp.wait()

    def norm(i, _):
        at = pl.multiple_of(i * step, step)
        acc = jnp.zeros((step, 128), F32)
        vals = []
        for j in range(16):
            a, b = (j // 4, j % 4) if first else (j % 4, j // 4)
            v = raw[a, b, pl.ds(at, step), :].astype(F32)
            vals.append(v)
            acc = acc + v * v
        scale = lax.rsqrt(jnp.sum(acc, axis=1, keepdims=True) * (1.0 / width) + EPS)
        for j in range(16):
            gain = gain_s[j // 4, j % 4, 0:1, :].astype(F32)
            xn[pl.ds(at, step), j * 128 : (j + 1) * 128] = (vals[j] * scale * gain).astype(BF16)
        return 0

    lax.fori_loop(0, rows // step, norm, 0)
    g_cp.wait()
    gate = jnp.dot(xn[...], g_s[...], preferred_element_type=F32)
    u_cp.wait()
    up = jnp.dot(xn[...], u_s[...], preferred_element_type=F32)
    hidden = (gate * up / (1.0 + jnp.exp(-gate))).astype(BF16)
    d_cp.wait()
    for y in range(4):
        res = jnp.dot(
            hidden, d_s[:, y * 512 : (y + 1) * 512], preferred_element_type=F32
        ).astype(BF16)
        for x in range(4):
            part = res[:, x * 128 : (x + 1) * 128]
            if first:
                stage[y, x] = part
            else:
                stage[x, y] = part
        if first:
            cp = pltpu.make_async_copy(stage.at[y], out.at[y], osems.at[y])
            cp.start()
            copies.append(cp)
    if not first:
        for s in range(4):
            cp = pltpu.make_async_copy(stage.at[lax.rem(pos[0] + s, 4)], outs[s], osems.at[s])
            cp.start()
            copies.append(cp)
    for cp in copies:
        cp.wait()


def expert(first, pos, xs, weights, gain):
    rows = 512
    width, units = weights[0].shape
    hbm = pl.BlockSpec(memory_space=pltpu.HBM)
    gain_type = jax.ShapeDtypeStruct((4, 4, GAIN_ROWS, 128), BF16)
    if first:
        args = (xs, *weights)
        in_specs = [hbm] * 4
        outs = (jax.ShapeDtypeStruct((4, 4, rows, 128), BF16), gain_type)
    else:
        args = (pos, *xs, *weights, gain)
        in_specs = [pl.BlockSpec(memory_space=pltpu.SMEM)] + [hbm] * 8
        outs = tuple([jax.ShapeDtypeStruct((4, rows, 128), BF16)] * 4)
    return pl.pallas_call(
        functools.partial(expert_kernel, first, rows),
        out_shape=outs,
        in_specs=in_specs,
        out_specs=tuple([hbm] * len(outs)),
        scratch_shapes=[
            pltpu.VMEM((4, 4, rows, 128), BF16),
            pltpu.VMEM((4, 4, GAIN_ROWS, 128), BF16),
            pltpu.VMEM((rows, width), BF16),
            pltpu.VMEM((width, units), BF16),
            pltpu.VMEM((width, units), BF16),
            pltpu.VMEM((units, width), BF16),
            pltpu.VMEM((4, 4, rows, 128), BF16),
            pltpu.SemaphoreType.DMA((8,)),
            pltpu.SemaphoreType.DMA((5,)),
        ],
        compiler_params=pltpu.CompilerParams(vmem_limit_bytes=63 * 1024 * 1024),
        name="expert_a" if first else "expert_b",
    )(*args)


def combine_kernel(table, near, far, combined, squares):
    tok = table.shape[0]
    half = near.shape[0]
    cols = lax.broadcasted_iota(jnp.int32, (tok, half), 1)
    total = None
    for k in range(2):
        target = table[:, k : k + 1].astype(jnp.int32)
        got = None
        for at, src in ((0, near), (half, far)):
            pick = (cols + at == target).astype(F32).astype(BF16)
            part = jnp.dot(pick, src[...], preferred_element_type=F32)
            got = part if got is None else got + part
        term = got * table[:, 2 + k : 3 + k]
        total = term if total is None else total + term
    combined[...] = total
    squares[...] = jnp.sum((total * total).T, axis=0, keepdims=True)


def combine(table, near, far):
    tok = table.shape[0]
    share = near.shape[1]
    vmem = pl.BlockSpec(memory_space=pltpu.VMEM)
    return pl.pallas_call(
        combine_kernel,
        out_shape=(
            jax.ShapeDtypeStruct((tok, share), F32),
            jax.ShapeDtypeStruct((1, tok), F32),
        ),
        in_specs=[vmem] * 3,
        out_specs=(vmem, vmem),
        name="combine",
    )(table, near, far)


def exchange(v, axis):
    return lax.all_to_all(v, axis, split_axis=0, concat_axis=0, tiled=True)


def total_of(parts):
    total = parts[0].astype(F32)
    for p in parts[1:]:
        total = total + p.astype(F32)
    return total.astype(BF16)


def over_z(v):
    n = lax.axis_size("z")
    return exchange(v.reshape(n, v.shape[0] // n, v.shape[1]), "z").reshape(v.shape)


def shift(v, axis, step):
    n = lax.axis_size(axis)
    return lax.ppermute(v, axis, [(i, (i + step) % n) for i in range(n)])


def cross(v, step):
    pairs = [(c * 4 + y, (1 - c) * 4 + (y + step) % 4) for c in range(2) for y in range(4)]
    return lax.ppermute(v, ("c", "y"), pairs)


def pick(v, i):
    return lax.dynamic_index_in_dim(v, i, 0, keepdims=False, allow_negative_indices=False)


def local(tokens, norm_gain, w_gate, w_up, w_down, routes, route_weights, final_gain):
    tok, share = tokens.shape
    width = share * 16
    c = lax.axis_index("c").astype(jnp.int32)
    pos = lax.axis_index("x").astype(jnp.int32).reshape(1)
    near, far, table = pack(c.reshape(1), routes.T, route_weights.T, tokens)
    weights = (w_gate[0], w_up[0], w_down[0])
    near = over_z(near)
    far = over_z(shift(far, "c", 1))
    gain_rows = jnp.broadcast_to(norm_gain[None, :], (GAIN_ROWS, share))
    a = lax.all_gather(jnp.concatenate([near, gain_rows], axis=0), "x")
    a, far = lax.optimization_barrier((a, far))
    a = exchange(jnp.broadcast_to(a[None], (4, *a.shape)), "y")
    b = lax.all_gather(far, "y")
    b = [b] + [shift(b, "x", -s) for s in (1, 2, 3)]
    a, gain = expert(True, None, a, weights, None)
    b = expert(False, pos, b, weights, gain)
    a = exchange(a, "y").astype(F32).sum(axis=0).astype(BF16)
    a = exchange(a, "x").astype(F32).sum(axis=0).astype(BF16)
    near = over_z(a)
    b = total_of([b[0]] + [shift(b[s], "x", s) for s in (1, 2, 3)])
    y = lax.axis_index("y").astype(jnp.int32)
    b = total_of([cross(pick(b, jnp.bitwise_and(y + s, 3)), s) for s in range(4)])
    far = over_z(b)
    combined, squares = combine(table, near, far)
    copies = jnp.broadcast_to(squares, (16, tok))
    total = exchange(copies, ("y", "x")).sum(axis=0)
    scale = lax.rsqrt(total / width + EPS)
    return (combined * scale[:, None] * final_gain.astype(F32)[None, :]).astype(BF16)


def solution(mesh):
    fine = Mesh(mesh.devices.reshape(16, 2, 4, 4), ("z", "c", "y", "x"))
    ep = ("z", "c")
    tp = ("y", "x")
    in_specs = (
        P(ep, tp),
        P(tp),
        P(ep, None, tp),
        P(ep, None, tp),
        P(ep, tp, None),
        P(ep, None),
        P(ep, None),
        P(tp),
    )
    return jax.shard_map(
        local, mesh=fine, in_specs=in_specs, out_specs=P(ep, tp), check_vma=False
    )
```

profile of v0, /device:TPU:1, one launch (start us, length us, event | category | flops | bytes accessed | tf_op | source)
XLA Modules:
  0.0 274.3 jit_solution(6168712375218700054)
XLA Ops:
  2.1 15.7 %all-to-all-start = ((bf16[16,32,128]{2,1,0:T(8,128)(2,1)}), bf16[16,32,128]{2,1,0:T(8,128)(2,1)S(1)}, u32[]{:S(2)}, u32[]{:S(2)}) async-start(bf16[16,32,128]{2,1,0:T(8,128)(2,1)} %bitcast.42), calls=%async_computation | async-start | bytes 262144 | tf_op jit(solution)/shard_map/all_to_all | solution.py:218
  17.9 2.9 %collective-permute-start = (bf16[512,128]{1,0:T(8,128)(2,1)}, bf16[512,128]{1,0:T(8,128)(2,1)}, u32[]{:S(2)}, u32[]{:S(2)}) collective-permute-start(bf16[512,128]{1,0:T(8,128)(2,1)} %get-tuple-element.20), channel_id=1, source_target_pairs={{0,16},{16,0},{1,17},{17,1},{2,18},{18,2},{3,19},{19,3},{4,20},{20... | collective-permute-start | bytes 393224 | tf_op jit(solution)/shard_map/ppermute | solution.py:235
  22.0 7.8 %all-to-all-done = bf16[16,32,128]{2,1,0:T(8,128)(2,1)S(1)} async-done(((bf16[16,32,128]{2,1,0:T(8,128)(2,1)}), bf16[16,32,128]{2,1,0:T(8,128)(2,1)S(1)}, u32[]{:S(2)}, u32[]{:S(2)}) %all-to-all-start) | async-done | bytes 131104 | tf_op jit(solution)/shard_map/all_to_all | solution.py:218
  29.8 6.0 %all-to-all-start.1 = ((bf16[16,32,128]{2,1,0:T(8,128)(2,1)}), bf16[16,32,128]{2,1,0:T(8,128)(2,1)S(1)}, u32[]{:S(2)}, u32[]{:S(2)}) async-start(bf16[16,32,128]{2,1,0:T(8,128)(2,1)} %bitcast.6), calls=%async_computation.1 | async-start | bytes 262144 | tf_op jit(solution)/shard_map/all_to_all | solution.py:218
  36.5 11.5 %all-gather = bf16[2112,128]{1,0:T(8,128)(2,1)S(1)} all-gather(bf16[528,128]{1,0:T(8,128)(2,1)S(1)} %pad_maximum_fusion), channel_id=2, replica_groups=mesh['z'=16,'c'=2,'y'=4,'x'=4] {'x'}, dimensions={0}, use_global_device_ids=true | all-gather | bytes 675840 | tf_op jit(solution)/shard_map/all_gather | solution.py:257
  48.3 27.1 %all_to_all.41.refs_0_ = bf16[4,4,528,128]{3,2,1,0:T(8,128)(2,1)} all-to-all(bf16[4,4,528,128]{3,2,1,0:T(8,128)(2,1)S(1)} %broadcast_in_dim.7), channel_id=1, replica_groups=mesh['z'=16,'c'=2,'y'=4,'x'=4] {'y'}, dimensions={0} | all-to-all | bytes 4325376 | tf_op jit(solution)/shard_map/all_to_all | solution.py:218
  75.4 8.4 %expert_a.1 = (bf16[4,4,512,128]{3,2,1,0:T(8,128)(2,1)}, bf16[4,4,16,128]{3,2,1,0:T(8,128)(2,1)}) custom-call(bf16[4,4,528,128]{3,2,1,0:T(8,128)(2,1)} %all_to_all.41.refs_0_, bf16[2048,384]{1,0:T(8,128)(2,1)} %bitcast.26, bf16[2048,384]{1,0:T(8,128)(2,1)} %bitcast.28, bf16[384,2048]{1,0:T(8,128)(2,1)} %bitcast.30), custom_call_target="tpu_custom_call" | custom-call | tf_op jit(solution)/shard_map/expert_a/pallas_call | solution.py:162
  83.8 4.5 %all-to-all-start.3 = ((bf16[4,4,512,128]{3,2,1,0:T(8,128)(2,1)}), bf16[4,4,512,128]{3,2,1,0:T(8,128)(2,1)}, u32[]{:S(2)}, u32[]{:S(2)}) async-start(bf16[4,4,512,128]{3,2,1,0:T(8,128)(2,1)} %get-tuple-element.22), calls=%async_computation.3 | async-start | bytes 4194304 | tf_op jit(solution)/shard_map/all_to_all | solution.py:218
  88.3 29.6 %all-gather.1 = bf16[2048,128]{1,0:T(8,128)(2,1)S(1)} all-gather(bf16[512,128]{1,0:T(8,128)(2,1)S(1)} %bitcast.37), channel_id=3, replica_groups=mesh['z'=16,'c'=2,'y'=4,'x'=4] {'y'}, dimensions={0}, use_global_device_ids=true | all-gather | bytes 655360 | tf_op jit(solution)/shard_map/all_gather | solution.py:260
  117.9 4.2 %collective-permute-start.1 = (bf16[4,512,128]{2,1,0:T(8,128)(2,1)S(1)}, bf16[4,512,128]{2,1,0:T(8,128)(2,1)S(1)}, u32[]{:S(2)}, u32[]{:S(2)}) collective-permute-start(bf16[4,512,128]{2,1,0:T(8,128)(2,1)S(1)} %bitcast.33), channel_id=1, source_target_pairs={{0,3},{1,0},{2,1},{3,2},{4,7},{5,4},{6,5},{7,6},{8,11},{9,8},{10,9... | collective-permute-start | bytes 1572872 | tf_op jit(solution)/shard_map/ppermute | solution.py:235
  122.0 2.4 collective-permute-start.2
  124.5 2.5 collective-permute-start.3
  127.0 3.3 %collective-permute-done.1.refs_2_ = bf16[4,512,128]{2,1,0:T(8,128)(2,1)S(1)} collective-permute-done((bf16[4,512,128]{2,1,0:T(8,128)(2,1)S(1)}, bf16[4,512,128]{2,1,0:T(8,128)(2,1)S(1)}, u32[]{:S(2)}, u32[]{:S(2)}) %collective-permute-start.1) | collective-permute-done | bytes 524320 | tf_op jit(solution)/shard_map/ppermute | solution.py:235
  130.2 3.3 %collective-permute-done.2.refs_3_ = bf16[4,512,128]{2,1,0:T(8,128)(2,1)S(1)} collective-permute-done((bf16[4,512,128]{2,1,0:T(8,128)(2,1)S(1)}, bf16[4,512,128]{2,1,0:T(8,128)(2,1)S(1)}, u32[]{:S(2)}, u32[]{:S(2)}) %collective-permute-start.2) | collective-permute-done | bytes 524320 | tf_op jit(solution)/shard_map/ppermute | solution.py:235
  133.6 15.1 %collective-permute-done.3.refs_4_ = bf16[4,512,128]{2,1,0:T(8,128)(2,1)S(1)} collective-permute-done((bf16[4,512,128]{2,1,0:T(8,128)(2,1)S(1)}, bf16[4,512,128]{2,1,0:T(8,128)(2,1)S(1)}, u32[]{:S(2)}, u32[]{:S(2)}) %collective-permute-start.3) | collective-permute-done | bytes 524320 | tf_op jit(solution)/shard_map/ppermute | solution.py:235
  149.4 9.0 %expert_b.1 = (bf16[4,512,128]{2,1,0:T(8,128)(2,1)}, bf16[4,512,128]{2,1,0:T(8,128)(2,1)}, bf16[4,512,128]{2,1,0:T(8,128)(2,1)}, bf16[4,512,128]{2,1,0:T(8,128)(2,1)}) custom-call(s32[1]{0:T(128)} %bitcast.13.refs_0_, bf16[4,512,128]{2,1,0:T(8,128)(2,1)} %bitcast.36, bf16[4,512,128]{2,1,0:T(8,128)(2,1)} %copy-done.2, bf16[4,512,128]{2,1,0:T(8,128)(2,1)} %copy-done.3, ...), custom_call_target="tpu_custom_call" | custom-call | tf_op jit(solution)/shard_map/expert_b/pallas_call | solution.py:162
  162.4 3.2 %collective-permute-start.4 = (bf16[4,512,128]{2,1,0:T(8,128)(2,1)}, bf16[4,512,128]{2,1,0:T(8,128)(2,1)S(1)}, u32[]{:S(2)}, u32[]{:S(2)}) collective-permute-start(bf16[4,512,128]{2,1,0:T(8,128)(2,1)} %get-tuple-element.26), channel_id=1, source_target_pairs={{0,1},{1,2},{2,3},{3,0},{4,5},{5,6},{6,7},{7,4},{8,9},{9,10},{10,1... | collective-permute-start | bytes 1572872 | tf_op jit(solution)/shard_map/ppermute | solution.py:235
  165.6 6.0 %collective-permute-done.6 = bf16[4,512,128]{2,1,0:T(8,128)(2,1)S(1)} collective-permute-done((bf16[4,512,128]{2,1,0:T(8,128)(2,1)}, bf16[4,512,128]{2,1,0:T(8,128)(2,1)S(1)}, u32[]{:S(2)}, u32[]{:S(2)}) %collective-permute-start.6) | collective-permute-done | bytes 524320 | tf_op jit(solution)/shard_map/ppermute | solution.py:235
  171.6 2.9 %collective-permute-done.5 = bf16[4,512,128]{2,1,0:T(8,128)(2,1)S(1)} collective-permute-done((bf16[4,512,128]{2,1,0:T(8,128)(2,1)}, bf16[4,512,128]{2,1,0:T(8,128)(2,1)S(1)}, u32[]{:S(2)}, u32[]{:S(2)}) %collective-permute-start.5) | collective-permute-done | bytes 524320 | tf_op jit(solution)/shard_map/ppermute | solution.py:235
  174.5 14.5 %collective-permute-done.4 = bf16[4,512,128]{2,1,0:T(8,128)(2,1)S(1)} collective-permute-done((bf16[4,512,128]{2,1,0:T(8,128)(2,1)}, bf16[4,512,128]{2,1,0:T(8,128)(2,1)S(1)}, u32[]{:S(2)}, u32[]{:S(2)}) %collective-permute-start.4) | collective-permute-done | bytes 524320 | tf_op jit(solution)/shard_map/ppermute | solution.py:235
  190.3 2.9 %reduce_sum.33 = bf16[4,512,128]{2,1,0:T(8,128)(2,1)} reduce(bf16[4,4,512,128]{3,2,1,0:T(8,128)(2,1)} %all-to-all-done.3, bf16[]{:T(256)} %constant.25.clone.1), dimensions={0}, to_apply=%region_0.0 | reduce | flops 786432 | bytes 2621442 | tf_op jit(solution)/shard_map/reduce_sum | solution.py:264
  193.2 3.6 %all-to-all-start.4 = ((bf16[4,512,128]{2,1,0:T(8,128)(2,1)}), bf16[4,512,128]{2,1,0:T(8,128)(2,1)S(1)}, u32[]{:S(2)}, u32[]{:S(2)}) async-start(bf16[4,512,128]{2,1,0:T(8,128)(2,1)} %reduce_sum.33), calls=%async_computation.4 | async-start | bytes 1048576 | tf_op jit(solution)/shard_map/all_to_all | solution.py:218
  196.9 7.0 %collective-permute-start.10 = (bf16[512,128]{1,0:T(8,128)(2,1)S(1)}, bf16[512,128]{1,0:T(8,128)(2,1)S(1)}, u32[]{:S(2)}, u32[]{:S(2)}) collective-permute-start(bf16[512,128]{1,0:T(8,128)(2,1)S(1)} %get-tuple-element.32), channel_id=1, source_target_pairs={{0,28},{4,16},{8,20},{12,24},{16,12},{20,0},{24,4},{28,8},{1,29},{... | collective-permute-start | bytes 393224 | tf_op jit(solution)/shard_map/ppermute | solution.py:240
  203.9 2.7 collective-permute-start.9
  208.5 2.4 collective-permute-start.7
  213.1 2.7 collective-permute-done.8
  216.5 10.6 %all-to-all-start.6 = ((bf16[16,32,128]{2,1,0:T(8,128)(2,1)}), bf16[16,32,128]{2,1,0:T(8,128)(2,1)S(1)}, u32[]{:S(2)}, u32[]{:S(2)}) async-start(bf16[16,32,128]{2,1,0:T(8,128)(2,1)} %bitcast.19), calls=%async_computation.6 | async-start | bytes 262144 | tf_op jit(solution)/shard_map/all_to_all | solution.py:218
  227.2 12.0 %all-to-all-done.6 = bf16[16,32,128]{2,1,0:T(8,128)(2,1)S(1)} async-done(((bf16[16,32,128]{2,1,0:T(8,128)(2,1)}), bf16[16,32,128]{2,1,0:T(8,128)(2,1)S(1)}, u32[]{:S(2)}, u32[]{:S(2)}) %all-to-all-start.6) | async-done | bytes 131104 | tf_op jit(solution)/shard_map/all_to_all | solution.py:218
  239.2 18.4 %all_to_all.42 = bf16[16,32,128]{2,1,0:T(8,128)(2,1)} all-to-all(bf16[16,32,128]{2,1,0:T(8,128)(2,1)S(1)} %bitcast.41), channel_id=1, replica_groups=mesh['z'=16,'c'=2,'y'=4,'x'=4] {'z'}, dimensions={0} | all-to-all | bytes 262144 | tf_op jit(solution)/shard_map/all_to_all | solution.py:218
  257.6 2.2 combine.1
  261.0 5.1 %all-to-all-start.7 = ((f32[16,1,256]{2,1,0:T(1,128)}), f32[16,1,256]{2,1,0:T(1,128)S(1)}, u32[]{:S(2)}, u32[]{:S(2)}) async-start(f32[16,1,256]{2,1,0:T(1,128)} %broadcast_in_dim.8), calls=%async_computation.7 | async-start | bytes 32768 | tf_op jit(solution)/shard_map/all_to_all | solution.py:218
  266.2 6.4 %all-to-all-done.7 = f32[16,1,256]{2,1,0:T(1,128)S(1)} async-done(((f32[16,1,256]{2,1,0:T(1,128)}), f32[16,1,256]{2,1,0:T(1,128)S(1)}, u32[]{:S(2)}, u32[]{:S(2)}) %all-to-all-start.7) | async-done | bytes 16416 | tf_op jit(solution)/shard_map/all_to_all | solution.py:218
  (35 shorter events, 18.4 us)
Async XLA Ops:
  2.1 27.7 %all-to-all-start = ((bf16[16,32,128]{2,1,0:T(8,128)(2,1)}), bf16[16,32,128]{2,1,0:T(8,128)(2,1)S(1)}, u32[]{:S(2)}, u32[]{:S(2)}) async-start(bf16[16,32,128]{2,1,0:T(8,128)(2,1)} %bitcast.42), calls=%async_computation | async-start | bytes 262144 | tf_op jit(solution)/shard_map/all_to_all | solution.py:218
  17.9 4.2 %collective-permute-start = (bf16[512,128]{1,0:T(8,128)(2,1)}, bf16[512,128]{1,0:T(8,128)(2,1)}, u32[]{:S(2)}, u32[]{:S(2)}) collective-permute-start(bf16[512,128]{1,0:T(8,128)(2,1)} %get-tuple-element.20), channel_id=1, source_target_pairs={{0,16},{16,0},{1,17},{17,1},{2,18},{18,2},{3,19},{19,3},{4,20},{20... | collective-permute-start | bytes 393224 | tf_op jit(solution)/shard_map/ppermute | solution.py:235
  29.8 18.2 %all-to-all-start.1 = ((bf16[16,32,128]{2,1,0:T(8,128)(2,1)}), bf16[16,32,128]{2,1,0:T(8,128)(2,1)S(1)}, u32[]{:S(2)}, u32[]{:S(2)}) async-start(bf16[16,32,128]{2,1,0:T(8,128)(2,1)} %bitcast.6), calls=%async_computation.1 | async-start | bytes 262144 | tf_op jit(solution)/shard_map/all_to_all | solution.py:218
  83.8 106.5 %all-to-all-start.3 = ((bf16[4,4,512,128]{3,2,1,0:T(8,128)(2,1)}), bf16[4,4,512,128]{3,2,1,0:T(8,128)(2,1)}, u32[]{:S(2)}, u32[]{:S(2)}) async-start(bf16[4,4,512,128]{3,2,1,0:T(8,128)(2,1)} %get-tuple-element.22), calls=%async_computation.3 | async-start | bytes 4194304 | tf_op jit(solution)/shard_map/all_to_all | solution.py:218
  117.9 31.6 %copy-start = (bf16[2048,128]{1,0:T(8,128)(2,1)}, bf16[2048,128]{1,0:T(8,128)(2,1)S(1)}, u32[]{:S(2)}) copy-start(bf16[2048,128]{1,0:T(8,128)(2,1)S(1)} %all-gather.1) | copy-start | bytes 1572868
  117.9 12.4 %collective-permute-start.1 = (bf16[4,512,128]{2,1,0:T(8,128)(2,1)S(1)}, bf16[4,512,128]{2,1,0:T(8,128)(2,1)S(1)}, u32[]{:S(2)}, u32[]{:S(2)}) collective-permute-start(bf16[4,512,128]{2,1,0:T(8,128)(2,1)S(1)} %bitcast.33), channel_id=1, source_target_pairs={{0,3},{1,0},{2,1},{3,2},{4,7},{5,4},{6,5},{7,6},{8,11},{9,8},{10,9... | collective-permute-start | bytes 1572872 | tf_op jit(solution)/shard_map/ppermute | solution.py:235
  122.0 11.5 %collective-permute-start.2 = (bf16[4,512,128]{2,1,0:T(8,128)(2,1)S(1)}, bf16[4,512,128]{2,1,0:T(8,128)(2,1)S(1)}, u32[]{:S(2)}, u32[]{:S(2)}) collective-permute-start(bf16[4,512,128]{2,1,0:T(8,128)(2,1)S(1)} %bitcast.34), channel_id=1, source_target_pairs={{0,2},{1,3},{2,0},{3,1},{4,6},{5,7},{6,4},{7,5},{8,10},{9,11},{10,... | collective-permute-start | bytes 1572872 | tf_op jit(solution)/shard_map/ppermute | solution.py:235
  124.5 24.2 %collective-permute-start.3 = (bf16[4,512,128]{2,1,0:T(8,128)(2,1)S(1)}, bf16[4,512,128]{2,1,0:T(8,128)(2,1)S(1)}, u32[]{:S(2)}, u32[]{:S(2)}) collective-permute-start(bf16[4,512,128]{2,1,0:T(8,128)(2,1)S(1)} %bitcast.35), channel_id=1, source_target_pairs={{0,1},{1,2},{2,3},{3,0},{4,5},{5,6},{6,7},{7,4},{8,9},{9,10},{10,1... | collective-permute-start | bytes 1572872 | tf_op jit(solution)/shard_map/ppermute | solution.py:235
  130.2 18.4 %copy-start.2 = (bf16[4,512,128]{2,1,0:T(8,128)(2,1)}, bf16[4,512,128]{2,1,0:T(8,128)(2,1)S(1)}, u32[]{:S(2)}) copy-start(bf16[4,512,128]{2,1,0:T(8,128)(2,1)S(1)} %collective-permute-done.1.refs_2_) | copy-start | bytes 1572868
  133.6 15.1 %copy-start.3 = (bf16[4,512,128]{2,1,0:T(8,128)(2,1)}, bf16[4,512,128]{2,1,0:T(8,128)(2,1)S(1)}, u32[]{:S(2)}) copy-start(bf16[4,512,128]{2,1,0:T(8,128)(2,1)S(1)} %collective-permute-done.2.refs_3_) | copy-start | bytes 1572868
  148.6 0.8 copy-start.4
  158.4 13.2 %collective-permute-start.6 = (bf16[4,512,128]{2,1,0:T(8,128)(2,1)}, bf16[4,512,128]{2,1,0:T(8,128)(2,1)S(1)}, u32[]{:S(2)}, u32[]{:S(2)}) collective-permute-start(bf16[4,512,128]{2,1,0:T(8,128)(2,1)} %get-tuple-element.28), channel_id=1, source_target_pairs={{0,3},{1,0},{2,1},{3,2},{4,7},{5,4},{6,5},{7,6},{8,11},{9,8},{10,9... | collective-permute-start | bytes 1572872 | tf_op jit(solution)/shard_map/ppermute | solution.py:235
  160.3 14.2 %collective-permute-start.5 = (bf16[4,512,128]{2,1,0:T(8,128)(2,1)}, bf16[4,512,128]{2,1,0:T(8,128)(2,1)S(1)}, u32[]{:S(2)}, u32[]{:S(2)}) collective-permute-start(bf16[4,512,128]{2,1,0:T(8,128)(2,1)} %get-tuple-element.27), channel_id=1, source_target_pairs={{0,2},{1,3},{2,0},{3,1},{4,6},{5,7},{6,4},{7,5},{8,10},{9,11},{10,... | collective-permute-start | bytes 1572872 | tf_op jit(solution)/shard_map/ppermute | solution.py:235
  162.4 26.6 %collective-permute-start.4 = (bf16[4,512,128]{2,1,0:T(8,128)(2,1)}, bf16[4,512,128]{2,1,0:T(8,128)(2,1)S(1)}, u32[]{:S(2)}, u32[]{:S(2)}) collective-permute-start(bf16[4,512,128]{2,1,0:T(8,128)(2,1)} %get-tuple-element.26), channel_id=1, source_target_pairs={{0,1},{1,2},{2,3},{3,0},{4,5},{5,6},{6,7},{7,4},{8,9},{9,10},{10,1... | collective-permute-start | bytes 1572872 | tf_op jit(solution)/shard_map/ppermute | solution.py:235
  193.2 72.9 %copy-start.5 = (bf16[128]{0:T(256)(128)(2,1)S(1)}, bf16[128]{0:T(256)(128)(2,1)}, u32[]{:S(2)}) copy-start(bf16[128]{0:T(256)(128)(2,1)} %param.15) | copy-start | bytes 772
  193.2 23.3 %all-to-all-start.4 = ((bf16[4,512,128]{2,1,0:T(8,128)(2,1)}), bf16[4,512,128]{2,1,0:T(8,128)(2,1)S(1)}, u32[]{:S(2)}, u32[]{:S(2)}) async-start(bf16[4,512,128]{2,1,0:T(8,128)(2,1)} %reduce_sum.33), calls=%async_computation.4 | async-start | bytes 1048576 | tf_op jit(solution)/shard_map/all_to_all | solution.py:218
  196.9 14.1 %collective-permute-start.10 = (bf16[512,128]{1,0:T(8,128)(2,1)S(1)}, bf16[512,128]{1,0:T(8,128)(2,1)S(1)}, u32[]{:S(2)}, u32[]{:S(2)}) collective-permute-start(bf16[512,128]{1,0:T(8,128)(2,1)S(1)} %get-tuple-element.32), channel_id=1, source_target_pairs={{0,28},{4,16},{8,20},{12,24},{16,12},{20,0},{24,4},{28,8},{1,29},{... | collective-permute-start | bytes 393224 | tf_op jit(solution)/shard_map/ppermute | solution.py:240
  203.9 9.2 %collective-permute-start.9 = (bf16[512,128]{1,0:T(8,128)(2,1)S(1)}, bf16[512,128]{1,0:T(8,128)(2,1)S(1)}, u32[]{:S(2)}, u32[]{:S(2)}) collective-permute-start(bf16[512,128]{1,0:T(8,128)(2,1)S(1)} %get-tuple-element.33), channel_id=1, source_target_pairs={{0,24},{4,28},{8,16},{12,20},{16,8},{20,12},{24,0},{28,4},{1,25},{... | collective-permute-start | bytes 393224 | tf_op jit(solution)/shard_map/ppermute | solution.py:240
  206.6 9.2 %collective-permute-start.8 = (bf16[512,128]{1,0:T(8,128)(2,1)S(1)}, bf16[512,128]{1,0:T(8,128)(2,1)S(1)}, u32[]{:S(2)}, u32[]{:S(2)}) collective-permute-start(bf16[512,128]{1,0:T(8,128)(2,1)S(1)} %get-tuple-element.34), channel_id=1, source_target_pairs={{0,20},{4,24},{8,28},{12,16},{16,4},{20,8},{24,12},{28,0},{1,21},{... | collective-permute-start | bytes 393224 | tf_op jit(solution)/shard_map/ppermute | solution.py:240
  208.5 7.3 %collective-permute-start.7 = (bf16[512,128]{1,0:T(8,128)(2,1)S(1)}, bf16[512,128]{1,0:T(8,128)(2,1)S(1)}, u32[]{:S(2)}, u32[]{:S(2)}) collective-permute-start(bf16[512,128]{1,0:T(8,128)(2,1)S(1)} %get-tuple-element.31), channel_id=1, source_target_pairs={{0,16},{4,20},{8,24},{12,28},{16,0},{20,4},{24,8},{28,12},{1,17},{... | collective-permute-start | bytes 393224 | tf_op jit(solution)/shard_map/ppermute | solution.py:240
  216.5 22.7 %all-to-all-start.6 = ((bf16[16,32,128]{2,1,0:T(8,128)(2,1)}), bf16[16,32,128]{2,1,0:T(8,128)(2,1)S(1)}, u32[]{:S(2)}, u32[]{:S(2)}) async-start(bf16[16,32,128]{2,1,0:T(8,128)(2,1)} %bitcast.19), calls=%async_computation.6 | async-start | bytes 262144 | tf_op jit(solution)/shard_map/all_to_all | solution.py:218
  239.2 18.4 %copy-start.1 = (bf16[16,32,128]{2,1,0:T(8,128)(2,1)}, bf16[16,32,128]{2,1,0:T(8,128)(2,1)S(1)}, u32[]{:S(2)}) copy-start(bf16[16,32,128]{2,1,0:T(8,128)(2,1)S(1)} %all-to-all-done.6) | copy-start | bytes 393220
  261.0 11.5 %all-to-all-start.7 = ((f32[16,1,256]{2,1,0:T(1,128)}), f32[16,1,256]{2,1,0:T(1,128)S(1)}, u32[]{:S(2)}, u32[]{:S(2)}) async-start(f32[16,1,256]{2,1,0:T(1,128)} %broadcast_in_dim.8), calls=%async_computation.7 | async-start | bytes 32768 | tf_op jit(solution)/shard_map/all_to_all | solution.py:218
where the time goes:
time: 279 us; the launch traced here: 274 us
  blocking collectives  86.5 us (31%)
  starting transfers between devices  78.7 us (28%)
  waiting for transfers between devices  77.4 us (28%)
  Pallas kernels  21.7 us (8%)
  other arithmetic  6.68 us (2%)
  local copies, waits for them, and re-layouts  3.08 us (1%)
    ppermute x7, waiting for transfers between devices, shift(): return lax.ppermute(v, axis, [(i, (i + step) % n) for i in range(n)])  46.3 us
    all_to_all x6, starting transfers between devices, exchange(): return lax.all_to_all(v, axis, split_axis=0, concat_axis=0, tiled=True)  45.5 us
    all_to_all x2, blocking collectives, exchange(): return lax.all_to_all(v, axis, split_axis=0, concat_axis=0, tiled=True)  45.4 us
    all_gather x1, blocking collectives, local(): b = lax.all_gather(far, 'y')  29.6 us
    all_to_all x6, waiting for transfers between devices, exchange(): return lax.all_to_all(v, axis, split_axis=0, concat_axis=0, tiled=True)  26.2 us
    ppermute x7, starting transfers between devices, shift(): return lax.ppermute(v, axis, [(i, (i + step) % n) for i in range(n)])  19.2 us
    pallas_call x2, Pallas kernels, expert(): pl.pallas_call(functools.partial(expert_kernel, first, rows), out_shape=o...  17.4 us
    ppermute x4, starting transfers between devices, cross(): return lax.ppermute(v, ('c', 'y'), pairs)  14 us
  transfers between devices with their start and end apart: 17, of which 12 were waited for; matrix products, arithmetic and copies ran while one was open for 1% of the time, Pallas kernels for 3%

commit v1 on v0

--- a/solution.py
+++ b/solution.py
@@ -65,37 +65,58 @@
 
 
 def expert_kernel(first, rows, *refs):
+    where = refs[0]
+    xs = refs[1:5]
+    wg, wu, wd = refs[5:8]
+    refs = refs[8:]
     if first:
-        xs, wg, wu, wd, out, gain_out = refs[:6]
-        refs = refs[6:]
+        outs = refs[0:1]
+        gain_out = refs[1]
+        refs = refs[2:]
     else:
-        pos = refs[0]
-        xs = refs[1:5]
-        wg, wu, wd, gain_in = refs[5:9]
-        outs = refs[9:13]
-        refs = refs[13:]
+        gain_in = refs[0]
+        outs = refs[1:5]
+        refs = refs[5:]
     raw, gain_s, xn, g_s, u_s, d_s, stage, sems, osems = refs
+    core = where[0]
+    at_outer = where[1]
+
+    def block(step, inner):
+        outer = jnp.bitwise_and(at_outer + step, 3)
+        return jnp.where(core == 0, outer * 4 + inner, inner * 4 + outer)
 
     def fetch(n, src, dst):
         cp = pltpu.make_async_copy(src, dst, sems.at[n])
         cp.start()
         return cp
 
-    if first:
-        gain_cp = fetch(0, xs.at[:, :, pl.ds(rows, GAIN_ROWS), :], gain_s)
-        x_cp = [fetch(1, xs.at[:, :, pl.ds(0, rows), :], raw)]
-    else:
-        gain_cp = fetch(0, gain_in, gain_s)
-        x_cp = [fetch(1 + s, xs[s], raw.at[lax.rem(pos[0] + s, 4)]) for s in range(4)]
-    g_cp = fetch(5, wg, g_s)
-    u_cp = fetch(6, wu, u_s)
-    d_cp = fetch(7, wd, d_s)
-    gain_cp.wait()
+    gain_cp = []
+    x_cp = []
+    for s in range(4):
+        for i in range(4):
+            n = s * 4 + i
+            j = block(s, i)
+            x_cp.append(fetch(n, xs[s].at[i, pl.ds(0, rows), :], raw.at[j]))
+            if first:
+                gain_cp.append(
+                    fetch(16 + n, xs[s].at[i, pl.ds(rows, GAIN_ROWS), :], gain_s.at[j])
+                )
+    if not first:
+        gain_cp.append(fetch(16, gain_in, gain_s))
+    g_cp = fetch(32, wg, g_s)
+    u_cp = fetch(33, wu, u_s)
+    d_cp = fetch(34, wd, d_s)
+    for cp in gain_cp:
+        cp.wait()
     copies = []
-    if first:
-        cp = pltpu.make_async_copy(gain_s, gain_out, osems.at[4])
+
+    def store(n, src, dst):
+        cp = pltpu.make_async_copy(src, dst, osems.at[n])
         cp.start()
         copies.append(cp)
+
+    if first:
+        store(16, gain_s, gain_out)
     width = xn.shape[1]
     step = 32
     for cp in x_cp:
@@ -106,13 +127,12 @@
         acc = jnp.zeros((step, 128), F32)
         vals = []
         for j in range(16):
-            a, b = (j // 4, j % 4) if first else (j % 4, j // 4)
-            v = raw[a, b, pl.ds(at, step), :].astype(F32)
+            v = raw[j, pl.ds(at, step), :].astype(F32)
             vals.append(v)
             acc = acc + v * v
         scale = lax.rsqrt(jnp.sum(acc, axis=1, keepdims=True) * (1.0 / width) + EPS)
         for j in range(16):
-            gain = gain_s[j // 4, j % 4, 0:1, :].astype(F32)
+            gain = gain_s[j, 0:1, :].astype(F32)
             xn[pl.ds(at, step), j * 128 : (j + 1) * 128] = (vals[j] * scale * gain).astype(BF16)
         return 0
 
@@ -128,55 +148,50 @@
             hidden, d_s[:, y * 512 : (y + 1) * 512], preferred_element_type=F32
         ).astype(BF16)
         for x in range(4):
-            part = res[:, x * 128 : (x + 1) * 128]
+            stage[y * 4 + x] = res[:, x * 128 : (x + 1) * 128]
             if first:
-                stage[y, x] = part
-            else:
-                stage[x, y] = part
-        if first:
-            cp = pltpu.make_async_copy(stage.at[y], out.at[y], osems.at[y])
-            cp.start()
-            copies.append(cp)
+                outer = jnp.where(core == 0, y, x)
+                inner = jnp.where(core == 0, x, y)
+                store(y * 4 + x, stage.at[y * 4 + x], outs[0].at[outer, inner])
     if not first:
         for s in range(4):
-            cp = pltpu.make_async_copy(stage.at[lax.rem(pos[0] + s, 4)], outs[s], osems.at[s])
-            cp.start()
-            copies.append(cp)
+            for i in range(4):
+                store(s * 4 + i, stage.at[block(s, i)], outs[s].at[i])
     for cp in copies:
         cp.wait()
 
 
-def expert(first, pos, xs, weights, gain):
+def expert(first, where, xs, weights, gain):
     rows = 512
     width, units = weights[0].shape
     hbm = pl.BlockSpec(memory_space=pltpu.HBM)
-    gain_type = jax.ShapeDtypeStruct((4, 4, GAIN_ROWS, 128), BF16)
     if first:
-        args = (xs, *weights)
-        in_specs = [hbm] * 4
-        outs = (jax.ShapeDtypeStruct((4, 4, rows, 128), BF16), gain_type)
+        args = (where, *xs, *weights)
+        outs = (
+            jax.ShapeDtypeStruct((4, 4, rows, 128), BF16),
+            jax.ShapeDtypeStruct((16, GAIN_ROWS, 128), BF16),
+        )
     else:
-        args = (pos, *xs, *weights, gain)
-        in_specs = [pl.BlockSpec(memory_space=pltpu.SMEM)] + [hbm] * 8
+        args = (where, *xs, *weights, gain)
         outs = tuple([jax.ShapeDtypeStruct((4, rows, 128), BF16)] * 4)
     return pl.pallas_call(
         functools.partial(expert_kernel, first, rows),
         out_shape=outs,
-        in_specs=in_specs,
+        in_specs=[pl.BlockSpec(memory_space=pltpu.SMEM)] + [hbm] * (len(args) - 1),
         out_specs=tuple([hbm] * len(outs)),
         scratch_shapes=[
-            pltpu.VMEM((4, 4, rows, 128), BF16),
-            pltpu.VMEM((4, 4, GAIN_ROWS, 128), BF16),
+            pltpu.VMEM((16, rows, 128), BF16),
+            pltpu.VMEM((16, GAIN_ROWS, 128), BF16),
             pltpu.VMEM((rows, width), BF16),
             pltpu.VMEM((width, units), BF16),
             pltpu.VMEM((width, units), BF16),
             pltpu.VMEM((units, width), BF16),
-            pltpu.VMEM((4, 4, rows, 128), BF16),
-            pltpu.SemaphoreType.DMA((8,)),
-            pltpu.SemaphoreType.DMA((5,)),
+            pltpu.VMEM((16, rows, 128), BF16),
+            pltpu.SemaphoreType.DMA((35,)),
+            pltpu.SemaphoreType.DMA((17,)),
         ],
         compiler_params=pltpu.CompilerParams(vmem_limit_bytes=63 * 1024 * 1024),
-        name="expert_a" if first else "expert_b",
+        name="expert_far" if first else "expert_near",
     )(*args)
 
 
@@ -214,8 +229,51 @@
     )(table, near, far)
 
 
-def exchange(v, axis):
-    return lax.all_to_all(v, axis, split_axis=0, concat_axis=0, tiled=True)
+ALL = ("z", "c", "y", "x")
+
+
+def flat(z, c, y, x):
+    return ((z * 2 + c) * 4 + y) * 4 + x
+
+
+def lines(along_x_for):
+    groups = []
+    for z in range(16):
+        for c in range(2):
+            for i in range(4):
+                if c == along_x_for:
+                    groups.append([flat(z, c, i, x) for x in range(4)])
+                else:
+                    groups.append([flat(z, c, y, i) for y in range(4)])
+    return groups
+
+
+def exchange(v, axis, groups=None):
+    return lax.all_to_all(
+        v, axis, split_axis=0, concat_axis=0, tiled=True, axis_index_groups=groups
+    )
+
+
+def inner_exchange(v):
+    return exchange(v, ALL, lines(0))
+
+
+def outer_exchange(v):
+    return exchange(v, ALL, lines(1))
+
+
+def outer_shift(v, step):
+    pairs = []
+    for z in range(16):
+        for y in range(4):
+            for x in range(4):
+                pairs.append((flat(z, 0, y, x), flat(z, 0, (y + step) % 4, x)))
+                pairs.append((flat(z, 1, y, x), flat(z, 1, y, (x + step) % 4)))
+    return lax.ppermute(v, ALL, pairs)
+
+
+def swap(v):
+    return lax.ppermute(v, "c", [(0, 1), (1, 0)])
 
 
 def total_of(parts):
@@ -225,49 +283,41 @@
     return total.astype(BF16)
 
 
-def over_z(v):
-    n = lax.axis_size("z")
-    return exchange(v.reshape(n, v.shape[0] // n, v.shape[1]), "z").reshape(v.shape)
-
-
-def shift(v, axis, step):
-    n = lax.axis_size(axis)
-    return lax.ppermute(v, axis, [(i, (i + step) % n) for i in range(n)])
-
-
-def cross(v, step):
-    pairs = [(c * 4 + y, (1 - c) * 4 + (y + step) % 4) for c in range(2) for y in range(4)]
-    return lax.ppermute(v, ("c", "y"), pairs)
-
-
-def pick(v, i):
-    return lax.dynamic_index_in_dim(v, i, 0, keepdims=False, allow_negative_indices=False)
+def summed(v):
+    return v.astype(F32).sum(axis=0).astype(BF16)
+
+
+def over_z(near, far):
+    share = near.shape[1]
+    both = jnp.stack([near.reshape(16, -1, share), far.reshape(16, -1, share)], axis=1)
+    both = exchange(both, "z")
+    return both[:, 0].reshape(near.shape), both[:, 1].reshape(far.shape)
 
 
 def local(tokens, norm_gain, w_gate, w_up, w_down, routes, route_weights, final_gain):
     tok, share = tokens.shape
     width = share * 16
     c = lax.axis_index("c").astype(jnp.int32)
-    pos = lax.axis_index("x").astype(jnp.int32).reshape(1)
+    y = lax.axis_index("y").astype(jnp.int32)
+    x = lax.axis_index("x").astype(jnp.int32)
+    where = jnp.stack([c, jnp.where(c == 0, y, x)])
     near, far, table = pack(c.reshape(1), routes.T, route_weights.T, tokens)
     weights = (w_gate[0], w_up[0], w_down[0])
-    near = over_z(near)
-    far = over_z(shift(far, "c", 1))
+    near, far = over_z(near, swap(far))
     gain_rows = jnp.broadcast_to(norm_gain[None, :], (GAIN_ROWS, share))
-    a = lax.all_gather(jnp.concatenate([near, gain_rows], axis=0), "x")
-    a, far = lax.optimization_barrier((a, far))
-    a = exchange(jnp.broadcast_to(a[None], (4, *a.shape)), "y")
-    b = lax.all_gather(far, "y")
-    b = [b] + [shift(b, "x", -s) for s in (1, 2, 3)]
-    a, gain = expert(True, None, a, weights, None)
-    b = expert(False, pos, b, weights, gain)
-    a = exchange(a, "y").astype(F32).sum(axis=0).astype(BF16)
-    a = exchange(a, "x").astype(F32).sum(axis=0).astype(BF16)
-    near = over_z(a)
-    b = total_of([b[0]] + [shift(b[s], "x", s) for s in (1, 2, 3)])
-    y = lax.axis_index("y").astype(jnp.int32)
-    b = total_of([cross(pick(b, jnp.bitwise_and(y + s, 3)), s) for s in range(4)])
-    far = over_z(b)
+    rows = jnp.concatenate([far, gain_rows, near], axis=0)
+    rows = inner_exchange(jnp.broadcast_to(rows[None], (4, *rows.shape)))
+    first = far.shape[0] + GAIN_ROWS
+    far, near = rows[:, :first], rows[:, first:]
+    far = [far] + [outer_shift(far, -s) for s in (1, 2, 3)]
+    near = [near] + [outer_shift(near, -s) for s in (1, 2, 3)]
+    far, gain = expert(True, where, far, weights, None)
+    far = summed(outer_exchange(far))
+    near = expert(False, where, near, weights, gain)
+    near = total_of([near[0]] + [outer_shift(near[s], s) for s in (1, 2, 3)])
+    far = swap(summed(inner_exchange(far)))
+    near = summed(inner_exchange(near))
+    near, far = over_z(near, far)
     combined, squares = combine(table, near, far)
     copies = jnp.broadcast_to(squares, (16, tok))
     total = exchange(copies, ("y", "x")).sum(axis=0)

time: 279 us -> 212 us (0.76)
  the two profiles are of different devices: /device:TPU:1 before, /device:TPU:32 now
where the time goes in v1:
time: 212 us; the launch traced here: 211 us
  blocking collectives  68.9 us (33%)
  waiting for transfers between devices  53 us (25%)
  starting transfers between devices  51.5 us (24%)
  Pallas kernels  23.9 us (11%)
  other arithmetic  7.36 us (3%)
  local copies, waits for them, and re-layouts  5.97 us (3%)
    all_to_all x3, blocking collectives, exchange(): lax.all_to_all(v, axis, split_axis=0, concat_axis=0, tiled=True, axis_ind...  68.9 us
    ppermute x9, waiting for transfers between devices, outer_shift(): return lax.ppermute(v, ALL, pairs)  37.9 us
    ppermute x9, starting transfers between devices, outer_shift(): return lax.ppermute(v, ALL, pairs)  30.3 us
    pallas_call x2, Pallas kernels, expert(): pl.pallas_call(functools.partial(expert_kernel, first, rows), out_shape=o...  19.6 us
    all_to_all x4, starting transfers between devices, exchange(): lax.all_to_all(v, axis, split_axis=0, concat_axis=0, tiled=True, axis_ind...  17.4 us
    all_to_all x4, waiting for transfers between devices, exchange(): lax.all_to_all(v, axis, split_axis=0, concat_axis=0, tiled=True, axis_ind...  13.6 us
  transfers between devices with their start and end apart: 15, of which 11 were waited for; matrix products, arithmetic and copies ran while one was open for 3% of the time, Pallas kernels for 5%

profile of v1, /device:TPU:32, one launch (start us, length us, event | category | flops | bytes accessed | tf_op | source)
XLA Modules:
  0.0 210.9 jit_solution(5501448939769457883)
XLA Ops:
  0.0 2.1 %pack.1 = (bf16[512,128]{1,0:T(8,128)(2,1)}, bf16[512,128]{1,0:T(8,128)(2,1)}, f32[256,8]{1,0:T(8,128)}) custom-call(s32[1]{0:T(128)} %bitcast.pos, s32[2,256]{1,0:T(2,128)} %bitcast.36, f32[2,256]{1,0:T(2,128)} %bitcast.37, bf16[256,128]{1,0:T(8,128)(2,1)} %tokens.1), custom_call_target="tpu_custom_call" | custom-call | tf_op jit(solution)/shard_map/pack/pallas_call | solution.py:54
  2.1 1.9 collective-permute-start
  6.5 33.4 %all_to_all.36 = bf16[16,2,32,128]{3,2,1,0:T(8,128)(2,1)S(1)} all-to-all(bf16[16,2,32,128]{3,2,1,0:T(8,128)(2,1)S(1)} %pad_maximum_fusion.1), channel_id=1, replica_groups=mesh['z'=16,'c'=2,'y'=4,'x'=4] {'z'}, dimensions={0} | all-to-all | bytes 524288 | tf_op jit(solution)/shard_map/all_to_all | solution.py:252
  40.1 15.1 %all_to_all.37 = bf16[4,1040,128]{2,1,0:T(8,128)(2,1)S(1)} all-to-all(bf16[4,1040,128]{2,1,0:T(8,128)(2,1)S(1)} %broadcast_in_dim.7), channel_id=1, replica_groups={{0,1,2,3},{4,5,6,7},{8,9,10,11},{12,13,14,15},{16,20,24,28},{17,21,25,2..., dimensions={0} | all-to-all | bytes 2129920 | tf_op jit(solution)/shard_map/all_to_all | solution.py:252
  56.2 4.9 %collective-permute-start.4 = (bf16[4,528,128]{2,1,0:T(8,128)(2,1)S(1)}, bf16[4,528,128]{2,1,0:T(8,128)(2,1)S(1)}, u32[]{:S(2)}, u32[]{:S(2)}) collective-permute-start(bf16[4,528,128]{2,1,0:T(8,128)(2,1)S(1)} %slice.27.refs_1_), channel_id=1, source_target_pairs={{0,12},{16,19},{1,13},{17,16},{2,14},{18,17},{3,15},{19,18},{4,0},... | collective-permute-start | bytes 1622024 | tf_op jit(solution)/shard_map/ppermute | solution.py:272
  61.2 2.5 %collective-permute-start.5 = (bf16[4,528,128]{2,1,0:T(8,128)(2,1)S(1)}, bf16[4,528,128]{2,1,0:T(8,128)(2,1)S(1)}, u32[]{:S(2)}, u32[]{:S(2)}) collective-permute-start(bf16[4,528,128]{2,1,0:T(8,128)(2,1)S(1)} %slice.27.refs_1_), channel_id=1, source_target_pairs={{0,8},{16,18},{1,9},{17,19},{2,10},{18,16},{3,11},{19,17},{4,12},{... | collective-permute-start | bytes 1622024 | tf_op jit(solution)/shard_map/ppermute | solution.py:272
  63.7 2.9 %collective-permute-start.6 = (bf16[4,528,128]{2,1,0:T(8,128)(2,1)S(1)}, bf16[4,528,128]{2,1,0:T(8,128)(2,1)S(1)}, u32[]{:S(2)}, u32[]{:S(2)}) collective-permute-start(bf16[4,528,128]{2,1,0:T(8,128)(2,1)S(1)} %slice.27.refs_1_), channel_id=1, source_target_pairs={{0,4},{16,17},{1,5},{17,18},{2,6},{18,19},{3,7},{19,16},{4,8},{20,... | collective-permute-start | bytes 1622024 | tf_op jit(solution)/shard_map/ppermute | solution.py:272
  67.2 6.6 %collective-permute-done.4.refs_2_ = bf16[4,528,128]{2,1,0:T(8,128)(2,1)S(1)} collective-permute-done((bf16[4,528,128]{2,1,0:T(8,128)(2,1)S(1)}, bf16[4,528,128]{2,1,0:T(8,128)(2,1)S(1)}, u32[]{:S(2)}, u32[]{:S(2)}) %collective-permute-start.4) | collective-permute-done | bytes 540704 | tf_op jit(solution)/shard_map/ppermute | solution.py:272
  74.0 5.7 %collective-permute-done.6.refs_4_ = bf16[4,528,128]{2,1,0:T(8,128)(2,1)S(1)} collective-permute-done((bf16[4,528,128]{2,1,0:T(8,128)(2,1)S(1)}, bf16[4,528,128]{2,1,0:T(8,128)(2,1)S(1)}, u32[]{:S(2)}, u32[]{:S(2)}) %collective-permute-start.6) | collective-permute-done | bytes 540704 | tf_op jit(solution)/shard_map/ppermute | solution.py:272
  80.5 9.6 %expert_far.1 = (bf16[4,4,512,128]{3,2,1,0:T(8,128)(2,1)}, bf16[16,16,128]{2,1,0:T(8,128)(2,1)}) custom-call(s32[2]{0:T(128)} %pad_add_fusion.refs_0_, bf16[4,528,128]{2,1,0:T(8,128)(2,1)} %copy-done.1, bf16[4,528,128]{2,1,0:T(8,128)(2,1)} %copy-done.3, bf16[4,528,128]{2,1,0:T(8,128)(2,1)} %copy-done.4, bf16[4,528,128]{2,1,0:T(8,128)(2,1)} %copy-done.5, ...), custom_call_target="tpu_custom_call" | custom-call | tf_op jit(solution)/shard_map/expert_far/pallas_call | solution.py:177
  90.2 4.5 %all-to-all-start.3 = ((bf16[4,4,512,128]{3,2,1,0:T(8,128)(2,1)}), bf16[4,4,512,128]{3,2,1,0:T(8,128)(2,1)}, u32[]{:S(2)}, u32[]{:S(2)}) async-start(bf16[4,4,512,128]{3,2,1,0:T(8,128)(2,1)} %get-tuple-element.24), calls=%async_computation.3 | async-start | bytes 4194304 | tf_op jit(solution)/shard_map/all_to_all | solution.py:252
  95.7 5.1 %collective-permute-start.1 = (bf16[4,512,128]{2,1,0:T(8,128)(2,1)S(1)}, bf16[4,512,128]{2,1,0:T(8,128)(2,1)S(1)}, u32[]{:S(2)}, u32[]{:S(2)}) collective-permute-start(bf16[4,512,128]{2,1,0:T(8,128)(2,1)S(1)} %slice.26.refs_1_), channel_id=1, source_target_pairs={{0,12},{16,19},{1,13},{17,16},{2,14},{18,17},{3,15},{19,18},{4,0},... | collective-permute-start | bytes 1572872 | tf_op jit(solution)/shard_map/ppermute | solution.py:272
  100.8 2.8 %collective-permute-start.2 = (bf16[4,512,128]{2,1,0:T(8,128)(2,1)S(1)}, bf16[4,512,128]{2,1,0:T(8,128)(2,1)S(1)}, u32[]{:S(2)}, u32[]{:S(2)}) collective-permute-start(bf16[4,512,128]{2,1,0:T(8,128)(2,1)S(1)} %slice.26.refs_1_), channel_id=1, source_target_pairs={{0,8},{16,18},{1,9},{17,19},{2,10},{18,16},{3,11},{19,17},{4,12},{... | collective-permute-start | bytes 1572872 | tf_op jit(solution)/shard_map/ppermute | solution.py:272
  103.6 2.8 %collective-permute-start.3 = (bf16[4,512,128]{2,1,0:T(8,128)(2,1)S(1)}, bf16[4,512,128]{2,1,0:T(8,128)(2,1)S(1)}, u32[]{:S(2)}, u32[]{:S(2)}) collective-permute-start(bf16[4,512,128]{2,1,0:T(8,128)(2,1)S(1)} %slice.26.refs_1_), channel_id=1, source_target_pairs={{0,4},{16,17},{1,5},{17,18},{2,6},{18,19},{3,7},{19,16},{4,8},{20,... | collective-permute-start | bytes 1572872 | tf_op jit(solution)/shard_map/ppermute | solution.py:272
  106.4 8.9 %collective-permute-done.1.refs_2_ = bf16[4,512,128]{2,1,0:T(8,128)(2,1)S(1)} collective-permute-done((bf16[4,512,128]{2,1,0:T(8,128)(2,1)S(1)}, bf16[4,512,128]{2,1,0:T(8,128)(2,1)S(1)}, u32[]{:S(2)}, u32[]{:S(2)}) %collective-permute-start.1) | collective-permute-done | bytes 524320 | tf_op jit(solution)/shard_map/ppermute | solution.py:272
  116.8 5.5 %collective-permute-done.3.refs_4_ = bf16[4,512,128]{2,1,0:T(8,128)(2,1)S(1)} collective-permute-done((bf16[4,512,128]{2,1,0:T(8,128)(2,1)S(1)}, bf16[4,512,128]{2,1,0:T(8,128)(2,1)S(1)}, u32[]{:S(2)}, u32[]{:S(2)}) %collective-permute-start.3) | collective-permute-done | bytes 524320 | tf_op jit(solution)/shard_map/ppermute | solution.py:272
  123.2 10.0 %expert_near.1 = (bf16[4,512,128]{2,1,0:T(8,128)(2,1)}, bf16[4,512,128]{2,1,0:T(8,128)(2,1)}, bf16[4,512,128]{2,1,0:T(8,128)(2,1)}, bf16[4,512,128]{2,1,0:T(8,128)(2,1)}) custom-call(s32[2]{0:T(128)} %pad_add_fusion.refs_0_, bf16[4,512,128]{2,1,0:T(8,128)(2,1)} %copy-done.2, bf16[4,512,128]{2,1,0:T(8,128)(2,1)} %copy-done.7, bf16[4,512,128]{2,1,0:T(8,128)(2,1)} %copy-done.8, ...), custom_call_target="tpu_custom_call" | custom-call | tf_op jit(solution)/shard_map/expert_near/pallas_call | solution.py:177
  133.2 3.9 %collective-permute-start.9 = (bf16[4,512,128]{2,1,0:T(8,128)(2,1)}, bf16[4,512,128]{2,1,0:T(8,128)(2,1)S(1)}, u32[]{:S(2)}, u32[]{:S(2)}) collective-permute-start(bf16[4,512,128]{2,1,0:T(8,128)(2,1)} %get-tuple-element.23), channel_id=1, source_target_pairs={{0,12},{16,19},{1,13},{17,16},{2,14},{18,17},{3,15},{19,18},{4,0},... | collective-permute-start | bytes 1572872 | tf_op jit(solution)/shard_map/ppermute | solution.py:272
  137.1 3.4 %collective-permute-start.8 = (bf16[4,512,128]{2,1,0:T(8,128)(2,1)}, bf16[4,512,128]{2,1,0:T(8,128)(2,1)S(1)}, u32[]{:S(2)}, u32[]{:S(2)}) collective-permute-start(bf16[4,512,128]{2,1,0:T(8,128)(2,1)} %get-tuple-element.22), channel_id=1, source_target_pairs={{0,8},{16,18},{1,9},{17,19},{2,10},{18,16},{3,11},{19,17},{4,12},{... | collective-permute-start | bytes 1572872 | tf_op jit(solution)/shard_map/ppermute | solution.py:272
  140.5 2.1 collective-permute-start.7
  142.5 2.9 %reduce_sum.46 = bf16[4,512,128]{2,1,0:T(8,128)(2,1)} reduce(bf16[4,4,512,128]{3,2,1,0:T(8,128)(2,1)} %all-to-all-done.3, bf16[]{:T(256)} %constant.22.clone.1), dimensions={0}, to_apply=%region_1.2 | reduce | flops 786432 | bytes 2621442 | tf_op jit(solution)/shard_map/reduce_sum | solution.py:287
  145.4 3.5 %all-to-all-start.4 = ((bf16[4,512,128]{2,1,0:T(8,128)(2,1)}), bf16[4,512,128]{2,1,0:T(8,128)(2,1)S(1)}, u32[]{:S(2)}, u32[]{:S(2)}) async-start(bf16[4,512,128]{2,1,0:T(8,128)(2,1)} %reduce_sum.46), calls=%async_computation.4 | async-start | bytes 1048576 | tf_op jit(solution)/shard_map/all_to_all | solution.py:252
  148.9 2.3 %collective-permute-done.8 = bf16[4,512,128]{2,1,0:T(8,128)(2,1)S(1)} collective-permute-done((bf16[4,512,128]{2,1,0:T(8,128)(2,1)}, bf16[4,512,128]{2,1,0:T(8,128)(2,1)S(1)}, u32[]{:S(2)}, u32[]{:S(2)}) %collective-permute-start.8) | collective-permute-done | bytes 524320 | tf_op jit(solution)/shard_map/ppermute | solution.py:272
  151.2 7.1 %collective-permute-done.7 = bf16[4,512,128]{2,1,0:T(8,128)(2,1)S(1)} collective-permute-done((bf16[4,512,128]{2,1,0:T(8,128)(2,1)}, bf16[4,512,128]{2,1,0:T(8,128)(2,1)S(1)}, u32[]{:S(2)}, u32[]{:S(2)}) %collective-permute-start.7) | collective-permute-done | bytes 524320 | tf_op jit(solution)/shard_map/ppermute | solution.py:272
  159.4 3.5 %all-to-all-start.2 = ((bf16[4,512,128]{2,1,0:T(8,128)(2,1)}), bf16[4,512,128]{2,1,0:T(8,128)(2,1)S(1)}, u32[]{:S(2)}, u32[]{:S(2)}) async-start(bf16[4,512,128]{2,1,0:T(8,128)(2,1)} %add_convert_fusion), calls=%async_computation.2 | async-start | bytes 1048576 | tf_op jit(solution)/shard_map/all_to_all | solution.py:252
  163.0 1.9 collective-permute-start.10
  164.9 6.0 %all-to-all-done.2 = bf16[4,512,128]{2,1,0:T(8,128)(2,1)S(1)} async-done(((bf16[4,512,128]{2,1,0:T(8,128)(2,1)}), bf16[4,512,128]{2,1,0:T(8,128)(2,1)S(1)}, u32[]{:S(2)}, u32[]{:S(2)}) %all-to-all-start.2) | async-done | bytes 524320 | tf_op jit(solution)/shard_map/all_to_all | solution.py:252
  171.0 20.4 %all_to_all.38 = bf16[16,2,32,128]{3,2,1,0:T(8,128)(2,1)S(1)} all-to-all(bf16[16,2,32,128]{3,2,1,0:T(8,128)(2,1)S(1)} %pad_maximum_fusion.2), channel_id=1, replica_groups=mesh['z'=16,'c'=2,'y'=4,'x'=4] {'z'}, dimensions={0} | all-to-all | bytes 524288 | tf_op jit(solution)/shard_map/all_to_all | solution.py:252
  192.2 2.2 %combine.1 = (f32[256,128]{1,0:T(8,128)}, f32[1,256]{1,0:T(1,128)}) custom-call(f32[256,8]{1,0:T(8,128)} %get-tuple-element.16.table, bf16[512,128]{1,0:T(8,128)(2,1)} %bitcast.29, bf16[512,128]{1,0:T(8,128)(2,1)} %bitcast.28), custom_call_target="tpu_custom_call" | custom-call | tf_op jit(solution)/shard_map/combine/pallas_call | solution.py:220
  195.6 6.0 %all-to-all-start.6 = ((f32[16,1,256]{2,1,0:T(1,128)}), f32[16,1,256]{2,1,0:T(1,128)S(1)}, u32[]{:S(2)}, u32[]{:S(2)}) async-start(f32[16,1,256]{2,1,0:T(1,128)} %broadcast_in_dim.8), calls=%async_computation.6 | async-start | bytes 32768 | tf_op jit(solution)/shard_map/all_to_all | solution.py:252
  201.6 7.6 %all-to-all-done.6 = f32[16,1,256]{2,1,0:T(1,128)S(1)} async-done(((f32[16,1,256]{2,1,0:T(1,128)}), f32[16,1,256]{2,1,0:T(1,128)S(1)}, u32[]{:S(2)}, u32[]{:S(2)}) %all-to-all-start.6) | async-done | bytes 16416 | tf_op jit(solution)/shard_map/all_to_all | solution.py:252
  209.3 1.6 multiply_convert_fusion
  (48 shorter events, 12.1 us)
Async XLA Ops:
  0.0 39.9 %copy-start.10 = (bf16[128]{0:T(256)(128)(2,1)S(1)}, bf16[128]{0:T(256)(128)(2,1)}, u32[]{:S(2)}) copy-start(bf16[128]{0:T(256)(128)(2,1)} %param.9) | copy-start | bytes 772
  2.1 3.4 %collective-permute-start = (bf16[512,128]{1,0:T(8,128)(2,1)}, bf16[512,128]{1,0:T(8,128)(2,1)S(1)}, u32[]{:S(2)}, u32[]{:S(2)}) collective-permute-start(bf16[512,128]{1,0:T(8,128)(2,1)} %get-tuple-element.18), channel_id=1, source_target_pairs={{0,16},{16,0},{1,17},{17,1},{2,18},{18,2},{3,19},{19,3},{4,20},{20... | collective-permute-start | bytes 393224 | tf_op jit(solution)/shard_map/ppermute | solution.py:276
  55.2 1.0 copy-start
  56.2 24.3 %copy-start.1 = (bf16[4,528,128]{2,1,0:T(8,128)(2,1)}, bf16[4,528,128]{2,1,0:T(8,128)(2,1)S(1)}, u32[]{:S(2)}) copy-start(bf16[4,528,128]{2,1,0:T(8,128)(2,1)S(1)} %slice.27.refs_1_) | copy-start | bytes 1622020
  56.2 17.6 %collective-permute-start.4 = (bf16[4,528,128]{2,1,0:T(8,128)(2,1)S(1)}, bf16[4,528,128]{2,1,0:T(8,128)(2,1)S(1)}, u32[]{:S(2)}, u32[]{:S(2)}) collective-permute-start(bf16[4,528,128]{2,1,0:T(8,128)(2,1)S(1)} %slice.27.refs_1_), channel_id=1, source_target_pairs={{0,12},{16,19},{1,13},{17,16},{2,14},{18,17},{3,15},{19,18},{4,0},... | collective-permute-start | bytes 1622024 | tf_op jit(solution)/shard_map/ppermute | solution.py:272
  61.2 12.9 %collective-permute-start.5 = (bf16[4,528,128]{2,1,0:T(8,128)(2,1)S(1)}, bf16[4,528,128]{2,1,0:T(8,128)(2,1)S(1)}, u32[]{:S(2)}, u32[]{:S(2)}) collective-permute-start(bf16[4,528,128]{2,1,0:T(8,128)(2,1)S(1)} %slice.27.refs_1_), channel_id=1, source_target_pairs={{0,8},{16,18},{1,9},{17,19},{2,10},{18,16},{3,11},{19,17},{4,12},{... | collective-permute-start | bytes 1622024 | tf_op jit(solution)/shard_map/ppermute | solution.py:272
  63.7 16.0 %collective-permute-start.6 = (bf16[4,528,128]{2,1,0:T(8,128)(2,1)S(1)}, bf16[4,528,128]{2,1,0:T(8,128)(2,1)S(1)}, u32[]{:S(2)}, u32[]{:S(2)}) collective-permute-start(bf16[4,528,128]{2,1,0:T(8,128)(2,1)S(1)} %slice.27.refs_1_), channel_id=1, source_target_pairs={{0,4},{16,17},{1,5},{17,18},{2,6},{18,19},{3,7},{19,16},{4,8},{20,... | collective-permute-start | bytes 1622024 | tf_op jit(solution)/shard_map/ppermute | solution.py:272
  73.8 5.9 %copy-start.3 = (bf16[4,528,128]{2,1,0:T(8,128)(2,1)}, bf16[4,528,128]{2,1,0:T(8,128)(2,1)S(1)}, u32[]{:S(2)}) copy-start(bf16[4,528,128]{2,1,0:T(8,128)(2,1)S(1)} %collective-permute-done.4.refs_2_) | copy-start | bytes 1622020
  74.0 5.7 %copy-start.4 = (bf16[4,528,128]{2,1,0:T(8,128)(2,1)}, bf16[4,528,128]{2,1,0:T(8,128)(2,1)S(1)}, u32[]{:S(2)}) copy-start(bf16[4,528,128]{2,1,0:T(8,128)(2,1)S(1)} %collective-permute-done.5.refs_3_) | copy-start | bytes 1622020
  79.7 0.8 copy-start.5
  90.2 52.4 %all-to-all-start.3 = ((bf16[4,4,512,128]{3,2,1,0:T(8,128)(2,1)}), bf16[4,4,512,128]{3,2,1,0:T(8,128)(2,1)}, u32[]{:S(2)}, u32[]{:S(2)}) async-start(bf16[4,4,512,128]{3,2,1,0:T(8,128)(2,1)} %get-tuple-element.24), calls=%async_computation.3 | async-start | bytes 4194304 | tf_op jit(solution)/shard_map/all_to_all | solution.py:252
  95.7 27.5 %copy-start.2 = (bf16[4,512,128]{2,1,0:T(8,128)(2,1)}, bf16[4,512,128]{2,1,0:T(8,128)(2,1)S(1)}, u32[]{:S(2)}) copy-start(bf16[4,512,128]{2,1,0:T(8,128)(2,1)S(1)} %slice.26.refs_1_) | copy-start | bytes 1572868
  95.7 19.5 %collective-permute-start.1 = (bf16[4,512,128]{2,1,0:T(8,128)(2,1)S(1)}, bf16[4,512,128]{2,1,0:T(8,128)(2,1)S(1)}, u32[]{:S(2)}, u32[]{:S(2)}) collective-permute-start(bf16[4,512,128]{2,1,0:T(8,128)(2,1)S(1)} %slice.26.refs_1_), channel_id=1, source_target_pairs={{0,12},{16,19},{1,13},{17,16},{2,14},{18,17},{3,15},{19,18},{4,0},... | collective-permute-start | bytes 1572872 | tf_op jit(solution)/shard_map/ppermute | solution.py:272
  100.8 16.0 %collective-permute-start.2 = (bf16[4,512,128]{2,1,0:T(8,128)(2,1)S(1)}, bf16[4,512,128]{2,1,0:T(8,128)(2,1)S(1)}, u32[]{:S(2)}, u32[]{:S(2)}) collective-permute-start(bf16[4,512,128]{2,1,0:T(8,128)(2,1)S(1)} %slice.26.refs_1_), channel_id=1, source_target_pairs={{0,8},{16,18},{1,9},{17,19},{2,10},{18,16},{3,11},{19,17},{4,12},{... | collective-permute-start | bytes 1572872 | tf_op jit(solution)/shard_map/ppermute | solution.py:272
  103.6 18.7 %collective-permute-start.3 = (bf16[4,512,128]{2,1,0:T(8,128)(2,1)S(1)}, bf16[4,512,128]{2,1,0:T(8,128)(2,1)S(1)}, u32[]{:S(2)}, u32[]{:S(2)}) collective-permute-start(bf16[4,512,128]{2,1,0:T(8,128)(2,1)S(1)} %slice.26.refs_1_), channel_id=1, source_target_pairs={{0,4},{16,17},{1,5},{17,18},{2,6},{18,19},{3,7},{19,16},{4,8},{20,... | collective-permute-start | bytes 1572872 | tf_op jit(solution)/shard_map/ppermute | solution.py:272
  115.3 7.1 %copy-start.7 = (bf16[4,512,128]{2,1,0:T(8,128)(2,1)}, bf16[4,512,128]{2,1,0:T(8,128)(2,1)S(1)}, u32[]{:S(2)}) copy-start(bf16[4,512,128]{2,1,0:T(8,128)(2,1)S(1)} %collective-permute-done.1.refs_2_) | copy-start | bytes 1572868
  116.8 5.5 %copy-start.8 = (bf16[4,512,128]{2,1,0:T(8,128)(2,1)}, bf16[4,512,128]{2,1,0:T(8,128)(2,1)S(1)}, u32[]{:S(2)}) copy-start(bf16[4,512,128]{2,1,0:T(8,128)(2,1)S(1)} %collective-permute-done.2.refs_3_) | copy-start | bytes 1572868
  122.3 0.9 copy-start.9
  133.2 15.7 %collective-permute-start.9 = (bf16[4,512,128]{2,1,0:T(8,128)(2,1)}, bf16[4,512,128]{2,1,0:T(8,128)(2,1)S(1)}, u32[]{:S(2)}, u32[]{:S(2)}) collective-permute-start(bf16[4,512,128]{2,1,0:T(8,128)(2,1)} %get-tuple-element.23), channel_id=1, source_target_pairs={{0,12},{16,19},{1,13},{17,16},{2,14},{18,17},{3,15},{19,18},{4,0},... | collective-permute-start | bytes 1572872 | tf_op jit(solution)/shard_map/ppermute | solution.py:272
  137.1 14.1 %collective-permute-start.8 = (bf16[4,512,128]{2,1,0:T(8,128)(2,1)}, bf16[4,512,128]{2,1,0:T(8,128)(2,1)S(1)}, u32[]{:S(2)}, u32[]{:S(2)}) collective-permute-start(bf16[4,512,128]{2,1,0:T(8,128)(2,1)} %get-tuple-element.22), channel_id=1, source_target_pairs={{0,8},{16,18},{1,9},{17,19},{2,10},{18,16},{3,11},{19,17},{4,12},{... | collective-permute-start | bytes 1572872 | tf_op jit(solution)/shard_map/ppermute | solution.py:272
  140.5 17.8 %copy-start.6 = (bf16[4,512,128]{2,1,0:T(8,128)(2,1)S(1)}, bf16[4,512,128]{2,1,0:T(8,128)(2,1)}, u32[]{:S(2)}) copy-start(bf16[4,512,128]{2,1,0:T(8,128)(2,1)} %get-tuple-element.20) | copy-start | bytes 1572868
  140.5 17.8 %collective-permute-start.7 = (bf16[4,512,128]{2,1,0:T(8,128)(2,1)}, bf16[4,512,128]{2,1,0:T(8,128)(2,1)S(1)}, u32[]{:S(2)}, u32[]{:S(2)}) collective-permute-start(bf16[4,512,128]{2,1,0:T(8,128)(2,1)} %get-tuple-element.21), channel_id=1, source_target_pairs={{0,4},{16,17},{1,5},{17,18},{2,6},{18,19},{3,7},{19,16},{4,8},{20,... | collective-permute-start | bytes 1572872 | tf_op jit(solution)/shard_map/ppermute | solution.py:272
  145.4 14.0 %all-to-all-start.4 = ((bf16[4,512,128]{2,1,0:T(8,128)(2,1)}), bf16[4,512,128]{2,1,0:T(8,128)(2,1)S(1)}, u32[]{:S(2)}, u32[]{:S(2)}) async-start(bf16[4,512,128]{2,1,0:T(8,128)(2,1)} %reduce_sum.46), calls=%async_computation.4 | async-start | bytes 1048576 | tf_op jit(solution)/shard_map/all_to_all | solution.py:252
  159.4 11.5 %all-to-all-start.2 = ((bf16[4,512,128]{2,1,0:T(8,128)(2,1)}), bf16[4,512,128]{2,1,0:T(8,128)(2,1)S(1)}, u32[]{:S(2)}, u32[]{:S(2)}) async-start(bf16[4,512,128]{2,1,0:T(8,128)(2,1)} %add_convert_fusion), calls=%async_computation.2 | async-start | bytes 1048576 | tf_op jit(solution)/shard_map/all_to_all | solution.py:252
  162.9 38.8 %copy-start.11 = (bf16[128]{0:T(256)(128)(2,1)S(1)}, bf16[128]{0:T(256)(128)(2,1)}, u32[]{:S(2)}) copy-start(bf16[128]{0:T(256)(128)(2,1)} %param.15) | copy-start | bytes 772
  163.0 8.0 %collective-permute-start.10 = (bf16[512,128]{1,0:T(8,128)(2,1)S(1)}, bf16[512,128]{1,0:T(8,128)(2,1)S(1)}, u32[]{:S(2)}, u32[]{:S(2)}) collective-permute-start(bf16[512,128]{1,0:T(8,128)(2,1)S(1)} %reduce_sum.47), channel_id=1, source_target_pairs={{0,16},{16,0},{1,17},{17,1},{2,18},{18,2},{3,19},{19,3},{4,20},{20... | collective-permute-start | bytes 393224 | tf_op jit(solution)/shard_map/ppermute | solution.py:276
  195.6 13.6 %all-to-all-start.6 = ((f32[16,1,256]{2,1,0:T(1,128)}), f32[16,1,256]{2,1,0:T(1,128)S(1)}, u32[]{:S(2)}, u32[]{:S(2)}) async-start(f32[16,1,256]{2,1,0:T(1,128)} %broadcast_in_dim.8), calls=%async_computation.6 | async-start | bytes 32768 | tf_op jit(solution)/shard_map/all_to_all | solution.py:252

commit v2 on v1

v2 whole, which is shorter than its diff:
```python
import functools

import jax
import jax.numpy as jnp
from jax import lax
from jax.experimental import pallas as pl
from jax.experimental.pallas import tpu as pltpu
from jax.sharding import Mesh, PartitionSpec as P


EPS = 1e-06
F32 = jnp.float32
BF16 = jnp.bfloat16
GAIN_ROWS = 16


def pack_kernel(pos, routes, weights, tokens, near, far, table):
    tok = tokens.shape[0]
    half = near.shape[0]
    experts = 2 * lax.axis_size("z")
    cap = half // (experts // 2)
    e0 = routes[0:1, :]
    e1 = routes[1:2, :]
    lanes = lax.broadcasted_iota(jnp.int32, (experts, tok), 0)
    hot0 = lanes == e0
    hot1 = lanes == e1
    hot = (hot0 | hot1).astype(F32).astype(BF16)
    row = lax.broadcasted_iota(jnp.int32, (tok, tok), 0)
    col = lax.broadcasted_iota(jnp.int32, (tok, tok), 1)
    earlier = (row < col).astype(F32).astype(BF16)
    before = jnp.dot(hot, earlier, preferred_element_type=F32)

    def place(e, mine):
        slot = jnp.sum(jnp.where(mine, before, 0.0), axis=0, keepdims=True)
        other = jnp.bitwise_xor(jnp.bitwise_and(e, 1), pos[0])
        return other * half + (e >> 1) * cap + slot.astype(jnp.int32)

    t0 = place(e0, hot0)
    t1 = place(e1, hot1)
    for at, out in ((0, near), (half, far)):
        rows = lax.broadcasted_iota(jnp.int32, (half, tok), 0) + at
        put = ((rows == t0) | (rows == t1)).astype(F32).astype(BF16)
        out[...] = jnp.dot(put, tokens[...], preferred_element_type=F32).astype(BF16)

    def packed(t):
        other = (t >= half).astype(jnp.int32)
        inside = t - other * half
        at_z = inside // cap
        return (at_z * 2 + other) * cap + (inside - at_z * cap)

    t0 = packed(t0)
    t1 = packed(t1)
    stack = jnp.concatenate(
        [t0.astype(F32), t1.astype(F32), weights[...], jnp.zeros((4, tok), F32)], axis=0
    )
    table[...] = stack.T


def pack(c, routes, weights, tokens):
    tok, share = tokens.shape
    half = lax.axis_size("z") * 32
    vmem = pl.BlockSpec(memory_space=pltpu.VMEM)
    return pl.pallas_call(
        pack_kernel,
        out_shape=(
            jax.ShapeDtypeStruct((half, share), BF16),
            jax.ShapeDtypeStruct((half, share), BF16),
            jax.ShapeDtypeStruct((tok, 8), F32),
        ),
        in_specs=[pl.BlockSpec(memory_space=pltpu.SMEM), vmem, vmem, vmem],
        out_specs=(vmem, vmem, vmem),
        name="pack",
    )(c, routes, weights, tokens)


def expert_kernel(first, rows, core_ref, y_ref, x_ref, xs, *refs):
    if first:
        wg, wu, wd, out, gain_out = refs[:5]
        refs = refs[5:]
        outs = [out.at[o] for o in range(4)]
    else:
        more = refs[0:3]
        wg, wu, wd, gain_in = refs[3:7]
        outs = refs[7:11]
        refs = refs[11:]
    raw, gain_s, xn, gu_s, d_s, stage, sems, osems = refs
    core = core_ref[0]
    at_outer = jnp.where(core == 0, y_ref[0], x_ref[0])

    def block(o, inner):
        outer = o if first else jnp.bitwise_and(at_outer + o, 3)
        return jnp.where(core == 0, outer * 4 + inner, inner * 4 + outer)

    def source(o):
        if first:
            return xs.at[o]
        return xs if o == 0 else more[o - 1]

    count = [0]

    def fetch(src, dst):
        cp = pltpu.make_async_copy(src, dst, sems.at[count[0]])
        count[0] += 1
        cp.start()
        return cp

    half = rows // 2
    width = xn.shape[1]
    units = gu_s.shape[1] // 2

    def fetch_rows(at):
        return [
            fetch(source(o).at[i, pl.ds(at, half), :], raw.at[block(o, i), pl.ds(at, half), :])
            for o in range(4)
            for i in range(4)
        ]

    x_cp = [fetch_rows(0)]
    if first:
        gain_cp = [
            fetch(source(o).at[i, pl.ds(rows, GAIN_ROWS), :], gain_s.at[block(o, i)])
            for o in range(4)
            for i in range(4)
        ]
    else:
        gain_cp = [fetch(gain_in, gain_s)]
    w_cp = [fetch(wg, gu_s.at[:, pl.ds(0, units)]), fetch(wu, gu_s.at[:, pl.ds(units, units)])]
    x_cp.append(fetch_rows(half))
    d_cp = [
        fetch(
            wd.at[:, pl.ds(pl.multiple_of(block(o, i) * 128, 128), 128)],
            d_s.at[:, pl.ds((o * 4 + i) * 128, 128)],
        )
        for o in range(4)
        for i in range(4)
    ]
    for cp in gain_cp:
        cp.wait()
    copies = []

    def store(n, src, dst):
        cp = pltpu.make_async_copy(src, dst, osems.at[n])
        cp.start()
        copies.append(cp)

    if first:
        store(4, gain_s, gain_out)
    step = 32

    def norm(i, _):
        at = pl.multiple_of(i * step, step)
        acc = jnp.zeros((step, 128), F32)
        vals = []
        for j in range(16):
            v = raw[j, pl.ds(at, step), :].astype(F32)
            vals.append(v)
            acc = acc + v * v
        scale = lax.rsqrt(jnp.sum(acc, axis=1, keepdims=True) * (1.0 / width) + EPS)
        for j in range(16):
            gain = gain_s[j, 0:1, :].astype(F32)
            xn[pl.ds(at, step), j * 128 : (j + 1) * 128] = (vals[j] * scale * gain).astype(BF16)
        return 0

    steps = half // step
    for h in range(2):
        for cp in x_cp[h]:
            cp.wait()
        lax.fori_loop(h * steps, (h + 1) * steps, norm, 0)
    for cp in w_cp:
        cp.wait()
    both = jnp.dot(xn[...], gu_s[...], preferred_element_type=F32)
    gate = both[:, :units]
    hidden = (gate * both[:, units:] / (1.0 + jnp.exp(-gate))).astype(BF16)
    for cp in d_cp:
        cp.wait()
    for o in range(4):
        res = jnp.dot(
            hidden, d_s[:, o * 512 : (o + 1) * 512], preferred_element_type=F32
        ).astype(BF16)
        for i in range(4):
            stage[o, i] = res[:, i * 128 : (i + 1) * 128]
        store(o, stage.at[o], outs[o])
    for cp in copies:
        cp.wait()


def expert(first, place, xs, weights, gain):
    rows = 512
    width, units = weights[0].shape
    hbm = pl.BlockSpec(memory_space=pltpu.HBM)
    if first:
        args = (*place, xs, *weights)
        outs = (
            jax.ShapeDtypeStruct((4, 4, rows, 128), BF16),
            jax.ShapeDtypeStruct((16, GAIN_ROWS, 128), BF16),
        )
    else:
        args = (*place, *xs, *weights, gain)
        outs = tuple([jax.ShapeDtypeStruct((4, rows, 128), BF16)] * 4)
    return pl.pallas_call(
        functools.partial(expert_kernel, first, rows),
        out_shape=outs,
        in_specs=[pl.BlockSpec(memory_space=pltpu.SMEM)] * 3 + [hbm] * (len(args) - 3),
        out_specs=tuple([hbm] * len(outs)),
        scratch_shapes=[
            pltpu.VMEM((16, rows, 128), BF16),
            pltpu.VMEM((16, GAIN_ROWS, 128), BF16),
            pltpu.VMEM((rows, width), BF16),
            pltpu.VMEM((width, 2 * units), BF16),
            pltpu.VMEM((units, width), BF16),
            pltpu.VMEM((4, 4, rows, 128), BF16),
            pltpu.SemaphoreType.DMA((66,)),
            pltpu.SemaphoreType.DMA((5,)),
        ],
        compiler_params=pltpu.CompilerParams(vmem_limit_bytes=63 * 1024 * 1024),
        name="expert_far" if first else "expert_near",
    )(*args)


def combine_kernel(table, rows, combined, squares):
    tok = table.shape[0]
    count = rows.shape[0]
    cols = lax.broadcasted_iota(jnp.int32, (tok, count), 1)
    total = None
    for k in range(2):
        target = table[:, k : k + 1].astype(jnp.int32)
        pick = (cols == target).astype(F32).astype(BF16)
        got = jnp.dot(pick, rows[...], preferred_element_type=F32)
        term = got * table[:, 2 + k : 3 + k]
        total = term if total is None else total + term
    combined[...] = total
    mine = jnp.sum((total * total).T, axis=0, keepdims=True)
    for i in range(squares.shape[0]):
        squares[i] = mine


def combine(table, rows):
    tok = table.shape[0]
    share = rows.shape[1]
    vmem = pl.BlockSpec(memory_space=pltpu.VMEM)
    return pl.pallas_call(
        combine_kernel,
        out_shape=(
            jax.ShapeDtypeStruct((tok, share), F32),
            jax.ShapeDtypeStruct((16, 1, tok), F32),
        ),
        in_specs=[vmem] * 2,
        out_specs=(vmem, vmem),
        name="combine",
    )(table, rows)


ALL = ("z", "c", "y", "x")


def flat(z, c, y, x):
    return ((z * 2 + c) * 4 + y) * 4 + x


def lines(along_x_for):
    groups = []
    for z in range(16):
        for c in range(2):
            for i in range(4):
                if c == along_x_for:
                    groups.append([flat(z, c, i, x) for x in range(4)])
                else:
                    groups.append([flat(z, c, y, i) for y in range(4)])
    return groups


def exchange(v, axis, groups=None):
    return lax.all_to_all(
        v, axis, split_axis=0, concat_axis=0, tiled=True, axis_index_groups=groups
    )


def inner_exchange(v):
    return exchange(v, ALL, lines(0))


def outer_exchange(v):
    return exchange(v, ALL, lines(1))


def outer_shift(v, step):
    pairs = []
    for z in range(16):
        for y in range(4):
            for x in range(4):
                pairs.append((flat(z, 0, y, x), flat(z, 0, (y + step) % 4, x)))
                pairs.append((flat(z, 1, y, x), flat(z, 1, y, (x + step) % 4)))
    return lax.ppermute(v, ALL, pairs)


def swap(v):
    return lax.ppermute(v, "c", [(0, 1), (1, 0)])


def total_of(parts):
    total = parts[0].astype(F32)
    for p in parts[1:]:
        total = total + p.astype(F32)
    return total.astype(BF16)


def summed(v):
    return v.astype(F32).sum(axis=0).astype(BF16)


def over_z(near, far):
    share = near.shape[1]
    both = jnp.stack([near.reshape(16, -1, share), far.reshape(16, -1, share)], axis=1)
    return exchange(both, "z")


def local(tokens, norm_gain, w_gate, w_up, w_down, routes, route_weights, final_gain):
    _, share = tokens.shape
    width = share * 16
    place = tuple(lax.axis_index(a).astype(jnp.int32).reshape(1) for a in ("c", "y", "x"))
    near, far, table = pack(place[0], routes.T, route_weights.T, tokens)
    weights = (w_gate[0], w_up[0], w_down[0])
    both = over_z(near, swap(far))
    near, far = (both[:, i].reshape(-1, share) for i in range(2))
    gain_rows = jnp.broadcast_to(norm_gain[None, :], (GAIN_ROWS, share))
    rows = jnp.concatenate([far, gain_rows, near], axis=0)
    rows = inner_exchange(jnp.broadcast_to(rows[None], (4, *rows.shape)))
    first = far.shape[0] + GAIN_ROWS
    far = rows[:, :first]
    far = outer_exchange(jnp.broadcast_to(far[None], (4, *far.shape)))
    near = rows[:, first:]
    near = [near] + [outer_shift(near, -s) for s in (1, 2, 3)]
    far, gain = expert(True, place, far, weights, None)
    far = summed(outer_exchange(far))
    near = expert(False, place, near, weights, gain)
    near = total_of([near[0]] + [outer_shift(near[s], s) for s in (1, 2, 3)])
    far = swap(summed(inner_exchange(far)))
    near = summed(inner_exchange(near))
    both = over_z(near, far)
    combined, squares = combine(table, both.reshape(-1, share))
    total = exchange(squares, ("y", "x")).sum(axis=(0, 1))
    scale = lax.rsqrt(total / width + EPS)
    return (combined * scale[:, None] * final_gain.astype(F32)[None, :]).astype(BF16)


def solution(mesh):
    fine = Mesh(mesh.devices.reshape(16, 2, 4, 4), ("z", "c", "y", "x"))
    ep = ("z", "c")
    tp = ("y", "x")
    in_specs = (
        P(ep, tp),
        P(tp),
        P(ep, None, tp),
        P(ep, None, tp),
        P(ep, tp, None),
        P(ep, None),
        P(ep, None),
        P(tp),
    )
    return jax.shard_map(
        local, mesh=fine, in_specs=in_specs, out_specs=P(ep, tp), check_vma=False
    )
```

time: 212 us -> 208 us (0.981)
  starting transfers between devices: 51.5 us -> 45.6 us
  waiting for transfers between devices: 53 us -> 57.4 us
    all_to_all x4 -> x5, waiting for transfers between devices: 13.6 us -> 30.5 us  [exchange(): lax.all_to_all(v, axis, split_axis=0, concat_axis=0, tiled=True, axis_ind...]
    ppermute x9 -> x6, waiting for transfers between devices: 37.9 us -> 25.4 us  [outer_shift(): return lax.ppermute(v, ALL, pairs)]
    ppermute x9 -> x6, starting transfers between devices: 30.3 us -> 20 us  [outer_shift(): return lax.ppermute(v, ALL, pairs)]
    all_to_all x4 -> x5, starting transfers between devices: 17.4 us -> 21.8 us  [exchange(): lax.all_to_all(v, axis, split_axis=0, concat_axis=0, tiled=True, axis_ind...]
  transfers between devices with their start and end apart: 15 -> 13, of which waited for: 11 -> 9; matrix products, arithmetic and copies ran while one was open for 3% -> 3% of each run, Pallas kernels for 5% -> 4%
where the time goes in v2:
time: 208 us; the launch traced here: 207 us
  blocking collectives  69 us (33%)
  waiting for transfers between devices  57.4 us (28%)
  starting transfers between devices  45.6 us (22%)
  Pallas kernels  22.7 us (11%)
  other arithmetic  6.78 us (3%)
  local copies, waits for them, and re-layouts  4.84 us (2%)
    all_to_all x3, blocking collectives, exchange(): lax.all_to_all(v, axis, split_axis=0, concat_axis=0, tiled=True, axis_ind...  69 us
    all_to_all x5, waiting for transfers between devices, exchange(): lax.all_to_all(v, axis, split_axis=0, concat_axis=0, tiled=True, axis_ind...  30.5 us
    ppermute x6, waiting for transfers between devices, outer_shift(): return lax.ppermute(v, ALL, pairs)  25.4 us
    all_to_all x5, starting transfers between devices, exchange(): lax.all_to_all(v, axis, split_axis=0, concat_axis=0, tiled=True, axis_ind...  21.8 us
    ppermute x6, starting transfers between devices, outer_shift(): return lax.ppermute(v, ALL, pairs)  20 us
    pallas_call x2, Pallas kernels, expert(): pl.pallas_call(functools.partial(expert_kernel, first, rows), out_shape=o...  18.4 us
  transfers between devices with their start and end apart: 13, of which 9 were waited for; matrix products, arithmetic and copies ran while one was open for 3% of the time, Pallas kernels for 4%

profile of v2, /device:TPU:32, one launch (start us, length us, event | category | flops | bytes accessed | tf_op | source)
XLA Modules:
  0.0 206.6 jit_solution(14906248953447406084)
XLA Ops:
  0.0 2.1 %pack.1 = (bf16[512,128]{1,0:T(8,128)(2,1)}, bf16[512,128]{1,0:T(8,128)(2,1)}, f32[256,8]{1,0:T(8,128)}) custom-call(s32[1]{0:T(128)} %bitcast.pos.core_ref, s32[2,256]{1,0:T(2,128)} %bitcast.34, f32[2,256]{1,0:T(2,128)} %bitcast.35, bf16[256,128]{1,0:T(8,128)(2,1)} %tokens.1), custom_call_target="tpu_custom_call" | custom-call | tf_op jit(solution)/shard_map/pack/pallas_call | solution.py:63
  2.1 1.9 collective-permute-start
  4.0 1.5 collective-permute-done
  6.5 33.4 %all_to_all.40 = bf16[16,2,32,128]{3,2,1,0:T(8,128)(2,1)S(1)} all-to-all(bf16[16,2,32,128]{3,2,1,0:T(8,128)(2,1)S(1)} %pad_maximum_fusion.1), channel_id=1, replica_groups=mesh['z'=16,'c'=2,'y'=4,'x'=4] {'z'}, dimensions={0} | all-to-all | bytes 524288 | tf_op jit(solution)/shard_map/all_to_all | solution.py:273
  40.1 15.1 %all_to_all.41 = bf16[4,1040,128]{2,1,0:T(8,128)(2,1)S(1)} all-to-all(bf16[4,1040,128]{2,1,0:T(8,128)(2,1)S(1)} %broadcast_in_dim.7), channel_id=1, replica_groups={{0,1,2,3},{4,5,6,7},{8,9,10,11},{12,13,14,15},{16,20,24,28},{17,21,25,2..., dimensions={0} | all-to-all | bytes 2129920 | tf_op jit(solution)/shard_map/all_to_all | solution.py:273
  56.2 1.7 broadcast_in_dim.8
  57.9 4.5 %all-to-all-start.2 = ((bf16[4,4,528,128]{3,2,1,0:T(8,128)(2,1)}), bf16[4,4,528,128]{3,2,1,0:T(8,128)(2,1)}, u32[]{:S(2)}, u32[]{:S(2)}) async-start(bf16[4,4,528,128]{3,2,1,0:T(8,128)(2,1)} %broadcast_in_dim.8), calls=%async_computation.2 | async-start | bytes 4325376 | tf_op jit(solution)/shard_map/all_to_all | solution.py:273
  62.4 16.9 %all-to-all-done.2.xs = bf16[4,4,528,128]{3,2,1,0:T(8,128)(2,1)} async-done(((bf16[4,4,528,128]{3,2,1,0:T(8,128)(2,1)}), bf16[4,4,528,128]{3,2,1,0:T(8,128)(2,1)}, u32[]{:S(2)}, u32[]{:S(2)}) %all-to-all-start.2) | async-done | bytes 2162720 | tf_op jit(solution)/shard_map/all_to_all | solution.py:273
  79.3 9.2 %expert_far.1 = (bf16[4,4,512,128]{3,2,1,0:T(8,128)(2,1)}, bf16[16,16,128]{2,1,0:T(8,128)(2,1)}) custom-call(s32[1]{0:T(128)} %bitcast.pos.core_ref, s32[1]{0:T(128)} %bitcast.3.y_ref, s32[1]{0:T(128)} %bitcast.4.x_ref, bf16[4,4,528,128]{3,2,1,0:T(8,128)(2,1)} %all-to-all-done.2.xs, bf16[2048,384]{1,0:T(8,128)(2,1)} %bitcast.21, bf16[2048,384]{1,0:T(8,128)(2,1)} %bitcast.23, ...), custom_call_target="tpu_custom_call" | custom-call | tf_op jit(solution)/shard_map/expert_far/pallas_call | solution.py:200
  88.5 4.5 %all-to-all-start.4 = ((bf16[4,4,512,128]{3,2,1,0:T(8,128)(2,1)}), bf16[4,4,512,128]{3,2,1,0:T(8,128)(2,1)}, u32[]{:S(2)}, u32[]{:S(2)}) async-start(bf16[4,4,512,128]{3,2,1,0:T(8,128)(2,1)} %get-tuple-element.24), calls=%async_computation.4 | async-start | bytes 4194304 | tf_op jit(solution)/shard_map/all_to_all | solution.py:273
  94.1 5.1 %collective-permute-start.1 = (bf16[4,512,128]{2,1,0:T(8,128)(2,1)S(1)}, bf16[4,512,128]{2,1,0:T(8,128)(2,1)S(1)}, u32[]{:S(2)}, u32[]{:S(2)}) collective-permute-start(bf16[4,512,128]{2,1,0:T(8,128)(2,1)S(1)} %slice.18.xs), channel_id=1, source_target_pairs={{0,12},{16,19},{1,13},{17,16},{2,14},{18,17},{3,15},{19,18},{4,0},... | collective-permute-start | bytes 1572872 | tf_op jit(solution)/shard_map/ppermute | solution.py:293
  99.2 2.8 %collective-permute-start.2 = (bf16[4,512,128]{2,1,0:T(8,128)(2,1)S(1)}, bf16[4,512,128]{2,1,0:T(8,128)(2,1)S(1)}, u32[]{:S(2)}, u32[]{:S(2)}) collective-permute-start(bf16[4,512,128]{2,1,0:T(8,128)(2,1)S(1)} %slice.18.xs), channel_id=1, source_target_pairs={{0,8},{16,18},{1,9},{17,19},{2,10},{18,16},{3,11},{19,17},{4,12},{... | collective-permute-start | bytes 1572872 | tf_op jit(solution)/shard_map/ppermute | solution.py:293
  102.0 2.8 %collective-permute-start.3 = (bf16[4,512,128]{2,1,0:T(8,128)(2,1)S(1)}, bf16[4,512,128]{2,1,0:T(8,128)(2,1)S(1)}, u32[]{:S(2)}, u32[]{:S(2)}) collective-permute-start(bf16[4,512,128]{2,1,0:T(8,128)(2,1)S(1)} %slice.18.xs), channel_id=1, source_target_pairs={{0,4},{16,17},{1,5},{17,18},{2,6},{18,19},{3,7},{19,16},{4,8},{20,... | collective-permute-start | bytes 1572872 | tf_op jit(solution)/shard_map/ppermute | solution.py:293
  104.8 8.9 %collective-permute-done.1.refs_0_ = bf16[4,512,128]{2,1,0:T(8,128)(2,1)S(1)} collective-permute-done((bf16[4,512,128]{2,1,0:T(8,128)(2,1)S(1)}, bf16[4,512,128]{2,1,0:T(8,128)(2,1)S(1)}, u32[]{:S(2)}, u32[]{:S(2)}) %collective-permute-start.1) | collective-permute-done | bytes 524320 | tf_op jit(solution)/shard_map/ppermute | solution.py:293
  113.7 1.6 collective-permute-done.2.refs_1_
  115.2 5.5 %collective-permute-done.3.refs_2_ = bf16[4,512,128]{2,1,0:T(8,128)(2,1)S(1)} collective-permute-done((bf16[4,512,128]{2,1,0:T(8,128)(2,1)S(1)}, bf16[4,512,128]{2,1,0:T(8,128)(2,1)S(1)}, u32[]{:S(2)}, u32[]{:S(2)}) %collective-permute-start.3) | collective-permute-done | bytes 524320 | tf_op jit(solution)/shard_map/ppermute | solution.py:293
  121.6 9.2 %expert_near.1 = (bf16[4,512,128]{2,1,0:T(8,128)(2,1)}, bf16[4,512,128]{2,1,0:T(8,128)(2,1)}, bf16[4,512,128]{2,1,0:T(8,128)(2,1)}, bf16[4,512,128]{2,1,0:T(8,128)(2,1)}) custom-call(s32[1]{0:T(128)} %bitcast.pos.core_ref, s32[1]{0:T(128)} %bitcast.3.y_ref, s32[1]{0:T(128)} %bitcast.4.x_ref, bf16[4,512,128]{2,1,0:T(8,128)(2,1)} %copy-done.1, ...), custom_call_target="tpu_custom_call" | custom-call | tf_op jit(solution)/shard_map/expert_near/pallas_call | solution.py:200
  130.8 3.9 %collective-permute-start.6 = (bf16[4,512,128]{2,1,0:T(8,128)(2,1)}, bf16[4,512,128]{2,1,0:T(8,128)(2,1)S(1)}, u32[]{:S(2)}, u32[]{:S(2)}) collective-permute-start(bf16[4,512,128]{2,1,0:T(8,128)(2,1)} %get-tuple-element.23), channel_id=1, source_target_pairs={{0,12},{16,19},{1,13},{17,16},{2,14},{18,17},{3,15},{19,18},{4,0},... | collective-permute-start | bytes 1572872 | tf_op jit(solution)/shard_map/ppermute | solution.py:293
  134.7 3.4 %collective-permute-start.5 = (bf16[4,512,128]{2,1,0:T(8,128)(2,1)}, bf16[4,512,128]{2,1,0:T(8,128)(2,1)S(1)}, u32[]{:S(2)}, u32[]{:S(2)}) collective-permute-start(bf16[4,512,128]{2,1,0:T(8,128)(2,1)} %get-tuple-element.22), channel_id=1, source_target_pairs={{0,8},{16,18},{1,9},{17,19},{2,10},{18,16},{3,11},{19,17},{4,12},{... | collective-permute-start | bytes 1572872 | tf_op jit(solution)/shard_map/ppermute | solution.py:293
  138.1 2.1 collective-permute-start.4
  140.2 2.9 %reduce_sum.46 = bf16[4,512,128]{2,1,0:T(8,128)(2,1)} reduce(bf16[4,4,512,128]{3,2,1,0:T(8,128)(2,1)} %all-to-all-done.4, bf16[]{:T(256)} %constant.20.clone.1), dimensions={0}, to_apply=%region_1.0 | reduce | flops 786432 | bytes 2621442 | tf_op jit(solution)/shard_map/reduce_sum | solution.py:308
  143.0 3.5 %all-to-all-start.5 = ((bf16[4,512,128]{2,1,0:T(8,128)(2,1)}), bf16[4,512,128]{2,1,0:T(8,128)(2,1)S(1)}, u32[]{:S(2)}, u32[]{:S(2)}) async-start(bf16[4,512,128]{2,1,0:T(8,128)(2,1)} %reduce_sum.46), calls=%async_computation.5 | async-start | bytes 1048576 | tf_op jit(solution)/shard_map/all_to_all | solution.py:273
  146.5 2.1 collective-permute-done.5
  148.6 7.3 %collective-permute-done.4 = bf16[4,512,128]{2,1,0:T(8,128)(2,1)S(1)} collective-permute-done((bf16[4,512,128]{2,1,0:T(8,128)(2,1)}, bf16[4,512,128]{2,1,0:T(8,128)(2,1)S(1)}, u32[]{:S(2)}, u32[]{:S(2)}) %collective-permute-start.4) | collective-permute-done | bytes 524320 | tf_op jit(solution)/shard_map/ppermute | solution.py:293
  157.0 3.5 %all-to-all-start.3 = ((bf16[4,512,128]{2,1,0:T(8,128)(2,1)}), bf16[4,512,128]{2,1,0:T(8,128)(2,1)S(1)}, u32[]{:S(2)}, u32[]{:S(2)}) async-start(bf16[4,512,128]{2,1,0:T(8,128)(2,1)} %add_convert_fusion), calls=%async_computation.3 | async-start | bytes 1048576 | tf_op jit(solution)/shard_map/all_to_all | solution.py:273
  160.6 1.9 collective-permute-start.7
  162.5 6.0 %all-to-all-done.3 = bf16[4,512,128]{2,1,0:T(8,128)(2,1)S(1)} async-done(((bf16[4,512,128]{2,1,0:T(8,128)(2,1)}), bf16[4,512,128]{2,1,0:T(8,128)(2,1)S(1)}, u32[]{:S(2)}, u32[]{:S(2)}) %all-to-all-start.3) | async-done | bytes 524320 | tf_op jit(solution)/shard_map/all_to_all | solution.py:273
  168.7 20.5 %all_to_all.42 = bf16[16,2,32,128]{3,2,1,0:T(8,128)(2,1)} all-to-all(bf16[16,2,32,128]{3,2,1,0:T(8,128)(2,1)S(1)} %pad_maximum_fusion.2), channel_id=1, replica_groups=mesh['z'=16,'c'=2,'y'=4,'x'=4] {'z'}, dimensions={0} | all-to-all | bytes 524288 | tf_op jit(solution)/shard_map/all_to_all | solution.py:273
  189.2 2.2 %combine.1 = (f32[256,128]{1,0:T(8,128)}, f32[16,1,256]{2,1,0:T(1,128)}) custom-call(f32[256,8]{1,0:T(8,128)} %get-tuple-element.16.table, bf16[1024,128]{1,0:T(8,128)(2,1)} %bitcast.27), custom_call_target="tpu_custom_call" | custom-call | tf_op jit(solution)/shard_map/combine/pallas_call | solution.py:241
  191.4 6.0 %all-to-all-start.7 = ((f32[16,1,256]{2,1,0:T(1,128)}), f32[16,1,256]{2,1,0:T(1,128)S(1)}, u32[]{:S(2)}, u32[]{:S(2)}) async-start(f32[16,1,256]{2,1,0:T(1,128)} %get-tuple-element.26), calls=%async_computation.7 | async-start | bytes 32768 | tf_op jit(solution)/shard_map/all_to_all | solution.py:273
  197.4 7.6 %all-to-all-done.7 = f32[16,1,256]{2,1,0:T(1,128)S(1)} async-done(((f32[16,1,256]{2,1,0:T(1,128)}), f32[16,1,256]{2,1,0:T(1,128)S(1)}, u32[]{:S(2)}, u32[]{:S(2)}) %all-to-all-start.7) | async-done | bytes 16416 | tf_op jit(solution)/shard_map/all_to_all | solution.py:273
  205.0 1.6 multiply_convert_fusion
  (34 shorter events, 5.5 us)
Async XLA Ops:
  0.0 39.9 %copy-start.6 = (bf16[128]{0:T(256)(128)(2,1)S(1)}, bf16[128]{0:T(256)(128)(2,1)}, u32[]{:S(2)}) copy-start(bf16[128]{0:T(256)(128)(2,1)} %param.9) | copy-start | bytes 772
  2.1 3.4 %collective-permute-start = (bf16[512,128]{1,0:T(8,128)(2,1)}, bf16[512,128]{1,0:T(8,128)(2,1)S(1)}, u32[]{:S(2)}, u32[]{:S(2)}) collective-permute-start(bf16[512,128]{1,0:T(8,128)(2,1)} %get-tuple-element.18), channel_id=1, source_target_pairs={{0,16},{16,0},{1,17},{17,1},{2,18},{18,2},{3,19},{19,3},{4,20},{20... | collective-permute-start | bytes 393224 | tf_op jit(solution)/shard_map/ppermute | solution.py:297
  55.2 1.0 copy-start
  57.9 21.4 %all-to-all-start.2 = ((bf16[4,4,528,128]{3,2,1,0:T(8,128)(2,1)}), bf16[4,4,528,128]{3,2,1,0:T(8,128)(2,1)}, u32[]{:S(2)}, u32[]{:S(2)}) async-start(bf16[4,4,528,128]{3,2,1,0:T(8,128)(2,1)} %broadcast_in_dim.8), calls=%async_computation.2 | async-start | bytes 4325376 | tf_op jit(solution)/shard_map/all_to_all | solution.py:273
  88.5 51.6 %all-to-all-start.4 = ((bf16[4,4,512,128]{3,2,1,0:T(8,128)(2,1)}), bf16[4,4,512,128]{3,2,1,0:T(8,128)(2,1)}, u32[]{:S(2)}, u32[]{:S(2)}) async-start(bf16[4,4,512,128]{3,2,1,0:T(8,128)(2,1)} %get-tuple-element.24), calls=%async_computation.4 | async-start | bytes 4194304 | tf_op jit(solution)/shard_map/all_to_all | solution.py:273
  94.1 27.5 %copy-start.1 = (bf16[4,512,128]{2,1,0:T(8,128)(2,1)}, bf16[4,512,128]{2,1,0:T(8,128)(2,1)S(1)}, u32[]{:S(2)}) copy-start(bf16[4,512,128]{2,1,0:T(8,128)(2,1)S(1)} %slice.18.xs) | copy-start | bytes 1572868
  94.1 19.5 %collective-permute-start.1 = (bf16[4,512,128]{2,1,0:T(8,128)(2,1)S(1)}, bf16[4,512,128]{2,1,0:T(8,128)(2,1)S(1)}, u32[]{:S(2)}, u32[]{:S(2)}) collective-permute-start(bf16[4,512,128]{2,1,0:T(8,128)(2,1)S(1)} %slice.18.xs), channel_id=1, source_target_pairs={{0,12},{16,19},{1,13},{17,16},{2,14},{18,17},{3,15},{19,18},{4,0},... | collective-permute-start | bytes 1572872 | tf_op jit(solution)/shard_map/ppermute | solution.py:293
  99.2 16.0 %collective-permute-start.2 = (bf16[4,512,128]{2,1,0:T(8,128)(2,1)S(1)}, bf16[4,512,128]{2,1,0:T(8,128)(2,1)S(1)}, u32[]{:S(2)}, u32[]{:S(2)}) collective-permute-start(bf16[4,512,128]{2,1,0:T(8,128)(2,1)S(1)} %slice.18.xs), channel_id=1, source_target_pairs={{0,8},{16,18},{1,9},{17,19},{2,10},{18,16},{3,11},{19,17},{4,12},{... | collective-permute-start | bytes 1572872 | tf_op jit(solution)/shard_map/ppermute | solution.py:293
  102.0 18.7 %collective-permute-start.3 = (bf16[4,512,128]{2,1,0:T(8,128)(2,1)S(1)}, bf16[4,512,128]{2,1,0:T(8,128)(2,1)S(1)}, u32[]{:S(2)}, u32[]{:S(2)}) collective-permute-start(bf16[4,512,128]{2,1,0:T(8,128)(2,1)S(1)} %slice.18.xs), channel_id=1, source_target_pairs={{0,4},{16,17},{1,5},{17,18},{2,6},{18,19},{3,7},{19,16},{4,8},{20,... | collective-permute-start | bytes 1572872 | tf_op jit(solution)/shard_map/ppermute | solution.py:293
  113.6 7.1 %copy-start.3 = (bf16[4,512,128]{2,1,0:T(8,128)(2,1)}, bf16[4,512,128]{2,1,0:T(8,128)(2,1)S(1)}, u32[]{:S(2)}) copy-start(bf16[4,512,128]{2,1,0:T(8,128)(2,1)S(1)} %collective-permute-done.1.refs_0_) | copy-start | bytes 1572868
  115.2 5.5 %copy-start.4 = (bf16[4,512,128]{2,1,0:T(8,128)(2,1)}, bf16[4,512,128]{2,1,0:T(8,128)(2,1)S(1)}, u32[]{:S(2)}) copy-start(bf16[4,512,128]{2,1,0:T(8,128)(2,1)S(1)} %collective-permute-done.2.refs_1_) | copy-start | bytes 1572868
  120.7 0.9 copy-start.5
  130.8 15.7 %collective-permute-start.6 = (bf16[4,512,128]{2,1,0:T(8,128)(2,1)}, bf16[4,512,128]{2,1,0:T(8,128)(2,1)S(1)}, u32[]{:S(2)}, u32[]{:S(2)}) collective-permute-start(bf16[4,512,128]{2,1,0:T(8,128)(2,1)} %get-tuple-element.23), channel_id=1, source_target_pairs={{0,12},{16,19},{1,13},{17,16},{2,14},{18,17},{3,15},{19,18},{4,0},... | collective-permute-start | bytes 1572872 | tf_op jit(solution)/shard_map/ppermute | solution.py:293
  134.7 13.9 %collective-permute-start.5 = (bf16[4,512,128]{2,1,0:T(8,128)(2,1)}, bf16[4,512,128]{2,1,0:T(8,128)(2,1)S(1)}, u32[]{:S(2)}, u32[]{:S(2)}) collective-permute-start(bf16[4,512,128]{2,1,0:T(8,128)(2,1)} %get-tuple-element.22), channel_id=1, source_target_pairs={{0,8},{16,18},{1,9},{17,19},{2,10},{18,16},{3,11},{19,17},{4,12},{... | collective-permute-start | bytes 1572872 | tf_op jit(solution)/shard_map/ppermute | solution.py:293
  138.1 17.8 %copy-start.2 = (bf16[4,512,128]{2,1,0:T(8,128)(2,1)S(1)}, bf16[4,512,128]{2,1,0:T(8,128)(2,1)}, u32[]{:S(2)}) copy-start(bf16[4,512,128]{2,1,0:T(8,128)(2,1)} %get-tuple-element.20) | copy-start | bytes 1572868
  138.1 17.8 %collective-permute-start.4 = (bf16[4,512,128]{2,1,0:T(8,128)(2,1)}, bf16[4,512,128]{2,1,0:T(8,128)(2,1)S(1)}, u32[]{:S(2)}, u32[]{:S(2)}) collective-permute-start(bf16[4,512,128]{2,1,0:T(8,128)(2,1)} %get-tuple-element.21), channel_id=1, source_target_pairs={{0,4},{16,17},{1,5},{17,18},{2,6},{18,19},{3,7},{19,16},{4,8},{20,... | collective-permute-start | bytes 1572872 | tf_op jit(solution)/shard_map/ppermute | solution.py:293
  143.0 14.0 %all-to-all-start.5 = ((bf16[4,512,128]{2,1,0:T(8,128)(2,1)}), bf16[4,512,128]{2,1,0:T(8,128)(2,1)S(1)}, u32[]{:S(2)}, u32[]{:S(2)}) async-start(bf16[4,512,128]{2,1,0:T(8,128)(2,1)} %reduce_sum.46), calls=%async_computation.5 | async-start | bytes 1048576 | tf_op jit(solution)/shard_map/all_to_all | solution.py:273
  157.0 11.5 %all-to-all-start.3 = ((bf16[4,512,128]{2,1,0:T(8,128)(2,1)}), bf16[4,512,128]{2,1,0:T(8,128)(2,1)S(1)}, u32[]{:S(2)}, u32[]{:S(2)}) async-start(bf16[4,512,128]{2,1,0:T(8,128)(2,1)} %add_convert_fusion), calls=%async_computation.3 | async-start | bytes 1048576 | tf_op jit(solution)/shard_map/all_to_all | solution.py:273
  160.5 36.9 %copy-start.7 = (bf16[128]{0:T(256)(128)(2,1)S(1)}, bf16[128]{0:T(256)(128)(2,1)}, u32[]{:S(2)}) copy-start(bf16[128]{0:T(256)(128)(2,1)} %param.15) | copy-start | bytes 772
  160.6 8.0 %collective-permute-start.7 = (bf16[512,128]{1,0:T(8,128)(2,1)S(1)}, bf16[512,128]{1,0:T(8,128)(2,1)S(1)}, u32[]{:S(2)}, u32[]{:S(2)}) collective-permute-start(bf16[512,128]{1,0:T(8,128)(2,1)S(1)} %reduce_sum.47), channel_id=1, source_target_pairs={{0,16},{16,0},{1,17},{17,1},{2,18},{18,2},{3,19},{19,3},{4,20},{20... | collective-permute-start | bytes 393224 | tf_op jit(solution)/shard_map/ppermute | solution.py:297
  191.4 13.6 %all-to-all-start.7 = ((f32[16,1,256]{2,1,0:T(1,128)}), f32[16,1,256]{2,1,0:T(1,128)S(1)}, u32[]{:S(2)}, u32[]{:S(2)}) async-start(f32[16,1,256]{2,1,0:T(1,128)} %get-tuple-element.26), calls=%async_computation.7 | async-start | bytes 32768 | tf_op jit(solution)/shard_map/all_to_all | solution.py:273

commit v3 on v2

--- a/solution.py
+++ b/solution.py
@@ -14,16 +14,16 @@
 GAIN_ROWS = 16
 
 
-def pack_kernel(pos, routes, weights, tokens, near, far, table):
+def pack_kernel(pos, routes, weights, tokens, out, table):
     tok = tokens.shape[0]
-    half = near.shape[0]
+    count = out.shape[0]
     experts = 2 * lax.axis_size("z")
-    cap = half // (experts // 2)
+    cap = count // experts
     e0 = routes[0:1, :]
     e1 = routes[1:2, :]
-    lanes = lax.broadcasted_iota(jnp.int32, (experts, tok), 0)
-    hot0 = lanes == e0
-    hot1 = lanes == e1
+    names = lax.broadcasted_iota(jnp.int32, (experts, tok), 0)
+    hot0 = names == e0
+    hot1 = names == e1
     hot = (hot0 | hot1).astype(F32).astype(BF16)
     row = lax.broadcasted_iota(jnp.int32, (tok, tok), 0)
     col = lax.broadcasted_iota(jnp.int32, (tok, tok), 1)
@@ -32,24 +32,13 @@
 
     def place(e, mine):
         slot = jnp.sum(jnp.where(mine, before, 0.0), axis=0, keepdims=True)
-        other = jnp.bitwise_xor(jnp.bitwise_and(e, 1), pos[0])
-        return other * half + (e >> 1) * cap + slot.astype(jnp.int32)
+        return jnp.bitwise_xor(e, pos[0]) * cap + slot.astype(jnp.int32)
 
     t0 = place(e0, hot0)
     t1 = place(e1, hot1)
-    for at, out in ((0, near), (half, far)):
-        rows = lax.broadcasted_iota(jnp.int32, (half, tok), 0) + at
-        put = ((rows == t0) | (rows == t1)).astype(F32).astype(BF16)
-        out[...] = jnp.dot(put, tokens[...], preferred_element_type=F32).astype(BF16)
-
-    def packed(t):
-        other = (t >= half).astype(jnp.int32)
-        inside = t - other * half
-        at_z = inside // cap
-        return (at_z * 2 + other) * cap + (inside - at_z * cap)
-
-    t0 = packed(t0)
-    t1 = packed(t1)
+    rows = lax.broadcasted_iota(jnp.int32, (count, tok), 0)
+    put = ((rows == t0) | (rows == t1)).astype(F32).astype(BF16)
+    out[...] = jnp.dot(put, tokens[...], preferred_element_type=F32).astype(BF16)
     stack = jnp.concatenate(
         [t0.astype(F32), t1.astype(F32), weights[...], jnp.zeros((4, tok), F32)], axis=0
     )
@@ -58,43 +47,34 @@
 
 def pack(c, routes, weights, tokens):
     tok, share = tokens.shape
-    half = lax.axis_size("z") * 32
+    count = 2 * lax.axis_size("z") * 32
     vmem = pl.BlockSpec(memory_space=pltpu.VMEM)
     return pl.pallas_call(
         pack_kernel,
         out_shape=(
-            jax.ShapeDtypeStruct((half, share), BF16),
-            jax.ShapeDtypeStruct((half, share), BF16),
+            jax.ShapeDtypeStruct((count, share), BF16),
             jax.ShapeDtypeStruct((tok, 8), F32),
         ),
         in_specs=[pl.BlockSpec(memory_space=pltpu.SMEM), vmem, vmem, vmem],
-        out_specs=(vmem, vmem, vmem),
+        out_specs=(vmem, vmem),
         name="pack",
     )(c, routes, weights, tokens)
 
 
-def expert_kernel(first, rows, core_ref, y_ref, x_ref, xs, *refs):
+def expert_kernel(first, rows, core_ref, y_ref, x_ref, xs, wg, wu, wd, *refs):
     if first:
-        wg, wu, wd, out, gain_out = refs[:5]
-        refs = refs[5:]
-        outs = [out.at[o] for o in range(4)]
+        out, gain_out = refs[:2]
     else:
-        more = refs[0:3]
-        wg, wu, wd, gain_in = refs[3:7]
-        outs = refs[7:11]
-        refs = refs[11:]
-    raw, gain_s, xn, gu_s, d_s, stage, sems, osems = refs
+        gain_in, out = refs[:2]
+    raw, gain_s, xn, gu_s, d_s, stage, sems, osems = refs[2:]
     core = core_ref[0]
-    at_outer = jnp.where(core == 0, y_ref[0], x_ref[0])
-
-    def block(o, inner):
-        outer = o if first else jnp.bitwise_and(at_outer + o, 3)
+    at_inner = jnp.where(core == 0, x_ref[0], y_ref[0])
+
+    def block(outer, inner):
         return jnp.where(core == 0, outer * 4 + inner, inner * 4 + outer)
 
-    def source(o):
-        if first:
-            return xs.at[o]
-        return xs if o == 0 else more[o - 1]
+    def taken(outer, inner):
+        return block(outer, inner if first else jnp.bitwise_and(at_inner + inner, 3))
 
     count = [0]
 
@@ -110,7 +90,7 @@
 
     def fetch_rows(at):
         return [
-            fetch(source(o).at[i, pl.ds(at, half), :], raw.at[block(o, i), pl.ds(at, half), :])
+            fetch(xs.at[o, i, pl.ds(at, half), :], raw.at[taken(o, i), pl.ds(at, half), :])
             for o in range(4)
             for i in range(4)
         ]
@@ -118,7 +98,7 @@
     x_cp = [fetch_rows(0)]
     if first:
         gain_cp = [
-            fetch(source(o).at[i, pl.ds(rows, GAIN_ROWS), :], gain_s.at[block(o, i)])
+            fetch(xs.at[o, i, pl.ds(rows, GAIN_ROWS), :], gain_s.at[taken(o, i)])
             for o in range(4)
             for i in range(4)
         ]
@@ -179,7 +159,7 @@
         ).astype(BF16)
         for i in range(4):
             stage[o, i] = res[:, i * 128 : (i + 1) * 128]
-        store(o, stage.at[o], outs[o])
+        store(o, stage.at[o], out.at[o])
     for cp in copies:
         cp.wait()
 
@@ -188,15 +168,12 @@
     rows = 512
     width, units = weights[0].shape
     hbm = pl.BlockSpec(memory_space=pltpu.HBM)
+    args = (*place, xs, *weights)
+    outs = (jax.ShapeDtypeStruct((4, 4, rows, 128), BF16),)
     if first:
-        args = (*place, xs, *weights)
-        outs = (
-            jax.ShapeDtypeStruct((4, 4, rows, 128), BF16),
-            jax.ShapeDtypeStruct((16, GAIN_ROWS, 128), BF16),
-        )
+        outs = (*outs, jax.ShapeDtypeStruct((16, GAIN_ROWS, 128), BF16))
     else:
-        args = (*place, *xs, *weights, gain)
-        outs = tuple([jax.ShapeDtypeStruct((4, rows, 128), BF16)] * 4)
+        args = (*args, gain)
     return pl.pallas_call(
         functools.partial(expert_kernel, first, rows),
         out_shape=outs,
@@ -213,7 +190,7 @@
             pltpu.SemaphoreType.DMA((5,)),
         ],
         compiler_params=pltpu.CompilerParams(vmem_limit_bytes=63 * 1024 * 1024),
-        name="expert_far" if first else "expert_near",
+        name="expert_near" if first else "expert_far",
     )(*args)
 
 
@@ -283,13 +260,13 @@
     return exchange(v, ALL, lines(1))
 
 
-def outer_shift(v, step):
+def inner_ahead(v, step):
     pairs = []
     for z in range(16):
         for y in range(4):
             for x in range(4):
-                pairs.append((flat(z, 0, y, x), flat(z, 0, (y + step) % 4, x)))
-                pairs.append((flat(z, 1, y, x), flat(z, 1, y, (x + step) % 4)))
+                pairs.append((flat(z, 0, y, (x + step) % 4), flat(z, 0, y, x)))
+                pairs.append((flat(z, 1, (y + step) % 4, x), flat(z, 1, y, x)))
     return lax.ppermute(v, ALL, pairs)
 
 
@@ -305,39 +282,36 @@
 
 
 def summed(v):
-    return v.astype(F32).sum(axis=0).astype(BF16)
-
-
-def over_z(near, far):
-    share = near.shape[1]
-    both = jnp.stack([near.reshape(16, -1, share), far.reshape(16, -1, share)], axis=1)
-    return exchange(both, "z")
+    return total_of([v[i] for i in range(v.shape[0])])
+
+
+def copies(v):
+    return jnp.broadcast_to(v[None], (4, *v.shape))
 
 
 def local(tokens, norm_gain, w_gate, w_up, w_down, routes, route_weights, final_gain):
     _, share = tokens.shape
     width = share * 16
     place = tuple(lax.axis_index(a).astype(jnp.int32).reshape(1) for a in ("c", "y", "x"))
-    near, far, table = pack(place[0], routes.T, route_weights.T, tokens)
+    rows, table = pack(place[0], routes.T, route_weights.T, tokens)
     weights = (w_gate[0], w_up[0], w_down[0])
-    both = over_z(near, swap(far))
+    both = exchange(rows.reshape(16, 2, -1, share), "z")
     near, far = (both[:, i].reshape(-1, share) for i in range(2))
     gain_rows = jnp.broadcast_to(norm_gain[None, :], (GAIN_ROWS, share))
-    rows = jnp.concatenate([far, gain_rows, near], axis=0)
-    rows = inner_exchange(jnp.broadcast_to(rows[None], (4, *rows.shape)))
-    first = far.shape[0] + GAIN_ROWS
-    far = rows[:, :first]
-    far = outer_exchange(jnp.broadcast_to(far[None], (4, *far.shape)))
-    near = rows[:, first:]
-    near = [near] + [outer_shift(near, -s) for s in (1, 2, 3)]
-    far, gain = expert(True, place, far, weights, None)
+    near = inner_exchange(copies(jnp.concatenate([near, gain_rows], axis=0)))
+    far = swap(far)
+    near = outer_exchange(copies(near))
+    far = jnp.stack([far] + [inner_ahead(far, s) for s in (1, 2, 3)])
+    far = outer_exchange(copies(far))
+    near, gain = expert(True, place, near, weights, None)
+    near = summed(outer_exchange(near))
+    far = expert(False, place, far, weights, gain)[0]
     far = summed(outer_exchange(far))
-    near = expert(False, place, near, weights, gain)
-    near = total_of([near[0]] + [outer_shift(near[s], s) for s in (1, 2, 3)])
-    far = swap(summed(inner_exchange(far)))
-    near = summed(inner_exchange(near))
-    both = over_z(near, far)
-    combined, squares = combine(table, both.reshape(-1, share))
+    last = summed(inner_exchange(jnp.concatenate([near, far], axis=1)))
+    near = last[: near.shape[1]]
+    far = swap(last[near.shape[0] :])
+    both = jnp.stack([near.reshape(16, -1, share), far.reshape(16, -1, share)], axis=1)
+    combined, squares = combine(table, exchange(both, "z").reshape(-1, share))
     total = exchange(squares, ("y", "x")).sum(axis=(0, 1))
     scale = lax.rsqrt(total / width + EPS)
     return (combined * scale[:, None] * final_gain.astype(F32)[None, :]).astype(BF16)

time: 208 us -> 205 us (0.986)
  blocking collectives: 69 us -> 104 us
  waiting for transfers between devices: 57.4 us -> 39.9 us
  starting transfers between devices: 45.6 us -> 28.2 us
  other arithmetic: 6.78 us -> 4.07 us
    all_to_all x3 -> x5, blocking collectives: 69 us -> 104 us  [exchange(): lax.all_to_all(v, axis, split_axis=0, concat_axis=0, tiled=True, axis_ind...]
    ppermute x6 -> x3, waiting for transfers between devices: 25.4 us -> 6.14 us  [inner_ahead(): return lax.ppermute(v, ALL, pairs)]
    ppermute x6 -> x3, starting transfers between devices: 20 us -> 8.36 us  [inner_ahead(): return lax.ppermute(v, ALL, pairs)]
    all_to_all x5 -> x4, starting transfers between devices: 21.8 us -> 16 us  [exchange(): lax.all_to_all(v, axis, split_axis=0, concat_axis=0, tiled=True, axis_ind...]
    reduce_sum x3 -> x0, other arithmetic: 3.02 us -> none  [summed(): return v.astype(F32).sum(axis=0).astype(BF16)]
    all_to_all x5 -> x4, waiting for transfers between devices: 30.5 us -> 31.2 us  [exchange(): lax.all_to_all(v, axis, split_axis=0, concat_axis=0, tiled=True, axis_ind...]
  transfers between devices with their start and end apart: 13 -> 9, of which waited for: 9 -> 8; matrix products, arithmetic and copies ran while one was open for 3% -> 1% of each run, Pallas kernels for 4% -> 5%
where the time goes in v3:
time: 205 us; the launch traced here: 204 us
  blocking collectives  104 us (51%)
  waiting for transfers between devices  39.9 us (19%)
  starting transfers between devices  28.2 us (14%)
  Pallas kernels  22.7 us (11%)
  local copies, waits for them, and re-layouts  4.42 us (2%)
  other arithmetic  4.07 us (2%)
    all_to_all x5, blocking collectives, exchange(): lax.all_to_all(v, axis, split_axis=0, concat_axis=0, tiled=True, axis_ind...  104 us
    all_to_all x4, waiting for transfers between devices, exchange(): lax.all_to_all(v, axis, split_axis=0, concat_axis=0, tiled=True, axis_ind...  31.2 us
    pallas_call x2, Pallas kernels, expert(): pl.pallas_call(functools.partial(expert_kernel, first, rows), out_shape=o...  18.4 us
    all_to_all x4, starting transfers between devices, exchange(): lax.all_to_all(v, axis, split_axis=0, concat_axis=0, tiled=True, axis_ind...  16 us
    ppermute x3, starting transfers between devices, inner_ahead(): return lax.ppermute(v, ALL, pairs)  8.36 us
    ppermute x3, waiting for transfers between devices, inner_ahead(): return lax.ppermute(v, ALL, pairs)  6.14 us
  transfers between devices with their start and end apart: 9, of which 8 were waited for; matrix products, arithmetic and copies ran while one was open for 1% of the time, Pallas kernels for 5%

profile of v3, /device:TPU:32, one launch (start us, length us, event | category | flops | bytes accessed | tf_op | source)
XLA Modules:
  0.0 203.6 jit_solution(16510291664896852856)
XLA Ops:
  0.0 2.1 %pack.1 = (bf16[1024,128]{1,0:T(8,128)(2,1)}, f32[256,8]{1,0:T(8,128)}) custom-call(s32[1]{0:T(128)} %bitcast.pos.core_ref, s32[2,256]{1,0:T(2,128)} %bitcast.44, f32[2,256]{1,0:T(2,128)} %bitcast.45, bf16[256,128]{1,0:T(8,128)(2,1)} %tokens.1), custom_call_target="tpu_custom_call" | custom-call | tf_op jit(solution)/shard_map/pack/pallas_call | solution.py:52
  2.1 33.1 %all_to_all.45 = bf16[16,2,32,128]{3,2,1,0:T(8,128)(2,1)S(1)} all-to-all(bf16[16,2,32,128]{3,2,1,0:T(8,128)(2,1)} %bitcast.37), channel_id=1, replica_groups=mesh['z'=16,'c'=2,'y'=4,'x'=4] {'z'}, dimensions={0} | all-to-all | bytes 524288 | tf_op jit(solution)/shard_map/all_to_all | solution.py:250
  35.2 0.7 broadcast_in_dim.8
  36.0 12.3 %all_to_all.46 = bf16[4,528,128]{2,1,0:T(8,128)(2,1)S(1)} all-to-all(bf16[4,528,128]{2,1,0:T(8,128)(2,1)S(1)} %broadcast_in_dim.9), channel_id=1, replica_groups={{0,1,2,3},{4,5,6,7},{8,9,10,11},{12,13,14,15},{16,20,24,28},{17,21,25,2..., dimensions={0} | all-to-all | bytes 1081344 | tf_op jit(solution)/shard_map/all_to_all | solution.py:250
  48.2 1.6 broadcast_in_dim.10
  49.9 4.5 %all-to-all-start.2 = ((bf16[4,4,528,128]{3,2,1,0:T(8,128)(2,1)}), bf16[4,4,528,128]{3,2,1,0:T(8,128)(2,1)S(1)}, u32[]{:S(2)}, u32[]{:S(2)}) async-start(bf16[4,4,528,128]{3,2,1,0:T(8,128)(2,1)} %broadcast_in_dim.10), calls=%async_computation.2 | async-start | bytes 4325376 | tf_op jit(solution)/shard_map/all_to_all | solution.py:250
  54.3 1.9 collective-permute-start
  56.2 1.3 collective-permute-done
  57.6 3.1 %collective-permute-start.1 = (bf16[512,128]{1,0:T(8,128)(2,1)S(1)}, bf16[512,128]{1,0:T(8,128)(2,1)S(1)}, u32[]{:S(2)}, u32[]{:S(2)}) collective-permute-start(bf16[512,128]{1,0:T(8,128)(2,1)S(1)} %collective-permute-done), channel_id=1, source_target_pairs={{1,0},{20,16},{2,1},{21,17},{3,2},{22,18},{0,3},{23,19},{5,4},{24,... | collective-permute-start | bytes 393224 | tf_op jit(solution)/shard_map/ppermute | solution.py:270
  60.6 3.4 %collective-permute-start.2 = (bf16[512,128]{1,0:T(8,128)(2,1)S(1)}, bf16[512,128]{1,0:T(8,128)(2,1)S(1)}, u32[]{:S(2)}, u32[]{:S(2)}) collective-permute-start(bf16[512,128]{1,0:T(8,128)(2,1)S(1)} %collective-permute-done), channel_id=1, source_target_pairs={{2,0},{24,16},{3,1},{25,17},{0,2},{26,18},{1,3},{27,19},{6,4},{28,... | collective-permute-start | bytes 393224 | tf_op jit(solution)/shard_map/ppermute | solution.py:270
  64.0 1.9 collective-permute-start.3
  66.0 3.0 %collective-permute-done.2 = bf16[512,128]{1,0:T(8,128)(2,1)S(1)} collective-permute-done((bf16[512,128]{1,0:T(8,128)(2,1)S(1)}, bf16[512,128]{1,0:T(8,128)(2,1)S(1)}, u32[]{:S(2)}, u32[]{:S(2)}) %collective-permute-start.2) | collective-permute-done | bytes 131104 | tf_op jit(solution)/shard_map/ppermute | solution.py:270
  69.0 3.1 %collective-permute-done.3 = bf16[512,128]{1,0:T(8,128)(2,1)S(1)} collective-permute-done((bf16[512,128]{1,0:T(8,128)(2,1)S(1)}, bf16[512,128]{1,0:T(8,128)(2,1)S(1)}, u32[]{:S(2)}, u32[]{:S(2)}) %collective-permute-start.3) | collective-permute-done | bytes 131104 | tf_op jit(solution)/shard_map/ppermute | solution.py:270
  72.2 1.7 all-to-all-done.2.xs
  73.8 2.0 broadcast_in_dim.11
  75.8 4.4 %all-to-all-start.4 = ((bf16[4,4,512,128]{3,2,1,0:T(8,128)(2,1)}), bf16[4,4,512,128]{3,2,1,0:T(8,128)(2,1)}, u32[]{:S(2)}, u32[]{:S(2)}) async-start(bf16[4,4,512,128]{3,2,1,0:T(8,128)(2,1)} %broadcast_in_dim.11), calls=%async_computation.4 | async-start | bytes 4194304 | tf_op jit(solution)/shard_map/all_to_all | solution.py:250
  80.3 9.2 %expert_near.1 = (bf16[4,4,512,128]{3,2,1,0:T(8,128)(2,1)}, bf16[16,16,128]{2,1,0:T(8,128)(2,1)}) custom-call(s32[1]{0:T(128)} %bitcast.pos.core_ref, s32[1]{0:T(128)} %bitcast.3.y_ref, s32[1]{0:T(128)} %bitcast.4.x_ref, bf16[4,4,528,128]{3,2,1,0:T(8,128)(2,1)} %copy-done, bf16[2048,384]{1,0:T(8,128)(2,1)} %bitcast.28, bf16[2048,384]{1,0:T(8,128)(2,1)} %bitcast.30, ...), custom_call_target="tpu_custom_call" | custom-call | tf_op jit(solution)/shard_map/expert_near/pallas_call | solution.py:177
  89.5 7.3 %all-to-all-done.4.xs = bf16[4,4,512,128]{3,2,1,0:T(8,128)(2,1)} async-done(((bf16[4,4,512,128]{3,2,1,0:T(8,128)(2,1)}), bf16[4,4,512,128]{3,2,1,0:T(8,128)(2,1)}, u32[]{:S(2)}, u32[]{:S(2)}) %all-to-all-start.4) | async-done | bytes 2097184 | tf_op jit(solution)/shard_map/all_to_all | solution.py:250
  96.9 9.2 %expert_far.1 = bf16[4,4,512,128]{3,2,1,0:T(8,128)(2,1)} custom-call(s32[1]{0:T(128)} %bitcast.pos.core_ref, s32[1]{0:T(128)} %bitcast.3.y_ref, s32[1]{0:T(128)} %bitcast.4.x_ref, bf16[4,4,512,128]{3,2,1,0:T(8,128)(2,1)} %all-to-all-done.4.xs, bf16[2048,384]{1,0:T(8,128)(2,1)} %bitcast.29, bf16[2048,384]{1,0:T(8,128)(2,1)} %bitcast.31, ...), custom_call_target="tpu_custom_call" | custom-call | tf_op jit(solution)/shard_map/expert_far/pallas_call | solution.py:177
  106.0 21.0 %all_to_all.47 = bf16[4,4,512,128]{3,2,1,0:T(8,128)(2,1)} all-to-all(bf16[4,4,512,128]{3,2,1,0:T(8,128)(2,1)} %expert_far.1), channel_id=1, replica_groups={{0,4,8,12},{1,5,9,13},{2,6,10,14},{3,7,11,15},{16,17,18,19},{20,21,22,2..., dimensions={0} | all-to-all | bytes 4194304 | tf_op jit(solution)/shard_map/all_to_all | solution.py:250
  127.0 3.6 %all-to-all-start.3 = ((bf16[4,4,512,128]{3,2,1,0:T(8,128)(2,1)}), bf16[4,4,512,128]{3,2,1,0:T(8,128)(2,1)S(1)}, u32[]{:S(2)}, u32[]{:S(2)}) async-start(bf16[4,4,512,128]{3,2,1,0:T(8,128)(2,1)} %get-tuple-element.13), calls=%async_computation.3 | async-start | bytes 4194304 | tf_op jit(solution)/shard_map/all_to_all | solution.py:250
  130.6 1.8 fusion.1
  132.4 14.7 %all-to-all-done.3 = bf16[4,4,512,128]{3,2,1,0:T(8,128)(2,1)S(1)} async-done(((bf16[4,4,512,128]{3,2,1,0:T(8,128)(2,1)}), bf16[4,4,512,128]{3,2,1,0:T(8,128)(2,1)S(1)}, u32[]{:S(2)}, u32[]{:S(2)}) %all-to-all-start.3) | async-done | bytes 2097184 | tf_op jit(solution)/shard_map/all_to_all | solution.py:250
  147.1 0.3 fusion
  147.5 13.3 %all_to_all.48 = bf16[4,1024,128]{2,1,0:T(8,128)(2,1)S(1)} all-to-all(bf16[4,1024,128]{2,1,0:T(8,128)(2,1)S(1)} %pad_maximum_fusion), channel_id=1, replica_groups={{0,1,2,3},{4,5,6,7},{8,9,10,11},{12,13,14,15},{16,20,24,28},{17,21,25,2..., dimensions={0} | all-to-all | bytes 2097152 | tf_op jit(solution)/shard_map/all_to_all | solution.py:250
  160.9 1.9 collective-permute-start.4
  162.9 1.3 collective-permute-done.4
  164.2 24.5 %all_to_all.49 = bf16[16,2,32,128]{3,2,1,0:T(8,128)(2,1)} all-to-all(bf16[16,2,32,128]{3,2,1,0:T(8,128)(2,1)S(1)} %pad_maximum_fusion.2), channel_id=1, replica_groups=mesh['z'=16,'c'=2,'y'=4,'x'=4] {'z'}, dimensions={0} | all-to-all | bytes 524288 | tf_op jit(solution)/shard_map/all_to_all | solution.py:250
  188.7 2.2 %combine.1 = (f32[256,128]{1,0:T(8,128)}, f32[16,1,256]{2,1,0:T(1,128)}) custom-call(f32[256,8]{1,0:T(8,128)} %get-tuple-element.11.table, bf16[1024,128]{1,0:T(8,128)(2,1)} %bitcast.34), custom_call_target="tpu_custom_call" | custom-call | tf_op jit(solution)/shard_map/combine/pallas_call | solution.py:218
  190.9 3.5 %all-to-all-start.8 = ((f32[16,1,256]{2,1,0:T(1,128)}), f32[16,1,256]{2,1,0:T(1,128)S(1)}, u32[]{:S(2)}, u32[]{:S(2)}) async-start(f32[16,1,256]{2,1,0:T(1,128)} %get-tuple-element.16), calls=%async_computation.8 | async-start | bytes 32768 | tf_op jit(solution)/shard_map/all_to_all | solution.py:250
  194.4 7.5 %all-to-all-done.8 = f32[16,1,256]{2,1,0:T(1,128)S(1)} async-done(((f32[16,1,256]{2,1,0:T(1,128)}), f32[16,1,256]{2,1,0:T(1,128)S(1)}, u32[]{:S(2)}, u32[]{:S(2)}) %all-to-all-start.8) | async-done | bytes 16416 | tf_op jit(solution)/shard_map/all_to_all | solution.py:250
  202.0 1.6 multiply_convert_fusion
  (16 shorter events, 0.5 us)
Async XLA Ops:
  49.9 24.0 %all-to-all-start.2 = ((bf16[4,4,528,128]{3,2,1,0:T(8,128)(2,1)}), bf16[4,4,528,128]{3,2,1,0:T(8,128)(2,1)S(1)}, u32[]{:S(2)}, u32[]{:S(2)}) async-start(bf16[4,4,528,128]{3,2,1,0:T(8,128)(2,1)} %broadcast_in_dim.10), calls=%async_computation.2 | async-start | bytes 4325376 | tf_op jit(solution)/shard_map/all_to_all | solution.py:250
  54.3 3.2 %collective-permute-start = (bf16[512,128]{1,0:T(8,128)(2,1)S(1)}, bf16[512,128]{1,0:T(8,128)(2,1)S(1)}, u32[]{:S(2)}, u32[]{:S(2)}) collective-permute-start(bf16[512,128]{1,0:T(8,128)(2,1)S(1)} %bitcast.38), channel_id=1, source_target_pairs={{0,16},{16,0},{1,17},{17,1},{2,18},{18,2},{3,19},{19,3},{4,20},{20... | collective-permute-start | bytes 393224 | tf_op jit(solution)/shard_map/ppermute | solution.py:274
  57.6 8.4 %collective-permute-start.1 = (bf16[512,128]{1,0:T(8,128)(2,1)S(1)}, bf16[512,128]{1,0:T(8,128)(2,1)S(1)}, u32[]{:S(2)}, u32[]{:S(2)}) collective-permute-start(bf16[512,128]{1,0:T(8,128)(2,1)S(1)} %collective-permute-done), channel_id=1, source_target_pairs={{1,0},{20,16},{2,1},{21,17},{3,2},{22,18},{0,3},{23,19},{5,4},{24,... | collective-permute-start | bytes 393224 | tf_op jit(solution)/shard_map/ppermute | solution.py:270
  60.6 8.4 %collective-permute-start.2 = (bf16[512,128]{1,0:T(8,128)(2,1)S(1)}, bf16[512,128]{1,0:T(8,128)(2,1)S(1)}, u32[]{:S(2)}, u32[]{:S(2)}) collective-permute-start(bf16[512,128]{1,0:T(8,128)(2,1)S(1)} %collective-permute-done), channel_id=1, source_target_pairs={{2,0},{24,16},{3,1},{25,17},{0,2},{26,18},{1,3},{27,19},{6,4},{28,... | collective-permute-start | bytes 393224 | tf_op jit(solution)/shard_map/ppermute | solution.py:270
  64.0 8.1 %collective-permute-start.3 = (bf16[512,128]{1,0:T(8,128)(2,1)S(1)}, bf16[512,128]{1,0:T(8,128)(2,1)S(1)}, u32[]{:S(2)}, u32[]{:S(2)}) collective-permute-start(bf16[512,128]{1,0:T(8,128)(2,1)S(1)} %collective-permute-done), channel_id=1, source_target_pairs={{3,0},{28,16},{0,1},{29,17},{1,2},{30,18},{2,3},{31,19},{7,4},{16,... | collective-permute-start | bytes 393224 | tf_op jit(solution)/shard_map/ppermute | solution.py:270
  73.8 2.0 copy-start
  75.8 21.0 %all-to-all-start.4 = ((bf16[4,4,512,128]{3,2,1,0:T(8,128)(2,1)}), bf16[4,4,512,128]{3,2,1,0:T(8,128)(2,1)}, u32[]{:S(2)}, u32[]{:S(2)}) async-start(bf16[4,4,512,128]{3,2,1,0:T(8,128)(2,1)} %broadcast_in_dim.11), calls=%async_computation.4 | async-start | bytes 4194304 | tf_op jit(solution)/shard_map/all_to_all | solution.py:250
  127.0 20.1 %all-to-all-start.3 = ((bf16[4,4,512,128]{3,2,1,0:T(8,128)(2,1)}), bf16[4,4,512,128]{3,2,1,0:T(8,128)(2,1)S(1)}, u32[]{:S(2)}, u32[]{:S(2)}) async-start(bf16[4,4,512,128]{3,2,1,0:T(8,128)(2,1)} %get-tuple-element.13), calls=%async_computation.3 | async-start | bytes 4194304 | tf_op jit(solution)/shard_map/all_to_all | solution.py:250
  160.8 33.7 %copy-start.1 = (bf16[128]{0:T(256)(128)(2,1)S(1)}, bf16[128]{0:T(256)(128)(2,1)}, u32[]{:S(2)}) copy-start(bf16[128]{0:T(256)(128)(2,1)} %param.15) | copy-start | bytes 772
  160.9 3.2 %collective-permute-start.4 = (bf16[512,128]{1,0:T(8,128)(2,1)S(1)}, bf16[512,128]{1,0:T(8,128)(2,1)S(1)}, u32[]{:S(2)}, u32[]{:S(2)}) collective-permute-start(bf16[512,128]{1,0:T(8,128)(2,1)S(1)} %get-tuple-element.18), channel_id=1, source_target_pairs={{0,16},{16,0},{1,17},{17,1},{2,18},{18,2},{3,19},{19,3},{4,20},{20... | collective-permute-start | bytes 393224 | tf_op jit(solution)/shard_map/ppermute | solution.py:274
  190.9 11.0 %all-to-all-start.8 = ((f32[16,1,256]{2,1,0:T(1,128)}), f32[16,1,256]{2,1,0:T(1,128)S(1)}, u32[]{:S(2)}, u32[]{:S(2)}) async-start(f32[16,1,256]{2,1,0:T(1,128)} %get-tuple-element.16), calls=%async_computation.8 | async-start | bytes 32768 | tf_op jit(solution)/shard_map/all_to_all | solution.py:250

commit v4 on v2

--- a/solution.py
+++ b/solution.py
@@ -85,11 +85,15 @@
         refs = refs[11:]
     raw, gain_s, xn, gu_s, d_s, stage, sems, osems = refs
     core = core_ref[0]
-    at_outer = jnp.where(core == 0, y_ref[0], x_ref[0])
-
-    def block(o, inner):
-        outer = o if first else jnp.bitwise_and(at_outer + o, 3)
-        return jnp.where(core == 0, outer * 4 + inner, inner * 4 + outer)
+    bit_y = jnp.bitwise_and(y_ref[0] + core, 1)
+    bit_x = jnp.bitwise_and(x_ref[0] + core, 1)
+    at_outer = bit_y * 2 + bit_x
+
+    def block(o, i):
+        outer = o if first else jnp.bitwise_xor(at_outer, o)
+        y = jnp.bitwise_and(2 * (i >> 1) + (outer >> 1) + core, 3)
+        x = jnp.bitwise_and(2 * (i & 1) + (outer & 1) + core, 3)
+        return y * 4 + x
 
     def source(o):
         if first:
@@ -257,16 +261,15 @@
     return ((z * 2 + c) * 4 + y) * 4 + x
 
 
-def lines(along_x_for):
-    groups = []
-    for z in range(16):
-        for c in range(2):
-            for i in range(4):
-                if c == along_x_for:
-                    groups.append([flat(z, c, i, x) for x in range(4)])
-                else:
-                    groups.append([flat(z, c, y, i) for y in range(4)])
-    return groups
+def member(z, c, o, i):
+    y = (2 * (i >> 1) + (o >> 1) + c) % 4
+    x = (2 * (i & 1) + (o & 1) + c) % 4
+    return flat(z, c, y, x)
+
+
+PLANES = [(z, c) for z in range(16) for c in range(2)]
+INNER = [[member(z, c, o, i) for i in range(4)] for z, c in PLANES for o in range(4)]
+OUTER = [[member(z, c, o, i) for o in range(4)] for z, c in PLANES for i in range(4)]
 
 
 def exchange(v, axis, groups=None):
@@ -276,20 +279,20 @@
 
 
 def inner_exchange(v):
-    return exchange(v, ALL, lines(0))
+    return exchange(v, ALL, INNER)
 
 
 def outer_exchange(v):
-    return exchange(v, ALL, lines(1))
-
-
-def outer_shift(v, step):
-    pairs = []
-    for z in range(16):
-        for y in range(4):
-            for x in range(4):
-                pairs.append((flat(z, 0, y, x), flat(z, 0, (y + step) % 4, x)))
-                pairs.append((flat(z, 1, y, x), flat(z, 1, y, (x + step) % 4)))
+    return exchange(v, ALL, OUTER)
+
+
+def outer_flip(v, bits):
+    pairs = [
+        (member(z, c, o, i), member(z, c, o ^ bits, i))
+        for z, c in PLANES
+        for o in range(4)
+        for i in range(4)
+    ]
     return lax.ppermute(v, ALL, pairs)
 
 
@@ -305,7 +308,7 @@
 
 
 def summed(v):
-    return v.astype(F32).sum(axis=0).astype(BF16)
+    return total_of([v[i] for i in range(v.shape[0])])
 
 
 def over_z(near, far):
@@ -329,11 +332,11 @@
     far = rows[:, :first]
     far = outer_exchange(jnp.broadcast_to(far[None], (4, *far.shape)))
     near = rows[:, first:]
-    near = [near] + [outer_shift(near, -s) for s in (1, 2, 3)]
+    near = [near] + [outer_flip(near, s) for s in (1, 2, 3)]
     far, gain = expert(True, place, far, weights, None)
     far = summed(outer_exchange(far))
     near = expert(False, place, near, weights, gain)
-    near = total_of([near[0]] + [outer_shift(near[s], s) for s in (1, 2, 3)])
+    near = total_of([near[0]] + [outer_flip(near[s], s) for s in (1, 2, 3)])
     far = swap(summed(inner_exchange(far)))
     near = summed(inner_exchange(near))
     both = over_z(near, far)

time: 208 us -> 218 us (1.048)
  blocking collectives: 69 us -> 76.7 us
  starting transfers between devices: 45.6 us -> 49.5 us
    ppermute x6, waiting for transfers between devices: 25.4 us -> 17.4 us  [outer_flip(): return lax.ppermute(v, ALL, pairs)]
    all_to_all x3, blocking collectives: 69 us -> 76.7 us  [exchange(): lax.all_to_all(v, axis, split_axis=0, concat_axis=0, tiled=True, axis_ind...]
    all_to_all x5, waiting for transfers between devices: 30.5 us -> 37 us  [exchange(): lax.all_to_all(v, axis, split_axis=0, concat_axis=0, tiled=True, axis_ind...]
    all_to_all x5, starting transfers between devices: 21.8 us -> 26.6 us  [exchange(): lax.all_to_all(v, axis, split_axis=0, concat_axis=0, tiled=True, axis_ind...]
    reduce_sum x3 -> x0, other arithmetic: 3.02 us -> none  [summed(): return v.astype(F32).sum(axis=0).astype(BF16)]
    add x0 -> x2, other arithmetic: none -> 2.67 us  [total_of(): total = total + p.astype(F32)]
  transfers between devices with their start and end apart: 13 -> 13, of which waited for: 9 -> 8; matrix products, arithmetic and copies ran while one was open for 3% -> 2% of each run, Pallas kernels for 4% -> 4%
where the time goes in v4:
time: 218 us; the launch traced here: 217 us
  blocking collectives  76.7 us (35%)
  waiting for transfers between devices  56 us (26%)
  starting transfers between devices  49.5 us (23%)
  Pallas kernels  22.7 us (10%)
  other arithmetic  6.48 us (3%)
  local copies, waits for them, and re-layouts  5.46 us (3%)
    all_to_all x3, blocking collectives, exchange(): lax.all_to_all(v, axis, split_axis=0, concat_axis=0, tiled=True, axis_ind...  76.7 us
    all_to_all x5, waiting for transfers between devices, exchange(): lax.all_to_all(v, axis, split_axis=0, concat_axis=0, tiled=True, axis_ind...  37 us
    all_to_all x5, starting transfers between devices, exchange(): lax.all_to_all(v, axis, split_axis=0, concat_axis=0, tiled=True, axis_ind...  26.6 us
    ppermute x6, starting transfers between devices, outer_flip(): return lax.ppermute(v, ALL, pairs)  18.6 us
    pallas_call x2, Pallas kernels, expert(): pl.pallas_call(functools.partial(expert_kernel, first, rows), out_shape=o...  18.4 us
    ppermute x6, waiting for transfers between devices, outer_flip(): return lax.ppermute(v, ALL, pairs)  17.4 us
    ppermute x2, starting transfers between devices, swap(): return lax.ppermute(v, 'c', [(0, 1), (1, 0)])  4.37 us
  transfers between devices with their start and end apart: 13, of which 8 were waited for; matrix products, arithmetic and copies ran while one was open for 2% of the time, Pallas kernels for 4%

profile of v4, /device:TPU:32, one launch (start us, length us, event | category | flops | bytes accessed | tf_op | source)
XLA Modules:
  0.0 217.0 jit_solution(7964215463495762053)
XLA Ops:
  0.0 2.1 pack.1
  2.1 1.9 collective-permute-start
  4.0 1.5 collective-permute-done
  6.5 33.4 %all_to_all.40 = bf16[16,2,32,128]{3,2,1,0:T(8,128)(2,1)S(1)} all-to-all(bf16[16,2,32,128]{3,2,1,0:T(8,128)(2,1)S(1)} %pad_maximum_fusion.1), channel_id=1, replica_groups=mesh['z'=16,'c'=2,'y'=4,'x'=4] {'z'}, dimensions={0} | all-to-all | bytes 524288 | tf_op jit(solution)/shard_map/all_to_all | solution.py:276
  40.7 20.1 %all_to_all.41 = bf16[4,1040,128]{2,1,0:T(8,128)(2,1)S(1)} all-to-all(bf16[4,1040,128]{2,1,0:T(8,128)(2,1)S(1)} %broadcast_in_dim.7), channel_id=1, replica_groups={{0,2,8,10},{1,3,9,11},{4,6,12,14},{5,7,13,15},{21,23,29,31},{22,20,30,2..., dimensions={0} | all-to-all | bytes 2129920 | tf_op jit(solution)/shard_map/all_to_all | solution.py:276
  61.9 1.7 broadcast_in_dim.8
  63.5 5.6 %all-to-all-start.2 = ((bf16[4,4,528,128]{3,2,1,0:T(8,128)(2,1)}), bf16[4,4,528,128]{3,2,1,0:T(8,128)(2,1)}, u32[]{:S(2)}, u32[]{:S(2)}) async-start(bf16[4,4,528,128]{3,2,1,0:T(8,128)(2,1)} %broadcast_in_dim.8), calls=%async_computation.2 | async-start | bytes 4325376 | tf_op jit(solution)/shard_map/all_to_all | solution.py:276
  69.1 15.5 %all-to-all-done.2.xs = bf16[4,4,528,128]{3,2,1,0:T(8,128)(2,1)} async-done(((bf16[4,4,528,128]{3,2,1,0:T(8,128)(2,1)}), bf16[4,4,528,128]{3,2,1,0:T(8,128)(2,1)}, u32[]{:S(2)}, u32[]{:S(2)}) %all-to-all-start.2) | async-done | bytes 2162720 | tf_op jit(solution)/shard_map/all_to_all | solution.py:276
  84.6 9.2 %expert_far.1 = (bf16[4,4,512,128]{3,2,1,0:T(8,128)(2,1)}, bf16[16,16,128]{2,1,0:T(8,128)(2,1)}) custom-call(s32[1]{0:T(128)} %bitcast.pos.core_ref, s32[1]{0:T(128)} %bitcast.3.y_ref, s32[1]{0:T(128)} %bitcast.4.x_ref, bf16[4,4,528,128]{3,2,1,0:T(8,128)(2,1)} %all-to-all-done.2.xs, bf16[2048,384]{1,0:T(8,128)(2,1)} %bitcast.27, bf16[2048,384]{1,0:T(8,128)(2,1)} %bitcast.29, ...), custom_call_target="tpu_custom_call" | custom-call | tf_op jit(solution)/shard_map/expert_far/pallas_call | solution.py:204
  93.9 4.5 %all-to-all-start.4 = ((bf16[4,4,512,128]{3,2,1,0:T(8,128)(2,1)}), bf16[4,4,512,128]{3,2,1,0:T(8,128)(2,1)}, u32[]{:S(2)}, u32[]{:S(2)}) async-start(bf16[4,4,512,128]{3,2,1,0:T(8,128)(2,1)} %get-tuple-element.24), calls=%async_computation.4 | async-start | bytes 4194304 | tf_op jit(solution)/shard_map/all_to_all | solution.py:276
  98.4 1.1 slice.66.xs
  99.5 3.9 %collective-permute-start.1 = (bf16[4,512,128]{2,1,0:T(8,128)(2,1)S(1)}, bf16[4,512,128]{2,1,0:T(8,128)(2,1)S(1)}, u32[]{:S(2)}, u32[]{:S(2)}) collective-permute-start(bf16[4,512,128]{2,1,0:T(8,128)(2,1)S(1)} %slice.66.xs), channel_id=1, source_target_pairs={{0,1},{2,3},{8,9},{10,11},{1,0},{3,2},{9,8},{11,10},{4,5},{6,7},{1... | collective-permute-start | bytes 1572872 | tf_op jit(solution)/shard_map/ppermute | solution.py:296
  103.3 3.4 %collective-permute-start.2 = (bf16[4,512,128]{2,1,0:T(8,128)(2,1)S(1)}, bf16[4,512,128]{2,1,0:T(8,128)(2,1)S(1)}, u32[]{:S(2)}, u32[]{:S(2)}) collective-permute-start(bf16[4,512,128]{2,1,0:T(8,128)(2,1)S(1)} %slice.66.xs), channel_id=1, source_target_pairs={{0,4},{2,6},{8,12},{10,14},{1,5},{3,7},{9,13},{11,15},{4,0},{6,2},... | collective-permute-start | bytes 1572872 | tf_op jit(solution)/shard_map/ppermute | solution.py:296
  106.7 2.0 collective-permute-start.3
  108.7 10.3 %collective-permute-done.1.refs_0_ = bf16[4,512,128]{2,1,0:T(8,128)(2,1)S(1)} collective-permute-done((bf16[4,512,128]{2,1,0:T(8,128)(2,1)S(1)}, bf16[4,512,128]{2,1,0:T(8,128)(2,1)S(1)}, u32[]{:S(2)}, u32[]{:S(2)}) %collective-permute-start.1) | collective-permute-done | bytes 524320 | tf_op jit(solution)/shard_map/ppermute | solution.py:296
  119.0 6.5 %collective-permute-done.3.refs_2_ = bf16[4,512,128]{2,1,0:T(8,128)(2,1)S(1)} collective-permute-done((bf16[4,512,128]{2,1,0:T(8,128)(2,1)S(1)}, bf16[4,512,128]{2,1,0:T(8,128)(2,1)S(1)}, u32[]{:S(2)}, u32[]{:S(2)}) %collective-permute-start.3) | collective-permute-done | bytes 524320 | tf_op jit(solution)/shard_map/ppermute | solution.py:296
  126.3 9.2 %expert_near.1 = (bf16[4,512,128]{2,1,0:T(8,128)(2,1)}, bf16[4,512,128]{2,1,0:T(8,128)(2,1)}, bf16[4,512,128]{2,1,0:T(8,128)(2,1)}, bf16[4,512,128]{2,1,0:T(8,128)(2,1)}) custom-call(s32[1]{0:T(128)} %bitcast.pos.core_ref, s32[1]{0:T(128)} %bitcast.3.y_ref, s32[1]{0:T(128)} %bitcast.4.x_ref, bf16[4,512,128]{2,1,0:T(8,128)(2,1)} %copy-done.1, ...), custom_call_target="tpu_custom_call" | custom-call | tf_op jit(solution)/shard_map/expert_near/pallas_call | solution.py:204
  135.5 3.4 %collective-permute-start.6 = (bf16[4,512,128]{2,1,0:T(8,128)(2,1)}, bf16[4,512,128]{2,1,0:T(8,128)(2,1)S(1)}, u32[]{:S(2)}, u32[]{:S(2)}) collective-permute-start(bf16[4,512,128]{2,1,0:T(8,128)(2,1)} %get-tuple-element.23), channel_id=1, source_target_pairs={{0,5},{2,7},{8,13},{10,15},{1,4},{3,6},{9,12},{11,14},{4,1},{6,3},... | collective-permute-start | bytes 1572872 | tf_op jit(solution)/shard_map/ppermute | solution.py:296
  138.9 2.6 %collective-permute-start.5 = (bf16[4,512,128]{2,1,0:T(8,128)(2,1)}, bf16[4,512,128]{2,1,0:T(8,128)(2,1)S(1)}, u32[]{:S(2)}, u32[]{:S(2)}) collective-permute-start(bf16[4,512,128]{2,1,0:T(8,128)(2,1)} %get-tuple-element.22), channel_id=1, source_target_pairs={{0,4},{2,6},{8,12},{10,14},{1,5},{3,7},{9,13},{11,15},{4,0},{6,2},... | collective-permute-start | bytes 1572872 | tf_op jit(solution)/shard_map/ppermute | solution.py:296
  141.5 3.4 %collective-permute-start.4 = (bf16[4,512,128]{2,1,0:T(8,128)(2,1)}, bf16[4,512,128]{2,1,0:T(8,128)(2,1)S(1)}, u32[]{:S(2)}, u32[]{:S(2)}) collective-permute-start(bf16[4,512,128]{2,1,0:T(8,128)(2,1)} %get-tuple-element.21), channel_id=1, source_target_pairs={{0,1},{2,3},{8,9},{10,11},{1,0},{3,2},{9,8},{11,10},{4,5},{6,7},{1... | collective-permute-start | bytes 1572872 | tf_op jit(solution)/shard_map/ppermute | solution.py:296
  144.9 2.6 %fusion = bf16[4,512,128]{2,1,0:T(8,128)(2,1)} fusion(bf16[4,4,512,128]{3,2,1,0:T(8,128)(2,1)} %all-to-all-done.4), kind=kLoop, calls=%fused_computation.2 | loop fusion | flops 2097152 | bytes 2621440 | tf_op jit(solution)/shard_map/add | solution.py:306
  147.5 5.4 %all-to-all-start.5 = ((bf16[4,512,128]{2,1,0:T(8,128)(2,1)}), bf16[4,512,128]{2,1,0:T(8,128)(2,1)S(1)}, u32[]{:S(2)}, u32[]{:S(2)}) async-start(bf16[4,512,128]{2,1,0:T(8,128)(2,1)} %fusion), calls=%async_computation.5 | async-start | bytes 1048576 | tf_op jit(solution)/shard_map/all_to_all | solution.py:276
  153.5 1.1 add_convert_fusion.1
  154.5 7.4 %all-to-all-done.5 = bf16[4,512,128]{2,1,0:T(8,128)(2,1)S(1)} async-done(((bf16[4,512,128]{2,1,0:T(8,128)(2,1)}), bf16[4,512,128]{2,1,0:T(8,128)(2,1)S(1)}, u32[]{:S(2)}, u32[]{:S(2)}) %all-to-all-start.5) | async-done | bytes 524320 | tf_op jit(solution)/shard_map/all_to_all | solution.py:276
  162.0 5.0 %all-to-all-start.3 = ((bf16[4,512,128]{2,1,0:T(8,128)(2,1)}), bf16[4,512,128]{2,1,0:T(8,128)(2,1)S(1)}, u32[]{:S(2)}, u32[]{:S(2)}) async-start(bf16[4,512,128]{2,1,0:T(8,128)(2,1)} %add_convert_fusion.1), calls=%async_computation.3 | async-start | bytes 1048576 | tf_op jit(solution)/shard_map/all_to_all | solution.py:276
  167.1 2.5 %collective-permute-start.7 = (bf16[512,128]{1,0:T(8,128)(2,1)S(1)}, bf16[512,128]{1,0:T(8,128)(2,1)S(1)}, u32[]{:S(2)}, u32[]{:S(2)}) collective-permute-start(bf16[512,128]{1,0:T(8,128)(2,1)S(1)} %fusion.1), channel_id=1, source_target_pairs={{0,16},{16,0},{1,17},{17,1},{2,18},{18,2},{3,19},{19,3},{4,20},{20... | collective-permute-start | bytes 393224 | tf_op jit(solution)/shard_map/ppermute | solution.py:300
  169.5 6.5 %all-to-all-done.3 = bf16[4,512,128]{2,1,0:T(8,128)(2,1)S(1)} async-done(((bf16[4,512,128]{2,1,0:T(8,128)(2,1)}), bf16[4,512,128]{2,1,0:T(8,128)(2,1)S(1)}, u32[]{:S(2)}, u32[]{:S(2)}) %all-to-all-start.3) | async-done | bytes 524320 | tf_op jit(solution)/shard_map/all_to_all | solution.py:276
  176.2 23.2 %all_to_all.42 = bf16[16,2,32,128]{3,2,1,0:T(8,128)(2,1)} all-to-all(bf16[16,2,32,128]{3,2,1,0:T(8,128)(2,1)S(1)} %pad_maximum_fusion.2), channel_id=1, replica_groups=mesh['z'=16,'c'=2,'y'=4,'x'=4] {'z'}, dimensions={0} | all-to-all | bytes 524288 | tf_op jit(solution)/shard_map/all_to_all | solution.py:276
  199.4 2.2 %combine.1 = (f32[256,128]{1,0:T(8,128)}, f32[16,1,256]{2,1,0:T(1,128)}) custom-call(f32[256,8]{1,0:T(8,128)} %get-tuple-element.16.table, bf16[1024,128]{1,0:T(8,128)(2,1)} %bitcast.33), custom_call_target="tpu_custom_call" | custom-call | tf_op jit(solution)/shard_map/combine/pallas_call | solution.py:245
  201.6 6.1 %all-to-all-start.7 = ((f32[16,1,256]{2,1,0:T(1,128)}), f32[16,1,256]{2,1,0:T(1,128)S(1)}, u32[]{:S(2)}, u32[]{:S(2)}) async-start(f32[16,1,256]{2,1,0:T(1,128)} %get-tuple-element.26), calls=%async_computation.7 | async-start | bytes 32768 | tf_op jit(solution)/shard_map/all_to_all | solution.py:276
  207.8 7.6 %all-to-all-done.7 = f32[16,1,256]{2,1,0:T(1,128)S(1)} async-done(((f32[16,1,256]{2,1,0:T(1,128)}), f32[16,1,256]{2,1,0:T(1,128)S(1)}, u32[]{:S(2)}, u32[]{:S(2)}) %all-to-all-start.7) | async-done | bytes 16416 | tf_op jit(solution)/shard_map/all_to_all | solution.py:276
  215.4 1.6 multiply_convert_fusion
  (32 shorter events, 4.5 us)
Async XLA Ops:
  2.1 3.4 %collective-permute-start = (bf16[512,128]{1,0:T(8,128)(2,1)}, bf16[512,128]{1,0:T(8,128)(2,1)S(1)}, u32[]{:S(2)}, u32[]{:S(2)}) collective-permute-start(bf16[512,128]{1,0:T(8,128)(2,1)} %get-tuple-element.18), channel_id=1, source_target_pairs={{0,16},{16,0},{1,17},{17,1},{2,18},{18,2},{3,19},{19,3},{4,20},{20... | collective-permute-start | bytes 393224 | tf_op jit(solution)/shard_map/ppermute | solution.py:300
  60.8 1.0 copy-start
  63.5 21.1 %all-to-all-start.2 = ((bf16[4,4,528,128]{3,2,1,0:T(8,128)(2,1)}), bf16[4,4,528,128]{3,2,1,0:T(8,128)(2,1)}, u32[]{:S(2)}, u32[]{:S(2)}) async-start(bf16[4,4,528,128]{3,2,1,0:T(8,128)(2,1)} %broadcast_in_dim.8), calls=%async_computation.2 | async-start | bytes 4325376 | tf_op jit(solution)/shard_map/all_to_all | solution.py:276
  93.9 51.0 %all-to-all-start.4 = ((bf16[4,4,512,128]{3,2,1,0:T(8,128)(2,1)}), bf16[4,4,512,128]{3,2,1,0:T(8,128)(2,1)}, u32[]{:S(2)}, u32[]{:S(2)}) async-start(bf16[4,4,512,128]{3,2,1,0:T(8,128)(2,1)} %get-tuple-element.24), calls=%async_computation.4 | async-start | bytes 4194304 | tf_op jit(solution)/shard_map/all_to_all | solution.py:276
  99.4 26.9 %copy-start.1 = (bf16[4,512,128]{2,1,0:T(8,128)(2,1)}, bf16[4,512,128]{2,1,0:T(8,128)(2,1)S(1)}, u32[]{:S(2)}) copy-start(bf16[4,512,128]{2,1,0:T(8,128)(2,1)S(1)} %slice.66.xs) | copy-start | bytes 1572868
  99.5 19.5 %collective-permute-start.1 = (bf16[4,512,128]{2,1,0:T(8,128)(2,1)S(1)}, bf16[4,512,128]{2,1,0:T(8,128)(2,1)S(1)}, u32[]{:S(2)}, u32[]{:S(2)}) collective-permute-start(bf16[4,512,128]{2,1,0:T(8,128)(2,1)S(1)} %slice.66.xs), channel_id=1, source_target_pairs={{0,1},{2,3},{8,9},{10,11},{1,0},{3,2},{9,8},{11,10},{4,5},{6,7},{1... | collective-permute-start | bytes 1572872 | tf_op jit(solution)/shard_map/ppermute | solution.py:296
  103.3 15.6 %collective-permute-start.2 = (bf16[4,512,128]{2,1,0:T(8,128)(2,1)S(1)}, bf16[4,512,128]{2,1,0:T(8,128)(2,1)S(1)}, u32[]{:S(2)}, u32[]{:S(2)}) collective-permute-start(bf16[4,512,128]{2,1,0:T(8,128)(2,1)S(1)} %slice.66.xs), channel_id=1, source_target_pairs={{0,4},{2,6},{8,12},{10,14},{1,5},{3,7},{9,13},{11,15},{4,0},{6,2},... | collective-permute-start | bytes 1572872 | tf_op jit(solution)/shard_map/ppermute | solution.py:296
  106.7 18.8 %collective-permute-start.3 = (bf16[4,512,128]{2,1,0:T(8,128)(2,1)S(1)}, bf16[4,512,128]{2,1,0:T(8,128)(2,1)S(1)}, u32[]{:S(2)}, u32[]{:S(2)}) collective-permute-start(bf16[4,512,128]{2,1,0:T(8,128)(2,1)S(1)} %slice.66.xs), channel_id=1, source_target_pairs={{0,5},{2,7},{8,13},{10,15},{1,4},{3,6},{9,12},{11,14},{4,1},{6,3},... | collective-permute-start | bytes 1572872 | tf_op jit(solution)/shard_map/ppermute | solution.py:296
  119.0 6.5 %copy-start.3 = (bf16[4,512,128]{2,1,0:T(8,128)(2,1)}, bf16[4,512,128]{2,1,0:T(8,128)(2,1)S(1)}, u32[]{:S(2)}) copy-start(bf16[4,512,128]{2,1,0:T(8,128)(2,1)S(1)} %collective-permute-done.1.refs_0_) | copy-start | bytes 1572868
  119.0 6.5 %copy-start.4 = (bf16[4,512,128]{2,1,0:T(8,128)(2,1)}, bf16[4,512,128]{2,1,0:T(8,128)(2,1)S(1)}, u32[]{:S(2)}) copy-start(bf16[4,512,128]{2,1,0:T(8,128)(2,1)S(1)} %collective-permute-done.2.refs_1_) | copy-start | bytes 1572868
  125.5 0.8 copy-start.5
  135.5 17.9 %copy-start.2 = (bf16[4,512,128]{2,1,0:T(8,128)(2,1)S(1)}, bf16[4,512,128]{2,1,0:T(8,128)(2,1)}, u32[]{:S(2)}) copy-start(bf16[4,512,128]{2,1,0:T(8,128)(2,1)} %get-tuple-element.20) | copy-start | bytes 1572868
  135.5 17.3 %collective-permute-start.6 = (bf16[4,512,128]{2,1,0:T(8,128)(2,1)}, bf16[4,512,128]{2,1,0:T(8,128)(2,1)S(1)}, u32[]{:S(2)}, u32[]{:S(2)}) collective-permute-start(bf16[4,512,128]{2,1,0:T(8,128)(2,1)} %get-tuple-element.23), channel_id=1, source_target_pairs={{0,5},{2,7},{8,13},{10,15},{1,4},{3,6},{9,12},{11,14},{4,1},{6,3},... | collective-permute-start | bytes 1572872 | tf_op jit(solution)/shard_map/ppermute | solution.py:296
  138.9 14.5 %collective-permute-start.5 = (bf16[4,512,128]{2,1,0:T(8,128)(2,1)}, bf16[4,512,128]{2,1,0:T(8,128)(2,1)S(1)}, u32[]{:S(2)}, u32[]{:S(2)}) collective-permute-start(bf16[4,512,128]{2,1,0:T(8,128)(2,1)} %get-tuple-element.22), channel_id=1, source_target_pairs={{0,4},{2,6},{8,12},{10,14},{1,5},{3,7},{9,13},{11,15},{4,0},{6,2},... | collective-permute-start | bytes 1572872 | tf_op jit(solution)/shard_map/ppermute | solution.py:296
  141.5 11.9 %collective-permute-start.4 = (bf16[4,512,128]{2,1,0:T(8,128)(2,1)}, bf16[4,512,128]{2,1,0:T(8,128)(2,1)S(1)}, u32[]{:S(2)}, u32[]{:S(2)}) collective-permute-start(bf16[4,512,128]{2,1,0:T(8,128)(2,1)} %get-tuple-element.21), channel_id=1, source_target_pairs={{0,1},{2,3},{8,9},{10,11},{1,0},{3,2},{9,8},{11,10},{4,5},{6,7},{1... | collective-permute-start | bytes 1572872 | tf_op jit(solution)/shard_map/ppermute | solution.py:296
  147.5 14.4 %all-to-all-start.5 = ((bf16[4,512,128]{2,1,0:T(8,128)(2,1)}), bf16[4,512,128]{2,1,0:T(8,128)(2,1)S(1)}, u32[]{:S(2)}, u32[]{:S(2)}) async-start(bf16[4,512,128]{2,1,0:T(8,128)(2,1)} %fusion), calls=%async_computation.5 | async-start | bytes 1048576 | tf_op jit(solution)/shard_map/all_to_all | solution.py:276
  154.5 53.2 %copy-start.6 = (bf16[128]{0:T(256)(128)(2,1)S(1)}, bf16[128]{0:T(256)(128)(2,1)}, u32[]{:S(2)}) copy-start(bf16[128]{0:T(256)(128)(2,1)} %param.15) | copy-start | bytes 772
  162.0 14.1 %all-to-all-start.3 = ((bf16[4,512,128]{2,1,0:T(8,128)(2,1)}), bf16[4,512,128]{2,1,0:T(8,128)(2,1)S(1)}, u32[]{:S(2)}, u32[]{:S(2)}) async-start(bf16[4,512,128]{2,1,0:T(8,128)(2,1)} %add_convert_fusion.1), calls=%async_computation.3 | async-start | bytes 1048576 | tf_op jit(solution)/shard_map/all_to_all | solution.py:276
  167.1 9.1 %collective-permute-start.7 = (bf16[512,128]{1,0:T(8,128)(2,1)S(1)}, bf16[512,128]{1,0:T(8,128)(2,1)S(1)}, u32[]{:S(2)}, u32[]{:S(2)}) collective-permute-start(bf16[512,128]{1,0:T(8,128)(2,1)S(1)} %fusion.1), channel_id=1, source_target_pairs={{0,16},{16,0},{1,17},{17,1},{2,18},{18,2},{3,19},{19,3},{4,20},{20... | collective-permute-start | bytes 393224 | tf_op jit(solution)/shard_map/ppermute | solution.py:300
  201.6 13.7 %all-to-all-start.7 = ((f32[16,1,256]{2,1,0:T(1,128)}), f32[16,1,256]{2,1,0:T(1,128)S(1)}, u32[]{:S(2)}, u32[]{:S(2)}) async-start(f32[16,1,256]{2,1,0:T(1,128)} %get-tuple-element.26), calls=%async_computation.7 | async-start | bytes 32768 | tf_op jit(solution)/shard_map/all_to_all | solution.py:276

commit v5 on v3

--- a/solution.py
+++ b/solution.py
@@ -61,20 +61,33 @@
     )(c, routes, weights, tokens)
 
 
-def expert_kernel(first, rows, core_ref, y_ref, x_ref, xs, wg, wu, wd, *refs):
+def expert_kernel(first, rows, core_ref, y_ref, x_ref, xs, *refs):
     if first:
-        out, gain_out = refs[:2]
+        wg, wu, wd, out, gain_out = refs[:5]
+        refs = refs[5:]
+        outs = [out.at[o] for o in range(4)]
     else:
-        gain_in, out = refs[:2]
-    raw, gain_s, xn, gu_s, d_s, stage, sems, osems = refs[2:]
+        more = refs[0:3]
+        wg, wu, wd, gain_in = refs[3:7]
+        outs = refs[7:11]
+        refs = refs[11:]
+    raw, gain_s, xn, gu_s, d_s, stage, sems, osems = refs
     core = core_ref[0]
-    at_inner = jnp.where(core == 0, x_ref[0], y_ref[0])
-
-    def block(outer, inner):
-        return jnp.where(core == 0, outer * 4 + inner, inner * 4 + outer)
-
-    def taken(outer, inner):
-        return block(outer, inner if first else jnp.bitwise_and(at_inner + inner, 3))
+    role = core if first else 1 - core
+    at_outer = jnp.where(role == 0, y_ref[0], x_ref[0])
+    at_inner = jnp.where(role == 0, x_ref[0], y_ref[0])
+
+    def block(o, i):
+        outer = o if first else jnp.bitwise_and(at_outer + o, 3)
+        return jnp.where(role == 0, outer * 4 + i, i * 4 + outer)
+
+    def taken(o, i):
+        return block(o, i if first else jnp.bitwise_and(at_inner + i, 3))
+
+    def source(o):
+        if first:
+            return xs.at[o]
+        return xs if o == 0 else more[o - 1]
 
     count = [0]
 
@@ -90,7 +103,7 @@
 
     def fetch_rows(at):
         return [
-            fetch(xs.at[o, i, pl.ds(at, half), :], raw.at[taken(o, i), pl.ds(at, half), :])
+            fetch(source(o).at[i, pl.ds(at, half), :], raw.at[taken(o, i), pl.ds(at, half), :])
             for o in range(4)
             for i in range(4)
         ]
@@ -98,7 +111,7 @@
     x_cp = [fetch_rows(0)]
     if first:
         gain_cp = [
-            fetch(xs.at[o, i, pl.ds(rows, GAIN_ROWS), :], gain_s.at[taken(o, i)])
+            fetch(source(o).at[i, pl.ds(rows, GAIN_ROWS), :], gain_s.at[block(o, i)])
             for o in range(4)
             for i in range(4)
         ]
@@ -127,8 +140,8 @@
         store(4, gain_s, gain_out)
     step = 32
 
-    def norm(i, _):
-        at = pl.multiple_of(i * step, step)
+    def norm(i):
+        at = i * step
         acc = jnp.zeros((step, 128), F32)
         vals = []
         for j in range(16):
@@ -139,18 +152,27 @@
         for j in range(16):
             gain = gain_s[j, 0:1, :].astype(F32)
             xn[pl.ds(at, step), j * 128 : (j + 1) * 128] = (vals[j] * scale * gain).astype(BF16)
-        return 0
 
     steps = half // step
-    for h in range(2):
-        for cp in x_cp[h]:
-            cp.wait()
-        lax.fori_loop(h * steps, (h + 1) * steps, norm, 0)
-    for cp in w_cp:
-        cp.wait()
-    both = jnp.dot(xn[...], gu_s[...], preferred_element_type=F32)
-    gate = both[:, :units]
-    hidden = (gate * both[:, units:] / (1.0 + jnp.exp(-gate))).astype(BF16)
+
+    def act(gate, up):
+        return (gate * up / (1.0 + jnp.exp(-gate))).astype(BF16)
+
+    for cp in x_cp[0]:
+        cp.wait()
+    for i in range(steps):
+        norm(i)
+    w_cp[0].wait()
+    gate = jnp.dot(xn[:half, :], gu_s[:, :units], preferred_element_type=F32)
+    w_cp[1].wait()
+    for cp in x_cp[1]:
+        cp.wait()
+    up = jnp.dot(xn[:half, :], gu_s[:, units:], preferred_element_type=F32)
+    low = act(gate, up)
+    for i in range(steps, 2 * steps):
+        norm(i)
+    both = jnp.dot(xn[half:, :], gu_s[...], preferred_element_type=F32)
+    hidden = jnp.concatenate([low, act(both[:, :units], both[:, units:])], axis=0)
     for cp in d_cp:
         cp.wait()
     for o in range(4):
@@ -159,7 +181,7 @@
         ).astype(BF16)
         for i in range(4):
             stage[o, i] = res[:, i * 128 : (i + 1) * 128]
-        store(o, stage.at[o], out.at[o])
+        store(o, stage.at[o], outs[o])
     for cp in copies:
         cp.wait()
 
@@ -168,12 +190,15 @@
     rows = 512
     width, units = weights[0].shape
     hbm = pl.BlockSpec(memory_space=pltpu.HBM)
-    args = (*place, xs, *weights)
-    outs = (jax.ShapeDtypeStruct((4, 4, rows, 128), BF16),)
     if first:
-        outs = (*outs, jax.ShapeDtypeStruct((16, GAIN_ROWS, 128), BF16))
+        args = (*place, xs, *weights)
+        outs = (
+            jax.ShapeDtypeStruct((4, 4, rows, 128), BF16),
+            jax.ShapeDtypeStruct((16, GAIN_ROWS, 128), BF16),
+        )
     else:
-        args = (*args, gain)
+        args = (*place, *xs, *weights, gain)
+        outs = tuple([jax.ShapeDtypeStruct((4, rows, 128), BF16)] * 4)
     return pl.pallas_call(
         functools.partial(expert_kernel, first, rows),
         out_shape=outs,
@@ -190,7 +215,7 @@
             pltpu.SemaphoreType.DMA((5,)),
         ],
         compiler_params=pltpu.CompilerParams(vmem_limit_bytes=63 * 1024 * 1024),
-        name="expert_near" if first else "expert_far",
+        name="expert_far" if first else "expert_near",
     )(*args)
 
 
@@ -252,21 +277,18 @@
     )
 
 
-def inner_exchange(v):
-    return exchange(v, ALL, lines(0))
-
-
-def outer_exchange(v):
-    return exchange(v, ALL, lines(1))
-
-
-def inner_ahead(v, step):
+def across(v, along_x_for):
+    return exchange(v, ALL, lines(along_x_for))
+
+
+def ahead(v, along_x_for, step):
     pairs = []
     for z in range(16):
-        for y in range(4):
-            for x in range(4):
-                pairs.append((flat(z, 0, y, (x + step) % 4), flat(z, 0, y, x)))
-                pairs.append((flat(z, 1, (y + step) % 4, x), flat(z, 1, y, x)))
+        for c in range(2):
+            for y in range(4):
+                for x in range(4):
+                    to_y, to_x = (y, x + step) if c == along_x_for else (y + step, x)
+                    pairs.append((flat(z, c, y, x), flat(z, c, to_y % 4, to_x % 4)))
     return lax.ppermute(v, ALL, pairs)
 
 
@@ -285,7 +307,7 @@
     return total_of([v[i] for i in range(v.shape[0])])
 
 
-def copies(v):
+def copies_of(v):
     return jnp.broadcast_to(v[None], (4, *v.shape))
 
 
@@ -297,19 +319,19 @@
     weights = (w_gate[0], w_up[0], w_down[0])
     both = exchange(rows.reshape(16, 2, -1, share), "z")
     near, far = (both[:, i].reshape(-1, share) for i in range(2))
+    far = swap(far)
     gain_rows = jnp.broadcast_to(norm_gain[None, :], (GAIN_ROWS, share))
-    near = inner_exchange(copies(jnp.concatenate([near, gain_rows], axis=0)))
-    far = swap(far)
-    near = outer_exchange(copies(near))
-    far = jnp.stack([far] + [inner_ahead(far, s) for s in (1, 2, 3)])
-    far = outer_exchange(copies(far))
-    near, gain = expert(True, place, near, weights, None)
-    near = summed(outer_exchange(near))
-    far = expert(False, place, far, weights, gain)[0]
-    far = summed(outer_exchange(far))
-    last = summed(inner_exchange(jnp.concatenate([near, far], axis=1)))
-    near = last[: near.shape[1]]
-    far = swap(last[near.shape[0] :])
+    far = across(copies_of(jnp.concatenate([far, gain_rows], axis=0)), 0)
+    near = jnp.stack([near] + [ahead(near, 1, -s) for s in (1, 2, 3)])
+    far = across(copies_of(far), 1)
+    near = [near] + [ahead(near, 0, -s) for s in (1, 2, 3)]
+    far, gain = expert(True, place, far, weights, None)
+    far = summed(across(far, 1))
+    near = expert(False, place, near, weights, gain)
+    two = ahead(near[2], 0, 2)
+    near = total_of([near[0], two, ahead(near[1], 0, 1), ahead(near[3], 0, 3)])
+    far = swap(summed(across(far, 0)))
+    near = summed(across(near, 1))
     both = jnp.stack([near.reshape(16, -1, share), far.reshape(16, -1, share)], axis=1)
     combined, squares = combine(table, exchange(both, "z").reshape(-1, share))
     total = exchange(squares, ("y", "x")).sum(axis=(0, 1))

time: 205 us -> 210 us (1.024)
  blocking collectives: 104 us -> 66 us
  starting transfers between devices: 28.2 us -> 55.4 us
  waiting for transfers between devices: 39.9 us -> 59.3 us
  Pallas kernels: 22.7 us -> 19.5 us
    all_to_all x5 -> x3, blocking collectives: 104 us -> 66 us  [exchange(): lax.all_to_all(v, axis, split_axis=0, concat_axis=0, tiled=True, axis_ind...]
    ppermute x3 -> x9, starting transfers between devices: 8.36 us -> 29.5 us  [ahead(): return lax.ppermute(v, ALL, pairs)]
    ppermute x3 -> x9, waiting for transfers between devices: 6.14 us -> 25.7 us  [ahead(): return lax.ppermute(v, ALL, pairs)]
    all_to_all x4 -> x5, starting transfers between devices: 16 us -> 22 us  [exchange(): lax.all_to_all(v, axis, split_axis=0, concat_axis=0, tiled=True, axis_ind...]
    pallas_call x2, Pallas kernels: 18.4 us -> 15.2 us  [expert(): pl.pallas_call(functools.partial(expert_kernel, first, rows), out_shape=o...]
    all_to_all x4 -> x5, waiting for transfers between devices: 31.2 us -> 32.3 us  [exchange(): lax.all_to_all(v, axis, split_axis=0, concat_axis=0, tiled=True, axis_ind...]
  transfers between devices with their start and end apart: 9 -> 16, of which waited for: 8 -> 11; matrix products, arithmetic and copies ran while one was open for 1% -> 2% of each run, Pallas kernels for 5% -> 4%
where the time goes in v5:
time: 210 us; the launch traced here: 209 us
  blocking collectives  66 us (31%)
  waiting for transfers between devices  59.3 us (28%)
  starting transfers between devices  55.4 us (26%)
  Pallas kernels  19.5 us (9%)
  other arithmetic  5.61 us (3%)
  local copies, waits for them, and re-layouts  3.26 us (2%)
    all_to_all x3, blocking collectives, exchange(): lax.all_to_all(v, axis, split_axis=0, concat_axis=0, tiled=True, axis_ind...  66 us
    all_to_all x5, waiting for transfers between devices, exchange(): lax.all_to_all(v, axis, split_axis=0, concat_axis=0, tiled=True, axis_ind...  32.3 us
    ppermute x9, starting transfers between devices, ahead(): return lax.ppermute(v, ALL, pairs)  29.5 us
    ppermute x9, waiting for transfers between devices, ahead(): return lax.ppermute(v, ALL, pairs)  25.7 us
    all_to_all x5, starting transfers between devices, exchange(): lax.all_to_all(v, axis, split_axis=0, concat_axis=0, tiled=True, axis_ind...  22 us
    pallas_call x2, Pallas kernels, expert(): pl.pallas_call(functools.partial(expert_kernel, first, rows), out_shape=o...  15.2 us
  transfers between devices with their start and end apart: 16, of which 11 were waited for; matrix products, arithmetic and copies ran while one was open for 2% of the time, Pallas kernels for 4%

profile of v5, /device:TPU:32, one launch (start us, length us, event | category | flops | bytes accessed | tf_op | source)
XLA Modules:
  0.0 209.3 jit_solution(6515180039287196200)
XLA Ops:
  0.0 2.1 pack.1
  2.1 33.1 %all_to_all.40 = bf16[16,2,32,128]{3,2,1,0:T(8,128)(2,1)S(1)} all-to-all(bf16[16,2,32,128]{3,2,1,0:T(8,128)(2,1)} %bitcast.38), channel_id=1, replica_groups=mesh['z'=16,'c'=2,'y'=4,'x'=4] {'z'}, dimensions={0} | all-to-all | bytes 524288 | tf_op jit(solution)/shard_map/all_to_all | solution.py:275
  35.2 1.9 collective-permute-start.6
  39.2 12.3 %all_to_all.41 = bf16[4,528,128]{2,1,0:T(8,128)(2,1)S(1)} all-to-all(bf16[4,528,128]{2,1,0:T(8,128)(2,1)S(1)} %broadcast_in_dim.7), channel_id=1, replica_groups={{0,1,2,3},{4,5,6,7},{8,9,10,11},{12,13,14,15},{16,20,24,28},{17,21,25,2..., dimensions={0} | all-to-all | bytes 1081344 | tf_op jit(solution)/shard_map/all_to_all | solution.py:275
  53.2 4.5 %all-to-all-start.2 = ((bf16[4,4,528,128]{3,2,1,0:T(8,128)(2,1)}), bf16[4,4,528,128]{3,2,1,0:T(8,128)(2,1)}, u32[]{:S(2)}, u32[]{:S(2)}) async-start(bf16[4,4,528,128]{3,2,1,0:T(8,128)(2,1)} %broadcast_in_dim.8), calls=%async_computation.2 | async-start | bytes 4325376 | tf_op jit(solution)/shard_map/all_to_all | solution.py:275
  57.6 16.9 %all-to-all-done.2.xs = bf16[4,4,528,128]{3,2,1,0:T(8,128)(2,1)} async-done(((bf16[4,4,528,128]{3,2,1,0:T(8,128)(2,1)}), bf16[4,4,528,128]{3,2,1,0:T(8,128)(2,1)}, u32[]{:S(2)}, u32[]{:S(2)}) %all-to-all-start.2) | async-done | bytes 2162720 | tf_op jit(solution)/shard_map/all_to_all | solution.py:275
  74.6 7.6 %expert_far.1 = (bf16[4,4,512,128]{3,2,1,0:T(8,128)(2,1)}, bf16[16,16,128]{2,1,0:T(8,128)(2,1)}) custom-call(s32[1]{0:T(128)} %bitcast.pos.core_ref, s32[1]{0:T(128)} %bitcast.3.y_ref, s32[1]{0:T(128)} %bitcast.4.x_ref, bf16[4,4,528,128]{3,2,1,0:T(8,128)(2,1)} %all-to-all-done.2.xs, bf16[2048,384]{1,0:T(8,128)(2,1)} %bitcast.26, bf16[2048,384]{1,0:T(8,128)(2,1)} %bitcast.28, ...), custom_call_target="tpu_custom_call" | custom-call | tf_op jit(solution)/shard_map/expert_far/pallas_call | solution.py:202
  82.2 4.5 %all-to-all-start.4 = ((bf16[4,4,512,128]{3,2,1,0:T(8,128)(2,1)}), bf16[4,4,512,128]{3,2,1,0:T(8,128)(2,1)}, u32[]{:S(2)}, u32[]{:S(2)}) async-start(bf16[4,4,512,128]{3,2,1,0:T(8,128)(2,1)} %get-tuple-element.22), calls=%async_computation.4 | async-start | bytes 4194304 | tf_op jit(solution)/shard_map/all_to_all | solution.py:275
  86.7 3.9 %collective-permute-start.2 = (bf16[512,128]{1,0:T(8,128)(2,1)S(1)}, bf16[512,128]{1,0:T(8,128)(2,1)S(1)}, u32[]{:S(2)}, u32[]{:S(2)}) collective-permute-start(bf16[512,128]{1,0:T(8,128)(2,1)S(1)} %bitcast.34), channel_id=1, source_target_pairs={{0,4},{1,5},{2,6},{3,7},{4,8},{5,9},{6,10},{7,11},{8,12},{9,13},{1... | collective-permute-start | bytes 393224 | tf_op jit(solution)/shard_map/ppermute | solution.py:292
  90.5 4.6 %collective-permute-start.1 = (bf16[512,128]{1,0:T(8,128)(2,1)S(1)}, bf16[512,128]{1,0:T(8,128)(2,1)S(1)}, u32[]{:S(2)}, u32[]{:S(2)}) collective-permute-start(bf16[512,128]{1,0:T(8,128)(2,1)S(1)} %bitcast.35), channel_id=1, source_target_pairs={{0,8},{1,9},{2,10},{3,11},{4,12},{5,13},{6,14},{7,15},{8,0},{9,1},... | collective-permute-start | bytes 393224 | tf_op jit(solution)/shard_map/ppermute | solution.py:292
  95.1 3.4 %collective-permute-start = (bf16[512,128]{1,0:T(8,128)(2,1)S(1)}, bf16[512,128]{1,0:T(8,128)(2,1)S(1)}, u32[]{:S(2)}, u32[]{:S(2)}) collective-permute-start(bf16[512,128]{1,0:T(8,128)(2,1)S(1)} %bitcast.36), channel_id=1, source_target_pairs={{0,12},{1,13},{2,14},{3,15},{4,0},{5,1},{6,2},{7,3},{8,4},{9,5},{1... | collective-permute-start | bytes 393224 | tf_op jit(solution)/shard_map/ppermute | solution.py:292
  98.5 5.7 %collective-permute-done.2 = bf16[512,128]{1,0:T(8,128)(2,1)S(1)} collective-permute-done((bf16[512,128]{1,0:T(8,128)(2,1)S(1)}, bf16[512,128]{1,0:T(8,128)(2,1)S(1)}, u32[]{:S(2)}, u32[]{:S(2)}) %collective-permute-start.2) | collective-permute-done | bytes 131104 | tf_op jit(solution)/shard_map/ppermute | solution.py:292
  106.1 3.1 %collective-permute-start.3 = (bf16[4,512,128]{2,1,0:T(8,128)(2,1)S(1)}, bf16[4,512,128]{2,1,0:T(8,128)(2,1)S(1)}, u32[]{:S(2)}, u32[]{:S(2)}) collective-permute-start(bf16[4,512,128]{2,1,0:T(8,128)(2,1)S(1)} %pad_maximum_fusion.xs), channel_id=1, source_target_pairs={{0,3},{1,0},{2,1},{3,2},{4,7},{5,4},{6,5},{7,6},{8,11},{9,8},{10,9... | collective-permute-start | bytes 1572872 | tf_op jit(solution)/shard_map/ppermute | solution.py:292
  109.2 3.4 %collective-permute-start.4 = (bf16[4,512,128]{2,1,0:T(8,128)(2,1)S(1)}, bf16[4,512,128]{2,1,0:T(8,128)(2,1)S(1)}, u32[]{:S(2)}, u32[]{:S(2)}) collective-permute-start(bf16[4,512,128]{2,1,0:T(8,128)(2,1)S(1)} %pad_maximum_fusion.xs), channel_id=1, source_target_pairs={{0,2},{1,3},{2,0},{3,1},{4,6},{5,7},{6,4},{7,5},{8,10},{9,11},{10,... | collective-permute-start | bytes 1572872 | tf_op jit(solution)/shard_map/ppermute | solution.py:292
  112.5 1.9 collective-permute-start.5
  114.5 2.7 %collective-permute-done.3.refs_0_ = bf16[4,512,128]{2,1,0:T(8,128)(2,1)S(1)} collective-permute-done((bf16[4,512,128]{2,1,0:T(8,128)(2,1)S(1)}, bf16[4,512,128]{2,1,0:T(8,128)(2,1)S(1)}, u32[]{:S(2)}, u32[]{:S(2)}) %collective-permute-start.3) | collective-permute-done | bytes 524320 | tf_op jit(solution)/shard_map/ppermute | solution.py:292
  117.1 4.7 %collective-permute-done.4.refs_1_ = bf16[4,512,128]{2,1,0:T(8,128)(2,1)S(1)} collective-permute-done((bf16[4,512,128]{2,1,0:T(8,128)(2,1)S(1)}, bf16[4,512,128]{2,1,0:T(8,128)(2,1)S(1)}, u32[]{:S(2)}, u32[]{:S(2)}) %collective-permute-start.4) | collective-permute-done | bytes 524320 | tf_op jit(solution)/shard_map/ppermute | solution.py:292
  121.8 5.5 %collective-permute-done.5.refs_2_ = bf16[4,512,128]{2,1,0:T(8,128)(2,1)S(1)} collective-permute-done((bf16[4,512,128]{2,1,0:T(8,128)(2,1)S(1)}, bf16[4,512,128]{2,1,0:T(8,128)(2,1)S(1)}, u32[]{:S(2)}, u32[]{:S(2)}) %collective-permute-start.5) | collective-permute-done | bytes 524320 | tf_op jit(solution)/shard_map/ppermute | solution.py:292
  128.2 7.6 %expert_near.1 = (bf16[4,512,128]{2,1,0:T(8,128)(2,1)}, bf16[4,512,128]{2,1,0:T(8,128)(2,1)}, bf16[4,512,128]{2,1,0:T(8,128)(2,1)}, bf16[4,512,128]{2,1,0:T(8,128)(2,1)}) custom-call(s32[1]{0:T(128)} %bitcast.pos.core_ref, s32[1]{0:T(128)} %bitcast.3.y_ref, s32[1]{0:T(128)} %bitcast.4.x_ref, bf16[4,512,128]{2,1,0:T(8,128)(2,1)} %copy-done, ...), custom_call_target="tpu_custom_call" | custom-call | tf_op jit(solution)/shard_map/expert_near/pallas_call | solution.py:202
  135.8 2.6 %collective-permute-start.9 = (bf16[4,512,128]{2,1,0:T(8,128)(2,1)}, bf16[4,512,128]{2,1,0:T(8,128)(2,1)S(1)}, u32[]{:S(2)}, u32[]{:S(2)}) collective-permute-start(bf16[4,512,128]{2,1,0:T(8,128)(2,1)} %get-tuple-element.21), channel_id=1, source_target_pairs={{0,3},{1,0},{2,1},{3,2},{4,7},{5,4},{6,5},{7,6},{8,11},{9,8},{10,9... | collective-permute-start | bytes 1572872 | tf_op jit(solution)/shard_map/ppermute | solution.py:292
  138.4 3.3 %collective-permute-start.8 = (bf16[4,512,128]{2,1,0:T(8,128)(2,1)}, bf16[4,512,128]{2,1,0:T(8,128)(2,1)S(1)}, u32[]{:S(2)}, u32[]{:S(2)}) collective-permute-start(bf16[4,512,128]{2,1,0:T(8,128)(2,1)} %get-tuple-element.20), channel_id=1, source_target_pairs={{0,1},{1,2},{2,3},{3,0},{4,5},{5,6},{6,7},{7,4},{8,9},{9,10},{10,1... | collective-permute-start | bytes 1572872 | tf_op jit(solution)/shard_map/ppermute | solution.py:292
  141.8 3.4 %collective-permute-start.7 = (bf16[4,512,128]{2,1,0:T(8,128)(2,1)}, bf16[4,512,128]{2,1,0:T(8,128)(2,1)S(1)}, u32[]{:S(2)}, u32[]{:S(2)}) collective-permute-start(bf16[4,512,128]{2,1,0:T(8,128)(2,1)} %get-tuple-element.19), channel_id=1, source_target_pairs={{0,2},{1,3},{2,0},{3,1},{4,6},{5,7},{6,4},{7,5},{8,10},{9,11},{10,... | collective-permute-start | bytes 1572872 | tf_op jit(solution)/shard_map/ppermute | solution.py:292
  145.2 2.6 %fusion = bf16[4,512,128]{2,1,0:T(8,128)(2,1)} fusion(bf16[4,4,512,128]{3,2,1,0:T(8,128)(2,1)} %all-to-all-done.4), kind=kLoop, calls=%fused_computation.2 | loop fusion | flops 2097152 | bytes 2621440 | tf_op jit(solution)/shard_map/add | solution.py:302
  147.8 3.5 %all-to-all-start.5 = ((bf16[4,512,128]{2,1,0:T(8,128)(2,1)}), bf16[4,512,128]{2,1,0:T(8,128)(2,1)S(1)}, u32[]{:S(2)}, u32[]{:S(2)}) async-start(bf16[4,512,128]{2,1,0:T(8,128)(2,1)} %fusion), calls=%async_computation.5 | async-start | bytes 1048576 | tf_op jit(solution)/shard_map/all_to_all | solution.py:275
  151.3 5.3 %collective-permute-done.8 = bf16[4,512,128]{2,1,0:T(8,128)(2,1)S(1)} collective-permute-done((bf16[4,512,128]{2,1,0:T(8,128)(2,1)}, bf16[4,512,128]{2,1,0:T(8,128)(2,1)S(1)}, u32[]{:S(2)}, u32[]{:S(2)}) %collective-permute-start.8) | collective-permute-done | bytes 524320 | tf_op jit(solution)/shard_map/ppermute | solution.py:292
  159.4 3.5 %all-to-all-start.3 = ((bf16[4,512,128]{2,1,0:T(8,128)(2,1)}), bf16[4,512,128]{2,1,0:T(8,128)(2,1)S(1)}, u32[]{:S(2)}, u32[]{:S(2)}) async-start(bf16[4,512,128]{2,1,0:T(8,128)(2,1)} %add_convert_fusion.1), calls=%async_computation.3 | async-start | bytes 1048576 | tf_op jit(solution)/shard_map/all_to_all | solution.py:275
  162.9 1.9 collective-permute-start.10
  164.8 6.0 %all-to-all-done.3 = bf16[4,512,128]{2,1,0:T(8,128)(2,1)S(1)} async-done(((bf16[4,512,128]{2,1,0:T(8,128)(2,1)}), bf16[4,512,128]{2,1,0:T(8,128)(2,1)S(1)}, u32[]{:S(2)}, u32[]{:S(2)}) %all-to-all-start.3) | async-done | bytes 524320 | tf_op jit(solution)/shard_map/all_to_all | solution.py:275
  171.0 20.7 %all_to_all.42 = bf16[16,2,32,128]{3,2,1,0:T(8,128)(2,1)} all-to-all(bf16[16,2,32,128]{3,2,1,0:T(8,128)(2,1)S(1)} %pad_maximum_fusion.1), channel_id=1, replica_groups=mesh['z'=16,'c'=2,'y'=4,'x'=4] {'z'}, dimensions={0} | all-to-all | bytes 524288 | tf_op jit(solution)/shard_map/all_to_all | solution.py:275
  191.7 2.2 %combine.1 = (f32[256,128]{1,0:T(8,128)}, f32[16,1,256]{2,1,0:T(1,128)}) custom-call(f32[256,8]{1,0:T(8,128)} %get-tuple-element.15.table, bf16[1024,128]{1,0:T(8,128)(2,1)} %bitcast.32), custom_call_target="tpu_custom_call" | custom-call | tf_op jit(solution)/shard_map/combine/pallas_call | solution.py:243
  193.9 6.1 %all-to-all-start.7 = ((f32[16,1,256]{2,1,0:T(1,128)}), f32[16,1,256]{2,1,0:T(1,128)S(1)}, u32[]{:S(2)}, u32[]{:S(2)}) async-start(f32[16,1,256]{2,1,0:T(1,128)} %get-tuple-element.24), calls=%async_computation.7 | async-start | bytes 32768 | tf_op jit(solution)/shard_map/all_to_all | solution.py:275
  200.0 7.6 %all-to-all-done.7 = f32[16,1,256]{2,1,0:T(1,128)S(1)} async-done(((f32[16,1,256]{2,1,0:T(1,128)}), f32[16,1,256]{2,1,0:T(1,128)S(1)}, u32[]{:S(2)}, u32[]{:S(2)}) %all-to-all-start.7) | async-done | bytes 16416 | tf_op jit(solution)/shard_map/all_to_all | solution.py:275
  (34 shorter events, 11.1 us)
Async XLA Ops:
  35.2 3.2 %collective-permute-start.6 = (bf16[512,128]{1,0:T(8,128)(2,1)S(1)}, bf16[512,128]{1,0:T(8,128)(2,1)S(1)}, u32[]{:S(2)}, u32[]{:S(2)}) collective-permute-start(bf16[512,128]{1,0:T(8,128)(2,1)S(1)} %bitcast.40), channel_id=1, source_target_pairs={{0,16},{16,0},{1,17},{17,1},{2,18},{18,2},{3,19},{19,3},{4,20},{20... | collective-permute-start | bytes 393224 | tf_op jit(solution)/shard_map/ppermute | solution.py:296
  53.2 21.4 %all-to-all-start.2 = ((bf16[4,4,528,128]{3,2,1,0:T(8,128)(2,1)}), bf16[4,4,528,128]{3,2,1,0:T(8,128)(2,1)}, u32[]{:S(2)}, u32[]{:S(2)}) async-start(bf16[4,4,528,128]{3,2,1,0:T(8,128)(2,1)} %broadcast_in_dim.8), calls=%async_computation.2 | async-start | bytes 4325376 | tf_op jit(solution)/shard_map/all_to_all | solution.py:275
  82.2 63.0 %all-to-all-start.4 = ((bf16[4,4,512,128]{3,2,1,0:T(8,128)(2,1)}), bf16[4,4,512,128]{3,2,1,0:T(8,128)(2,1)}, u32[]{:S(2)}, u32[]{:S(2)}) async-start(bf16[4,4,512,128]{3,2,1,0:T(8,128)(2,1)} %get-tuple-element.22), calls=%async_computation.4 | async-start | bytes 4194304 | tf_op jit(solution)/shard_map/all_to_all | solution.py:275
  86.7 17.6 %collective-permute-start.2 = (bf16[512,128]{1,0:T(8,128)(2,1)S(1)}, bf16[512,128]{1,0:T(8,128)(2,1)S(1)}, u32[]{:S(2)}, u32[]{:S(2)}) collective-permute-start(bf16[512,128]{1,0:T(8,128)(2,1)S(1)} %bitcast.34), channel_id=1, source_target_pairs={{0,4},{1,5},{2,6},{3,7},{4,8},{5,9},{6,10},{7,11},{8,12},{9,13},{1... | collective-permute-start | bytes 393224 | tf_op jit(solution)/shard_map/ppermute | solution.py:292
  90.5 15.4 %collective-permute-start.1 = (bf16[512,128]{1,0:T(8,128)(2,1)S(1)}, bf16[512,128]{1,0:T(8,128)(2,1)S(1)}, u32[]{:S(2)}, u32[]{:S(2)}) collective-permute-start(bf16[512,128]{1,0:T(8,128)(2,1)S(1)} %bitcast.35), channel_id=1, source_target_pairs={{0,8},{1,9},{2,10},{3,11},{4,12},{5,13},{6,14},{7,15},{8,0},{9,1},... | collective-permute-start | bytes 393224 | tf_op jit(solution)/shard_map/ppermute | solution.py:292
  95.1 10.8 %collective-permute-start = (bf16[512,128]{1,0:T(8,128)(2,1)S(1)}, bf16[512,128]{1,0:T(8,128)(2,1)S(1)}, u32[]{:S(2)}, u32[]{:S(2)}) collective-permute-start(bf16[512,128]{1,0:T(8,128)(2,1)S(1)} %bitcast.36), channel_id=1, source_target_pairs={{0,12},{1,13},{2,14},{3,15},{4,0},{5,1},{6,2},{7,3},{8,4},{9,5},{1... | collective-permute-start | bytes 393224 | tf_op jit(solution)/shard_map/ppermute | solution.py:292
  106.1 22.1 %copy-start = (bf16[4,512,128]{2,1,0:T(8,128)(2,1)}, bf16[4,512,128]{2,1,0:T(8,128)(2,1)S(1)}, u32[]{:S(2)}) copy-start(bf16[4,512,128]{2,1,0:T(8,128)(2,1)S(1)} %pad_maximum_fusion.xs) | copy-start | bytes 1572868
  106.1 11.1 %collective-permute-start.3 = (bf16[4,512,128]{2,1,0:T(8,128)(2,1)S(1)}, bf16[4,512,128]{2,1,0:T(8,128)(2,1)S(1)}, u32[]{:S(2)}, u32[]{:S(2)}) collective-permute-start(bf16[4,512,128]{2,1,0:T(8,128)(2,1)S(1)} %pad_maximum_fusion.xs), channel_id=1, source_target_pairs={{0,3},{1,0},{2,1},{3,2},{4,7},{5,4},{6,5},{7,6},{8,11},{9,8},{10,9... | collective-permute-start | bytes 1572872 | tf_op jit(solution)/shard_map/ppermute | solution.py:292
  109.2 12.7 %collective-permute-start.4 = (bf16[4,512,128]{2,1,0:T(8,128)(2,1)S(1)}, bf16[4,512,128]{2,1,0:T(8,128)(2,1)S(1)}, u32[]{:S(2)}, u32[]{:S(2)}) collective-permute-start(bf16[4,512,128]{2,1,0:T(8,128)(2,1)S(1)} %pad_maximum_fusion.xs), channel_id=1, source_target_pairs={{0,2},{1,3},{2,0},{3,1},{4,6},{5,7},{6,4},{7,5},{8,10},{9,11},{10,... | collective-permute-start | bytes 1572872 | tf_op jit(solution)/shard_map/ppermute | solution.py:292
  112.5 14.8 %collective-permute-start.5 = (bf16[4,512,128]{2,1,0:T(8,128)(2,1)S(1)}, bf16[4,512,128]{2,1,0:T(8,128)(2,1)S(1)}, u32[]{:S(2)}, u32[]{:S(2)}) collective-permute-start(bf16[4,512,128]{2,1,0:T(8,128)(2,1)S(1)} %pad_maximum_fusion.xs), channel_id=1, source_target_pairs={{0,1},{1,2},{2,3},{3,0},{4,5},{5,6},{6,7},{7,4},{8,9},{9,10},{10,1... | collective-permute-start | bytes 1572872 | tf_op jit(solution)/shard_map/ppermute | solution.py:292
  117.1 10.2 %copy-start.2 = (bf16[4,512,128]{2,1,0:T(8,128)(2,1)}, bf16[4,512,128]{2,1,0:T(8,128)(2,1)S(1)}, u32[]{:S(2)}) copy-start(bf16[4,512,128]{2,1,0:T(8,128)(2,1)S(1)} %collective-permute-done.3.refs_0_) | copy-start | bytes 1572868
  121.8 5.5 %copy-start.3 = (bf16[4,512,128]{2,1,0:T(8,128)(2,1)}, bf16[4,512,128]{2,1,0:T(8,128)(2,1)S(1)}, u32[]{:S(2)}) copy-start(bf16[4,512,128]{2,1,0:T(8,128)(2,1)S(1)} %collective-permute-done.4.refs_1_) | copy-start | bytes 1572868
  127.4 0.8 copy-start.4
  135.8 20.8 %copy-start.1 = (bf16[4,512,128]{2,1,0:T(8,128)(2,1)S(1)}, bf16[4,512,128]{2,1,0:T(8,128)(2,1)}, u32[]{:S(2)}) copy-start(bf16[4,512,128]{2,1,0:T(8,128)(2,1)} %get-tuple-element.18) | copy-start | bytes 1572868
  135.8 15.5 %collective-permute-start.9 = (bf16[4,512,128]{2,1,0:T(8,128)(2,1)}, bf16[4,512,128]{2,1,0:T(8,128)(2,1)S(1)}, u32[]{:S(2)}, u32[]{:S(2)}) collective-permute-start(bf16[4,512,128]{2,1,0:T(8,128)(2,1)} %get-tuple-element.21), channel_id=1, source_target_pairs={{0,3},{1,0},{2,1},{3,2},{4,7},{5,4},{6,5},{7,6},{8,11},{9,8},{10,9... | collective-permute-start | bytes 1572872 | tf_op jit(solution)/shard_map/ppermute | solution.py:292
  138.4 18.1 %collective-permute-start.8 = (bf16[4,512,128]{2,1,0:T(8,128)(2,1)}, bf16[4,512,128]{2,1,0:T(8,128)(2,1)S(1)}, u32[]{:S(2)}, u32[]{:S(2)}) collective-permute-start(bf16[4,512,128]{2,1,0:T(8,128)(2,1)} %get-tuple-element.20), channel_id=1, source_target_pairs={{0,1},{1,2},{2,3},{3,0},{4,5},{5,6},{6,7},{7,4},{8,9},{9,10},{10,1... | collective-permute-start | bytes 1572872 | tf_op jit(solution)/shard_map/ppermute | solution.py:292
  141.8 14.8 %collective-permute-start.7 = (bf16[4,512,128]{2,1,0:T(8,128)(2,1)}, bf16[4,512,128]{2,1,0:T(8,128)(2,1)S(1)}, u32[]{:S(2)}, u32[]{:S(2)}) collective-permute-start(bf16[4,512,128]{2,1,0:T(8,128)(2,1)} %get-tuple-element.19), channel_id=1, source_target_pairs={{0,2},{1,3},{2,0},{3,1},{4,6},{5,7},{6,4},{7,5},{8,10},{9,11},{10,... | collective-permute-start | bytes 1572872 | tf_op jit(solution)/shard_map/ppermute | solution.py:292
  147.8 11.6 %all-to-all-start.5 = ((bf16[4,512,128]{2,1,0:T(8,128)(2,1)}), bf16[4,512,128]{2,1,0:T(8,128)(2,1)S(1)}, u32[]{:S(2)}, u32[]{:S(2)}) async-start(bf16[4,512,128]{2,1,0:T(8,128)(2,1)} %fusion), calls=%async_computation.5 | async-start | bytes 1048576 | tf_op jit(solution)/shard_map/all_to_all | solution.py:275
  157.6 42.4 %copy-start.5 = (bf16[128]{0:T(256)(128)(2,1)S(1)}, bf16[128]{0:T(256)(128)(2,1)}, u32[]{:S(2)}) copy-start(bf16[128]{0:T(256)(128)(2,1)} %param.15) | copy-start | bytes 772
  159.4 11.5 %all-to-all-start.3 = ((bf16[4,512,128]{2,1,0:T(8,128)(2,1)}), bf16[4,512,128]{2,1,0:T(8,128)(2,1)S(1)}, u32[]{:S(2)}, u32[]{:S(2)}) async-start(bf16[4,512,128]{2,1,0:T(8,128)(2,1)} %add_convert_fusion.1), calls=%async_computation.3 | async-start | bytes 1048576 | tf_op jit(solution)/shard_map/all_to_all | solution.py:275
  162.9 8.0 %collective-permute-start.10 = (bf16[512,128]{1,0:T(8,128)(2,1)S(1)}, bf16[512,128]{1,0:T(8,128)(2,1)S(1)}, u32[]{:S(2)}, u32[]{:S(2)}) collective-permute-start(bf16[512,128]{1,0:T(8,128)(2,1)S(1)} %fusion.1), channel_id=1, source_target_pairs={{0,16},{16,0},{1,17},{17,1},{2,18},{18,2},{3,19},{19,3},{4,20},{20... | collective-permute-start | bytes 393224 | tf_op jit(solution)/shard_map/ppermute | solution.py:296
  193.9 13.7 %all-to-all-start.7 = ((f32[16,1,256]{2,1,0:T(1,128)}), f32[16,1,256]{2,1,0:T(1,128)S(1)}, u32[]{:S(2)}, u32[]{:S(2)}) async-start(f32[16,1,256]{2,1,0:T(1,128)} %get-tuple-element.24), calls=%async_computation.7 | async-start | bytes 32768 | tf_op jit(solution)/shard_map/all_to_all | solution.py:275

commit v6 on v5

--- a/solution.py
+++ b/solution.py
@@ -14,16 +14,16 @@
 GAIN_ROWS = 16
 
 
-def pack_kernel(pos, routes, weights, tokens, out, table):
+def pack_kernel(pos, routes, weights, tokens, near, far, table):
     tok = tokens.shape[0]
-    count = out.shape[0]
+    half = near.shape[0]
     experts = 2 * lax.axis_size("z")
-    cap = count // experts
+    cap = half // (experts // 2)
     e0 = routes[0:1, :]
     e1 = routes[1:2, :]
-    names = lax.broadcasted_iota(jnp.int32, (experts, tok), 0)
-    hot0 = names == e0
-    hot1 = names == e1
+    lanes = lax.broadcasted_iota(jnp.int32, (experts, tok), 0)
+    hot0 = lanes == e0
+    hot1 = lanes == e1
     hot = (hot0 | hot1).astype(F32).astype(BF16)
     row = lax.broadcasted_iota(jnp.int32, (tok, tok), 0)
     col = lax.broadcasted_iota(jnp.int32, (tok, tok), 1)
@@ -32,13 +32,24 @@
 
     def place(e, mine):
         slot = jnp.sum(jnp.where(mine, before, 0.0), axis=0, keepdims=True)
-        return jnp.bitwise_xor(e, pos[0]) * cap + slot.astype(jnp.int32)
+        other = jnp.bitwise_xor(jnp.bitwise_and(e, 1), pos[0])
+        return other * half + (e >> 1) * cap + slot.astype(jnp.int32)
 
     t0 = place(e0, hot0)
     t1 = place(e1, hot1)
-    rows = lax.broadcasted_iota(jnp.int32, (count, tok), 0)
-    put = ((rows == t0) | (rows == t1)).astype(F32).astype(BF16)
-    out[...] = jnp.dot(put, tokens[...], preferred_element_type=F32).astype(BF16)
+    for at, out in ((0, near), (half, far)):
+        rows = lax.broadcasted_iota(jnp.int32, (half, tok), 0) + at
+        put = ((rows == t0) | (rows == t1)).astype(F32).astype(BF16)
+        out[...] = jnp.dot(put, tokens[...], preferred_element_type=F32).astype(BF16)
+
+    def packed(t):
+        other = (t >= half).astype(jnp.int32)
+        inside = t - other * half
+        at_z = inside // cap
+        return (at_z * 2 + other) * cap + (inside - at_z * cap)
+
+    t0 = packed(t0)
+    t1 = packed(t1)
     stack = jnp.concatenate(
         [t0.astype(F32), t1.astype(F32), weights[...], jnp.zeros((4, tok), F32)], axis=0
     )
@@ -47,16 +58,17 @@
 
 def pack(c, routes, weights, tokens):
     tok, share = tokens.shape
-    count = 2 * lax.axis_size("z") * 32
+    half = lax.axis_size("z") * 32
     vmem = pl.BlockSpec(memory_space=pltpu.VMEM)
     return pl.pallas_call(
         pack_kernel,
         out_shape=(
-            jax.ShapeDtypeStruct((count, share), BF16),
+            jax.ShapeDtypeStruct((half, share), BF16),
+            jax.ShapeDtypeStruct((half, share), BF16),
             jax.ShapeDtypeStruct((tok, 8), F32),
         ),
         in_specs=[pl.BlockSpec(memory_space=pltpu.SMEM), vmem, vmem, vmem],
-        out_specs=(vmem, vmem),
+        out_specs=(vmem, vmem, vmem),
         name="pack",
     )(c, routes, weights, tokens)
 
@@ -73,16 +85,17 @@
         refs = refs[11:]
     raw, gain_s, xn, gu_s, d_s, stage, sems, osems = refs
     core = core_ref[0]
-    role = core if first else 1 - core
-    at_outer = jnp.where(role == 0, y_ref[0], x_ref[0])
-    at_inner = jnp.where(role == 0, x_ref[0], y_ref[0])
+    at_outer = jnp.where(core == 0, y_ref[0], x_ref[0])
 
     def block(o, i):
         outer = o if first else jnp.bitwise_and(at_outer + o, 3)
-        return jnp.where(role == 0, outer * 4 + i, i * 4 + outer)
-
-    def taken(o, i):
-        return block(o, i if first else jnp.bitwise_and(at_inner + i, 3))
+        return jnp.where(core == 0, outer * 4 + i, i * 4 + outer)
+
+    def sent(o, i):
+        if first:
+            return block(o, i)
+        outer = jnp.bitwise_and(jnp.where(core == 0, x_ref[0], y_ref[0]) + o, 3)
+        return jnp.where(core == 0, i * 4 + outer, outer * 4 + i)
 
     def source(o):
         if first:
@@ -103,7 +116,7 @@
 
     def fetch_rows(at):
         return [
-            fetch(source(o).at[i, pl.ds(at, half), :], raw.at[taken(o, i), pl.ds(at, half), :])
+            fetch(source(o).at[i, pl.ds(at, half), :], raw.at[block(o, i), pl.ds(at, half), :])
             for o in range(4)
             for i in range(4)
         ]
@@ -121,7 +134,7 @@
     x_cp.append(fetch_rows(half))
     d_cp = [
         fetch(
-            wd.at[:, pl.ds(pl.multiple_of(block(o, i) * 128, 128), 128)],
+            wd.at[:, pl.ds(pl.multiple_of(sent(o, i) * 128, 128), 128)],
             d_s.at[:, pl.ds((o * 4 + i) * 128, 128)],
         )
         for o in range(4)
@@ -311,20 +324,27 @@
     return jnp.broadcast_to(v[None], (4, *v.shape))
 
 
+def over_z(near, far):
+    share = near.shape[1]
+    both = jnp.stack([near.reshape(16, -1, share), far.reshape(16, -1, share)], axis=1)
+    return exchange(both, "z")
+
+
 def local(tokens, norm_gain, w_gate, w_up, w_down, routes, route_weights, final_gain):
     _, share = tokens.shape
     width = share * 16
     place = tuple(lax.axis_index(a).astype(jnp.int32).reshape(1) for a in ("c", "y", "x"))
-    rows, table = pack(place[0], routes.T, route_weights.T, tokens)
+    near, far, table = pack(place[0], routes.T, route_weights.T, tokens)
     weights = (w_gate[0], w_up[0], w_down[0])
-    both = exchange(rows.reshape(16, 2, -1, share), "z")
+    both = over_z(near, swap(far))
     near, far = (both[:, i].reshape(-1, share) for i in range(2))
-    far = swap(far)
     gain_rows = jnp.broadcast_to(norm_gain[None, :], (GAIN_ROWS, share))
-    far = across(copies_of(jnp.concatenate([far, gain_rows], axis=0)), 0)
-    near = jnp.stack([near] + [ahead(near, 1, -s) for s in (1, 2, 3)])
-    far = across(copies_of(far), 1)
-    near = [near] + [ahead(near, 0, -s) for s in (1, 2, 3)]
+    rows = jnp.concatenate([far, gain_rows, near], axis=0)
+    rows = across(copies_of(rows), 0)
+    first = far.shape[0] + GAIN_ROWS
+    far = across(copies_of(rows[:, :first]), 1)
+    near = rows[:, first:]
+    near = [near] + [ahead(near, 1, -s) for s in (1, 2, 3)]
     far, gain = expert(True, place, far, weights, None)
     far = summed(across(far, 1))
     near = expert(False, place, near, weights, gain)
@@ -332,8 +352,8 @@
     near = total_of([near[0], two, ahead(near[1], 0, 1), ahead(near[3], 0, 3)])
     far = swap(summed(across(far, 0)))
     near = summed(across(near, 1))
-    both = jnp.stack([near.reshape(16, -1, share), far.reshape(16, -1, share)], axis=1)
-    combined, squares = combine(table, exchange(both, "z").reshape(-1, share))
+    both = over_z(near, far)
+    combined, squares = combine(table, both.reshape(-1, share))
     total = exchange(squares, ("y", "x")).sum(axis=(0, 1))
     scale = lax.rsqrt(total / width + EPS)
     return (combined * scale[:, None] * final_gain.astype(F32)[None, :]).astype(BF16)

time: 210 us -> 205 us (0.976)
  starting transfers between devices: 55.4 us -> 45.2 us
  blocking collectives: 66 us -> 70.9 us
  waiting for transfers between devices: 59.3 us -> 55.8 us
  local copies, waits for them, and re-layouts: 3.26 us -> 5.46 us
    ppermute x9 -> x6, starting transfers between devices: 29.5 us -> 19.6 us  [ahead(): return lax.ppermute(v, ALL, pairs)]
    all_to_all x3, blocking collectives: 66 us -> 70.9 us  [exchange(): lax.all_to_all(v, axis, split_axis=0, concat_axis=0, tiled=True, axis_ind...]
    ppermute x9 -> x6, waiting for transfers between devices: 25.7 us -> 22 us  [ahead(): return lax.ppermute(v, ALL, pairs)]
  transfers between devices with their start and end apart: 16 -> 13, of which waited for: 11 -> 9; matrix products, arithmetic and copies ran while one was open for 2% -> 2% of each run, Pallas kernels for 4% -> 4%
where the time goes in v6:
time: 205 us; the launch traced here: 204 us
  blocking collectives  70.9 us (35%)
  waiting for transfers between devices  55.8 us (27%)
  starting transfers between devices  45.2 us (22%)
  Pallas kernels  19.5 us (10%)
  other arithmetic  6.48 us (3%)
  local copies, waits for them, and re-layouts  5.46 us (3%)
    all_to_all x3, blocking collectives, exchange(): lax.all_to_all(v, axis, split_axis=0, concat_axis=0, tiled=True, axis_ind...  70.9 us
    all_to_all x5, waiting for transfers between devices, exchange(): lax.all_to_all(v, axis, split_axis=0, concat_axis=0, tiled=True, axis_ind...  32.3 us
    ppermute x6, waiting for transfers between devices, ahead(): return lax.ppermute(v, ALL, pairs)  22 us
    all_to_all x5, starting transfers between devices, exchange(): lax.all_to_all(v, axis, split_axis=0, concat_axis=0, tiled=True, axis_ind...  21.7 us
    ppermute x6, starting transfers between devices, ahead(): return lax.ppermute(v, ALL, pairs)  19.6 us
    pallas_call x2, Pallas kernels, expert(): pl.pallas_call(functools.partial(expert_kernel, first, rows), out_shape=o...  15.2 us
  transfers between devices with their start and end apart: 13, of which 9 were waited for; matrix products, arithmetic and copies ran while one was open for 2% of the time, Pallas kernels for 4%

profile of v6, /device:TPU:32, one launch (start us, length us, event | category | flops | bytes accessed | tf_op | source)
XLA Modules:
  0.0 203.6 jit_solution(1929282023954513973)
XLA Ops:
  0.0 2.1 %pack.1 = (bf16[512,128]{1,0:T(8,128)(2,1)}, bf16[512,128]{1,0:T(8,128)(2,1)}, f32[256,8]{1,0:T(8,128)}) custom-call(s32[1]{0:T(128)} %bitcast.pos.core_ref, s32[2,256]{1,0:T(2,128)} %bitcast.40, f32[2,256]{1,0:T(2,128)} %bitcast.41, bf16[256,128]{1,0:T(8,128)(2,1)} %tokens.1), custom_call_target="tpu_custom_call" | custom-call | tf_op jit(solution)/shard_map/pack/pallas_call | solution.py:63
  2.1 1.9 collective-permute-start
  4.0 1.5 collective-permute-done
  6.5 33.4 %all_to_all.40 = bf16[16,2,32,128]{3,2,1,0:T(8,128)(2,1)S(1)} all-to-all(bf16[16,2,32,128]{3,2,1,0:T(8,128)(2,1)S(1)} %pad_maximum_fusion.1), channel_id=1, replica_groups=mesh['z'=16,'c'=2,'y'=4,'x'=4] {'z'}, dimensions={0} | all-to-all | bytes 524288 | tf_op jit(solution)/shard_map/all_to_all | solution.py:288
  40.7 15.1 %all_to_all.41 = bf16[4,1040,128]{2,1,0:T(8,128)(2,1)S(1)} all-to-all(bf16[4,1040,128]{2,1,0:T(8,128)(2,1)S(1)} %broadcast_in_dim.7), channel_id=1, replica_groups={{0,1,2,3},{4,5,6,7},{8,9,10,11},{12,13,14,15},{16,20,24,28},{17,21,25,2..., dimensions={0} | all-to-all | bytes 2129920 | tf_op jit(solution)/shard_map/all_to_all | solution.py:288
  56.9 1.7 broadcast_in_dim.8
  58.5 4.5 %all-to-all-start.2 = ((bf16[4,4,528,128]{3,2,1,0:T(8,128)(2,1)}), bf16[4,4,528,128]{3,2,1,0:T(8,128)(2,1)}, u32[]{:S(2)}, u32[]{:S(2)}) async-start(bf16[4,4,528,128]{3,2,1,0:T(8,128)(2,1)} %broadcast_in_dim.8), calls=%async_computation.2 | async-start | bytes 4325376 | tf_op jit(solution)/shard_map/all_to_all | solution.py:288
  63.0 17.0 %all-to-all-done.2.xs = bf16[4,4,528,128]{3,2,1,0:T(8,128)(2,1)} async-done(((bf16[4,4,528,128]{3,2,1,0:T(8,128)(2,1)}), bf16[4,4,528,128]{3,2,1,0:T(8,128)(2,1)}, u32[]{:S(2)}, u32[]{:S(2)}) %all-to-all-start.2) | async-done | bytes 2162720 | tf_op jit(solution)/shard_map/all_to_all | solution.py:288
  80.0 7.6 %expert_far.1 = (bf16[4,4,512,128]{3,2,1,0:T(8,128)(2,1)}, bf16[16,16,128]{2,1,0:T(8,128)(2,1)}) custom-call(s32[1]{0:T(128)} %bitcast.pos.core_ref, s32[1]{0:T(128)} %bitcast.3.y_ref, s32[1]{0:T(128)} %bitcast.4.x_ref, bf16[4,4,528,128]{3,2,1,0:T(8,128)(2,1)} %all-to-all-done.2.xs, bf16[2048,384]{1,0:T(8,128)(2,1)} %bitcast.27, bf16[2048,384]{1,0:T(8,128)(2,1)} %bitcast.29, ...), custom_call_target="tpu_custom_call" | custom-call | tf_op jit(solution)/shard_map/expert_far/pallas_call | solution.py:215
  87.6 4.5 %all-to-all-start.4 = ((bf16[4,4,512,128]{3,2,1,0:T(8,128)(2,1)}), bf16[4,4,512,128]{3,2,1,0:T(8,128)(2,1)}, u32[]{:S(2)}, u32[]{:S(2)}) async-start(bf16[4,4,512,128]{3,2,1,0:T(8,128)(2,1)} %get-tuple-element.24), calls=%async_computation.4 | async-start | bytes 4194304 | tf_op jit(solution)/shard_map/all_to_all | solution.py:288
  93.2 5.1 %collective-permute-start.1 = (bf16[4,512,128]{2,1,0:T(8,128)(2,1)S(1)}, bf16[4,512,128]{2,1,0:T(8,128)(2,1)S(1)}, u32[]{:S(2)}, u32[]{:S(2)}) collective-permute-start(bf16[4,512,128]{2,1,0:T(8,128)(2,1)S(1)} %slice.66.xs), channel_id=1, source_target_pairs={{0,12},{1,13},{2,14},{3,15},{4,0},{5,1},{6,2},{7,3},{8,4},{9,5},{1... | collective-permute-start | bytes 1572872 | tf_op jit(solution)/shard_map/ppermute | solution.py:305
  98.3 2.8 %collective-permute-start.2 = (bf16[4,512,128]{2,1,0:T(8,128)(2,1)S(1)}, bf16[4,512,128]{2,1,0:T(8,128)(2,1)S(1)}, u32[]{:S(2)}, u32[]{:S(2)}) collective-permute-start(bf16[4,512,128]{2,1,0:T(8,128)(2,1)S(1)} %slice.66.xs), channel_id=1, source_target_pairs={{0,8},{1,9},{2,10},{3,11},{4,12},{5,13},{6,14},{7,15},{8,0},{9,1},... | collective-permute-start | bytes 1572872 | tf_op jit(solution)/shard_map/ppermute | solution.py:305
  101.0 2.8 %collective-permute-start.3 = (bf16[4,512,128]{2,1,0:T(8,128)(2,1)S(1)}, bf16[4,512,128]{2,1,0:T(8,128)(2,1)S(1)}, u32[]{:S(2)}, u32[]{:S(2)}) collective-permute-start(bf16[4,512,128]{2,1,0:T(8,128)(2,1)S(1)} %slice.66.xs), channel_id=1, source_target_pairs={{0,4},{1,5},{2,6},{3,7},{4,8},{5,9},{6,10},{7,11},{8,12},{9,13},{1... | collective-permute-start | bytes 1572872 | tf_op jit(solution)/shard_map/ppermute | solution.py:305
  103.8 8.9 %collective-permute-done.1.refs_0_ = bf16[4,512,128]{2,1,0:T(8,128)(2,1)S(1)} collective-permute-done((bf16[4,512,128]{2,1,0:T(8,128)(2,1)S(1)}, bf16[4,512,128]{2,1,0:T(8,128)(2,1)S(1)}, u32[]{:S(2)}, u32[]{:S(2)}) %collective-permute-start.1) | collective-permute-done | bytes 524320 | tf_op jit(solution)/shard_map/ppermute | solution.py:305
  112.7 1.6 collective-permute-done.2.refs_1_
  114.2 5.5 %collective-permute-done.3.refs_2_ = bf16[4,512,128]{2,1,0:T(8,128)(2,1)S(1)} collective-permute-done((bf16[4,512,128]{2,1,0:T(8,128)(2,1)S(1)}, bf16[4,512,128]{2,1,0:T(8,128)(2,1)S(1)}, u32[]{:S(2)}, u32[]{:S(2)}) %collective-permute-start.3) | collective-permute-done | bytes 524320 | tf_op jit(solution)/shard_map/ppermute | solution.py:305
  120.6 7.6 %expert_near.1 = (bf16[4,512,128]{2,1,0:T(8,128)(2,1)}, bf16[4,512,128]{2,1,0:T(8,128)(2,1)}, bf16[4,512,128]{2,1,0:T(8,128)(2,1)}, bf16[4,512,128]{2,1,0:T(8,128)(2,1)}) custom-call(s32[1]{0:T(128)} %bitcast.pos.core_ref, s32[1]{0:T(128)} %bitcast.3.y_ref, s32[1]{0:T(128)} %bitcast.4.x_ref, bf16[4,512,128]{2,1,0:T(8,128)(2,1)} %copy-done.1, ...), custom_call_target="tpu_custom_call" | custom-call | tf_op jit(solution)/shard_map/expert_near/pallas_call | solution.py:215
  128.2 3.2 %collective-permute-start.6 = (bf16[4,512,128]{2,1,0:T(8,128)(2,1)}, bf16[4,512,128]{2,1,0:T(8,128)(2,1)S(1)}, u32[]{:S(2)}, u32[]{:S(2)}) collective-permute-start(bf16[4,512,128]{2,1,0:T(8,128)(2,1)} %get-tuple-element.23), channel_id=1, source_target_pairs={{0,3},{1,0},{2,1},{3,2},{4,7},{5,4},{6,5},{7,6},{8,11},{9,8},{10,9... | collective-permute-start | bytes 1572872 | tf_op jit(solution)/shard_map/ppermute | solution.py:305
  131.4 2.8 %collective-permute-start.5 = (bf16[4,512,128]{2,1,0:T(8,128)(2,1)}, bf16[4,512,128]{2,1,0:T(8,128)(2,1)S(1)}, u32[]{:S(2)}, u32[]{:S(2)}) collective-permute-start(bf16[4,512,128]{2,1,0:T(8,128)(2,1)} %get-tuple-element.22), channel_id=1, source_target_pairs={{0,1},{1,2},{2,3},{3,0},{4,5},{5,6},{6,7},{7,4},{8,9},{9,10},{10,1... | collective-permute-start | bytes 1572872 | tf_op jit(solution)/shard_map/ppermute | solution.py:305
  134.2 3.0 %collective-permute-start.4 = (bf16[4,512,128]{2,1,0:T(8,128)(2,1)}, bf16[4,512,128]{2,1,0:T(8,128)(2,1)S(1)}, u32[]{:S(2)}, u32[]{:S(2)}) collective-permute-start(bf16[4,512,128]{2,1,0:T(8,128)(2,1)} %get-tuple-element.21), channel_id=1, source_target_pairs={{0,2},{1,3},{2,0},{3,1},{4,6},{5,7},{6,4},{7,5},{8,10},{9,11},{10,... | collective-permute-start | bytes 1572872 | tf_op jit(solution)/shard_map/ppermute | solution.py:305
  137.2 2.6 %fusion = bf16[4,512,128]{2,1,0:T(8,128)(2,1)} fusion(bf16[4,4,512,128]{3,2,1,0:T(8,128)(2,1)} %all-to-all-done.4), kind=kLoop, calls=%fused_computation.2 | loop fusion | flops 2097152 | bytes 2621440 | tf_op jit(solution)/shard_map/add | solution.py:315
  139.8 3.7 %all-to-all-start.5 = ((bf16[4,512,128]{2,1,0:T(8,128)(2,1)}), bf16[4,512,128]{2,1,0:T(8,128)(2,1)S(1)}, u32[]{:S(2)}, u32[]{:S(2)}) async-start(bf16[4,512,128]{2,1,0:T(8,128)(2,1)} %fusion), calls=%async_computation.5 | async-start | bytes 1048576 | tf_op jit(solution)/shard_map/all_to_all | solution.py:288
  143.5 6.0 %collective-permute-done.5 = bf16[4,512,128]{2,1,0:T(8,128)(2,1)S(1)} collective-permute-done((bf16[4,512,128]{2,1,0:T(8,128)(2,1)}, bf16[4,512,128]{2,1,0:T(8,128)(2,1)S(1)}, u32[]{:S(2)}, u32[]{:S(2)}) %collective-permute-start.5) | collective-permute-done | bytes 524320 | tf_op jit(solution)/shard_map/ppermute | solution.py:305
  150.6 1.7 all-to-all-done.5
  152.3 3.5 %all-to-all-start.3 = ((bf16[4,512,128]{2,1,0:T(8,128)(2,1)}), bf16[4,512,128]{2,1,0:T(8,128)(2,1)S(1)}, u32[]{:S(2)}, u32[]{:S(2)}) async-start(bf16[4,512,128]{2,1,0:T(8,128)(2,1)} %add_convert_fusion.1), calls=%async_computation.3 | async-start | bytes 1048576 | tf_op jit(solution)/shard_map/all_to_all | solution.py:288
  155.9 1.9 collective-permute-start.7
  157.8 6.0 %all-to-all-done.3 = bf16[4,512,128]{2,1,0:T(8,128)(2,1)S(1)} async-done(((bf16[4,512,128]{2,1,0:T(8,128)(2,1)}), bf16[4,512,128]{2,1,0:T(8,128)(2,1)S(1)}, u32[]{:S(2)}, u32[]{:S(2)}) %all-to-all-start.3) | async-done | bytes 524320 | tf_op jit(solution)/shard_map/all_to_all | solution.py:288
  164.0 22.5 %all_to_all.42 = bf16[16,2,32,128]{3,2,1,0:T(8,128)(2,1)} all-to-all(bf16[16,2,32,128]{3,2,1,0:T(8,128)(2,1)S(1)} %pad_maximum_fusion.2), channel_id=1, replica_groups=mesh['z'=16,'c'=2,'y'=4,'x'=4] {'z'}, dimensions={0} | all-to-all | bytes 524288 | tf_op jit(solution)/shard_map/all_to_all | solution.py:288
  186.5 2.2 %combine.1 = (f32[256,128]{1,0:T(8,128)}, f32[16,1,256]{2,1,0:T(1,128)}) custom-call(f32[256,8]{1,0:T(8,128)} %get-tuple-element.16.table, bf16[1024,128]{1,0:T(8,128)(2,1)} %bitcast.33), custom_call_target="tpu_custom_call" | custom-call | tf_op jit(solution)/shard_map/combine/pallas_call | solution.py:256
  188.7 5.7 %all-to-all-start.7 = ((f32[16,1,256]{2,1,0:T(1,128)}), f32[16,1,256]{2,1,0:T(1,128)S(1)}, u32[]{:S(2)}, u32[]{:S(2)}) async-start(f32[16,1,256]{2,1,0:T(1,128)} %get-tuple-element.26), calls=%async_computation.7 | async-start | bytes 32768 | tf_op jit(solution)/shard_map/all_to_all | solution.py:288
  194.4 7.6 %all-to-all-done.7 = f32[16,1,256]{2,1,0:T(1,128)S(1)} async-done(((f32[16,1,256]{2,1,0:T(1,128)}), f32[16,1,256]{2,1,0:T(1,128)S(1)}, u32[]{:S(2)}, u32[]{:S(2)}) %all-to-all-start.7) | async-done | bytes 16416 | tf_op jit(solution)/shard_map/all_to_all | solution.py:288
  202.0 1.6 multiply_convert_fusion
  (32 shorter events, 6.1 us)
Async XLA Ops:
  2.1 3.4 %collective-permute-start = (bf16[512,128]{1,0:T(8,128)(2,1)}, bf16[512,128]{1,0:T(8,128)(2,1)S(1)}, u32[]{:S(2)}, u32[]{:S(2)}) collective-permute-start(bf16[512,128]{1,0:T(8,128)(2,1)} %get-tuple-element.18), channel_id=1, source_target_pairs={{0,16},{16,0},{1,17},{17,1},{2,18},{18,2},{3,19},{19,3},{4,20},{20... | collective-permute-start | bytes 393224 | tf_op jit(solution)/shard_map/ppermute | solution.py:309
  55.8 1.0 copy-start
  58.5 21.4 %all-to-all-start.2 = ((bf16[4,4,528,128]{3,2,1,0:T(8,128)(2,1)}), bf16[4,4,528,128]{3,2,1,0:T(8,128)(2,1)}, u32[]{:S(2)}, u32[]{:S(2)}) async-start(bf16[4,4,528,128]{3,2,1,0:T(8,128)(2,1)} %broadcast_in_dim.8), calls=%async_computation.2 | async-start | bytes 4325376 | tf_op jit(solution)/shard_map/all_to_all | solution.py:288
  87.6 49.6 %all-to-all-start.4 = ((bf16[4,4,512,128]{3,2,1,0:T(8,128)(2,1)}), bf16[4,4,512,128]{3,2,1,0:T(8,128)(2,1)}, u32[]{:S(2)}, u32[]{:S(2)}) async-start(bf16[4,4,512,128]{3,2,1,0:T(8,128)(2,1)} %get-tuple-element.24), calls=%async_computation.4 | async-start | bytes 4194304 | tf_op jit(solution)/shard_map/all_to_all | solution.py:288
  93.1 27.5 %copy-start.1 = (bf16[4,512,128]{2,1,0:T(8,128)(2,1)}, bf16[4,512,128]{2,1,0:T(8,128)(2,1)S(1)}, u32[]{:S(2)}) copy-start(bf16[4,512,128]{2,1,0:T(8,128)(2,1)S(1)} %slice.66.xs) | copy-start | bytes 1572868
  93.2 19.5 %collective-permute-start.1 = (bf16[4,512,128]{2,1,0:T(8,128)(2,1)S(1)}, bf16[4,512,128]{2,1,0:T(8,128)(2,1)S(1)}, u32[]{:S(2)}, u32[]{:S(2)}) collective-permute-start(bf16[4,512,128]{2,1,0:T(8,128)(2,1)S(1)} %slice.66.xs), channel_id=1, source_target_pairs={{0,12},{1,13},{2,14},{3,15},{4,0},{5,1},{6,2},{7,3},{8,4},{9,5},{1... | collective-permute-start | bytes 1572872 | tf_op jit(solution)/shard_map/ppermute | solution.py:305
  98.3 16.0 %collective-permute-start.2 = (bf16[4,512,128]{2,1,0:T(8,128)(2,1)S(1)}, bf16[4,512,128]{2,1,0:T(8,128)(2,1)S(1)}, u32[]{:S(2)}, u32[]{:S(2)}) collective-permute-start(bf16[4,512,128]{2,1,0:T(8,128)(2,1)S(1)} %slice.66.xs), channel_id=1, source_target_pairs={{0,8},{1,9},{2,10},{3,11},{4,12},{5,13},{6,14},{7,15},{8,0},{9,1},... | collective-permute-start | bytes 1572872 | tf_op jit(solution)/shard_map/ppermute | solution.py:305
  101.0 18.7 %collective-permute-start.3 = (bf16[4,512,128]{2,1,0:T(8,128)(2,1)S(1)}, bf16[4,512,128]{2,1,0:T(8,128)(2,1)S(1)}, u32[]{:S(2)}, u32[]{:S(2)}) collective-permute-start(bf16[4,512,128]{2,1,0:T(8,128)(2,1)S(1)} %slice.66.xs), channel_id=1, source_target_pairs={{0,4},{1,5},{2,6},{3,7},{4,8},{5,9},{6,10},{7,11},{8,12},{9,13},{1... | collective-permute-start | bytes 1572872 | tf_op jit(solution)/shard_map/ppermute | solution.py:305
  112.7 7.1 %copy-start.3 = (bf16[4,512,128]{2,1,0:T(8,128)(2,1)}, bf16[4,512,128]{2,1,0:T(8,128)(2,1)S(1)}, u32[]{:S(2)}) copy-start(bf16[4,512,128]{2,1,0:T(8,128)(2,1)S(1)} %collective-permute-done.1.refs_0_) | copy-start | bytes 1572868
  114.2 5.5 %copy-start.4 = (bf16[4,512,128]{2,1,0:T(8,128)(2,1)}, bf16[4,512,128]{2,1,0:T(8,128)(2,1)S(1)}, u32[]{:S(2)}) copy-start(bf16[4,512,128]{2,1,0:T(8,128)(2,1)S(1)} %collective-permute-done.2.refs_1_) | copy-start | bytes 1572868
  119.8 0.8 copy-start.5
  128.2 21.3 %copy-start.2 = (bf16[4,512,128]{2,1,0:T(8,128)(2,1)S(1)}, bf16[4,512,128]{2,1,0:T(8,128)(2,1)}, u32[]{:S(2)}) copy-start(bf16[4,512,128]{2,1,0:T(8,128)(2,1)} %get-tuple-element.20) | copy-start | bytes 1572868
  128.2 15.3 %collective-permute-start.6 = (bf16[4,512,128]{2,1,0:T(8,128)(2,1)}, bf16[4,512,128]{2,1,0:T(8,128)(2,1)S(1)}, u32[]{:S(2)}, u32[]{:S(2)}) collective-permute-start(bf16[4,512,128]{2,1,0:T(8,128)(2,1)} %get-tuple-element.23), channel_id=1, source_target_pairs={{0,3},{1,0},{2,1},{3,2},{4,7},{5,4},{6,5},{7,6},{8,11},{9,8},{10,9... | collective-permute-start | bytes 1572872 | tf_op jit(solution)/shard_map/ppermute | solution.py:305
  131.4 18.1 %collective-permute-start.5 = (bf16[4,512,128]{2,1,0:T(8,128)(2,1)}, bf16[4,512,128]{2,1,0:T(8,128)(2,1)S(1)}, u32[]{:S(2)}, u32[]{:S(2)}) collective-permute-start(bf16[4,512,128]{2,1,0:T(8,128)(2,1)} %get-tuple-element.22), channel_id=1, source_target_pairs={{0,1},{1,2},{2,3},{3,0},{4,5},{5,6},{6,7},{7,4},{8,9},{9,10},{10,1... | collective-permute-start | bytes 1572872 | tf_op jit(solution)/shard_map/ppermute | solution.py:305
  134.2 15.3 %collective-permute-start.4 = (bf16[4,512,128]{2,1,0:T(8,128)(2,1)}, bf16[4,512,128]{2,1,0:T(8,128)(2,1)S(1)}, u32[]{:S(2)}, u32[]{:S(2)}) collective-permute-start(bf16[4,512,128]{2,1,0:T(8,128)(2,1)} %get-tuple-element.21), channel_id=1, source_target_pairs={{0,2},{1,3},{2,0},{3,1},{4,6},{5,7},{6,4},{7,5},{8,10},{9,11},{10,... | collective-permute-start | bytes 1572872 | tf_op jit(solution)/shard_map/ppermute | solution.py:305
  139.8 12.5 %all-to-all-start.5 = ((bf16[4,512,128]{2,1,0:T(8,128)(2,1)}), bf16[4,512,128]{2,1,0:T(8,128)(2,1)S(1)}, u32[]{:S(2)}, u32[]{:S(2)}) async-start(bf16[4,512,128]{2,1,0:T(8,128)(2,1)} %fusion), calls=%async_computation.5 | async-start | bytes 1048576 | tf_op jit(solution)/shard_map/all_to_all | solution.py:288
  150.6 43.8 %copy-start.6 = (bf16[128]{0:T(256)(128)(2,1)S(1)}, bf16[128]{0:T(256)(128)(2,1)}, u32[]{:S(2)}) copy-start(bf16[128]{0:T(256)(128)(2,1)} %param.15) | copy-start | bytes 772
  152.3 11.5 %all-to-all-start.3 = ((bf16[4,512,128]{2,1,0:T(8,128)(2,1)}), bf16[4,512,128]{2,1,0:T(8,128)(2,1)S(1)}, u32[]{:S(2)}, u32[]{:S(2)}) async-start(bf16[4,512,128]{2,1,0:T(8,128)(2,1)} %add_convert_fusion.1), calls=%async_computation.3 | async-start | bytes 1048576 | tf_op jit(solution)/shard_map/all_to_all | solution.py:288
  155.9 8.0 %collective-permute-start.7 = (bf16[512,128]{1,0:T(8,128)(2,1)S(1)}, bf16[512,128]{1,0:T(8,128)(2,1)S(1)}, u32[]{:S(2)}, u32[]{:S(2)}) collective-permute-start(bf16[512,128]{1,0:T(8,128)(2,1)S(1)} %fusion.1), channel_id=1, source_target_pairs={{0,16},{16,0},{1,17},{17,1},{2,18},{18,2},{3,19},{19,3},{4,20},{20... | collective-permute-start | bytes 393224 | tf_op jit(solution)/shard_map/ppermute | solution.py:309
  188.7 13.3 %all-to-all-start.7 = ((f32[16,1,256]{2,1,0:T(1,128)}), f32[16,1,256]{2,1,0:T(1,128)S(1)}, u32[]{:S(2)}, u32[]{:S(2)}) async-start(f32[16,1,256]{2,1,0:T(1,128)} %get-tuple-element.26), calls=%async_computation.7 | async-start | bytes 32768 | tf_op jit(solution)/shard_map/all_to_all | solution.py:288

commit v7 on v6

--- a/solution.py
+++ b/solution.py
@@ -94,8 +94,9 @@
     def sent(o, i):
         if first:
             return block(o, i)
-        outer = jnp.bitwise_and(jnp.where(core == 0, x_ref[0], y_ref[0]) + o, 3)
-        return jnp.where(core == 0, i * 4 + outer, outer * 4 + i)
+        y = jnp.bitwise_and(y_ref[0] + jnp.where(core == 0, i, o), 3)
+        x = jnp.bitwise_and(x_ref[0] + jnp.where(core == 0, o, i), 3)
+        return y * 4 + x
 
     def source(o):
         if first:
@@ -349,9 +350,10 @@
     far = summed(across(far, 1))
     near = expert(False, place, near, weights, gain)
     two = ahead(near[2], 0, 2)
-    near = total_of([near[0], two, ahead(near[1], 0, 1), ahead(near[3], 0, 3)])
+    near = (near[0], two, ahead(near[1], 0, 1), ahead(near[3], 0, 3))
+    near = [total_of([v[i] for v in near]) for i in range(4)]
     far = swap(summed(across(far, 0)))
-    near = summed(across(near, 1))
+    near = total_of([near[0]] + [ahead(near[s], 1, s) for s in (1, 2, 3)])
     both = over_z(near, far)
     combined, squares = combine(table, both.reshape(-1, share))
     total = exchange(squares, ("y", "x")).sum(axis=(0, 1))

time: 205 us -> 206 us (level)
  starting transfers between devices: 45.2 us -> 50 us
  waiting for transfers between devices: 55.8 us -> 52.1 us
    ppermute x6 -> x9, starting transfers between devices: 19.6 us -> 28.9 us  [ahead(): return lax.ppermute(v, ALL, pairs)]
    all_to_all x5 -> x4, waiting for transfers between devices: 32.3 us -> 24.5 us  [exchange(): lax.all_to_all(v, axis, split_axis=0, concat_axis=0, tiled=True, axis_ind...]
    all_to_all x5 -> x4, starting transfers between devices: 21.7 us -> 17.3 us  [exchange(): lax.all_to_all(v, axis, split_axis=0, concat_axis=0, tiled=True, axis_ind...]
    ppermute x6 -> x9, waiting for transfers between devices: 22 us -> 26.1 us  [ahead(): return lax.ppermute(v, ALL, pairs)]
  transfers between devices with their start and end apart: 13 -> 15, of which waited for: 9 -> 9; matrix products, arithmetic and copies ran while one was open for 2% -> 2% of each run, Pallas kernels for 4% -> 4%
where the time goes in v7:
time: 206 us; the launch traced here: 205 us
  blocking collectives  71.6 us (35%)
  waiting for transfers between devices  52.1 us (25%)
  starting transfers between devices  50 us (24%)
  Pallas kernels  19.5 us (9%)
  other arithmetic  5.68 us (3%)
  local copies, waits for them, and re-layouts  5.48 us (3%)
    all_to_all x3, blocking collectives, exchange(): lax.all_to_all(v, axis, split_axis=0, concat_axis=0, tiled=True, axis_ind...  71.6 us
    ppermute x9, starting transfers between devices, ahead(): return lax.ppermute(v, ALL, pairs)  28.9 us
    ppermute x9, waiting for transfers between devices, ahead(): return lax.ppermute(v, ALL, pairs)  26.1 us
    all_to_all x4, waiting for transfers between devices, exchange(): lax.all_to_all(v, axis, split_axis=0, concat_axis=0, tiled=True, axis_ind...  24.5 us
    all_to_all x4, starting transfers between devices, exchange(): lax.all_to_all(v, axis, split_axis=0, concat_axis=0, tiled=True, axis_ind...  17.3 us
    pallas_call x2, Pallas kernels, expert(): pl.pallas_call(functools.partial(expert_kernel, first, rows), out_shape=o...  15.2 us
  transfers between devices with their start and end apart: 15, of which 9 were waited for; matrix products, arithmetic and copies ran while one was open for 2% of the time, Pallas kernels for 4%

profile of v7, /device:TPU:32, one launch (start us, length us, event | category | flops | bytes accessed | tf_op | source)
XLA Modules:
  0.0 204.7 jit_solution(7712673467477338852)
XLA Ops:
  0.0 2.1 %pack.1 = (bf16[512,128]{1,0:T(8,128)(2,1)}, bf16[512,128]{1,0:T(8,128)(2,1)}, f32[256,8]{1,0:T(8,128)}) custom-call(s32[1]{0:T(128)} %bitcast.pos.core_ref, s32[2,256]{1,0:T(2,128)} %bitcast.51, f32[2,256]{1,0:T(2,128)} %bitcast.52, bf16[256,128]{1,0:T(8,128)(2,1)} %tokens.1), custom_call_target="tpu_custom_call" | custom-call | tf_op jit(solution)/shard_map/pack/pallas_call | solution.py:63
  2.1 1.9 collective-permute-start
  6.5 33.4 %all_to_all.35 = bf16[16,2,32,128]{3,2,1,0:T(8,128)(2,1)S(1)} all-to-all(bf16[16,2,32,128]{3,2,1,0:T(8,128)(2,1)S(1)} %pad_maximum_fusion.1), channel_id=1, replica_groups=mesh['z'=16,'c'=2,'y'=4,'x'=4] {'z'}, dimensions={0} | all-to-all | bytes 524288 | tf_op jit(solution)/shard_map/all_to_all | solution.py:289
  40.7 15.1 %all_to_all.36 = bf16[4,1040,128]{2,1,0:T(8,128)(2,1)S(1)} all-to-all(bf16[4,1040,128]{2,1,0:T(8,128)(2,1)S(1)} %broadcast_in_dim.7), channel_id=1, replica_groups={{0,1,2,3},{4,5,6,7},{8,9,10,11},{12,13,14,15},{16,20,24,28},{17,21,25,2..., dimensions={0} | all-to-all | bytes 2129920 | tf_op jit(solution)/shard_map/all_to_all | solution.py:289
  56.9 1.7 broadcast_in_dim.8
  58.6 4.5 %all-to-all-start.2 = ((bf16[4,4,528,128]{3,2,1,0:T(8,128)(2,1)}), bf16[4,4,528,128]{3,2,1,0:T(8,128)(2,1)}, u32[]{:S(2)}, u32[]{:S(2)}) async-start(bf16[4,4,528,128]{3,2,1,0:T(8,128)(2,1)} %broadcast_in_dim.8), calls=%async_computation.2 | async-start | bytes 4325376 | tf_op jit(solution)/shard_map/all_to_all | solution.py:289
  63.0 17.0 %all-to-all-done.2.xs = bf16[4,4,528,128]{3,2,1,0:T(8,128)(2,1)} async-done(((bf16[4,4,528,128]{3,2,1,0:T(8,128)(2,1)}), bf16[4,4,528,128]{3,2,1,0:T(8,128)(2,1)}, u32[]{:S(2)}, u32[]{:S(2)}) %all-to-all-start.2) | async-done | bytes 2162720 | tf_op jit(solution)/shard_map/all_to_all | solution.py:289
  80.0 7.6 %expert_far.1 = (bf16[4,4,512,128]{3,2,1,0:T(8,128)(2,1)}, bf16[16,16,128]{2,1,0:T(8,128)(2,1)}) custom-call(s32[1]{0:T(128)} %bitcast.pos.core_ref, s32[1]{0:T(128)} %bitcast.3.y_ref, s32[1]{0:T(128)} %bitcast.4.x_ref, bf16[4,4,528,128]{3,2,1,0:T(8,128)(2,1)} %all-to-all-done.2.xs, bf16[2048,384]{1,0:T(8,128)(2,1)} %bitcast.38, bf16[2048,384]{1,0:T(8,128)(2,1)} %bitcast.40, ...), custom_call_target="tpu_custom_call" | custom-call | tf_op jit(solution)/shard_map/expert_far/pallas_call | solution.py:216
  87.6 4.5 %all-to-all-start.3 = ((bf16[4,4,512,128]{3,2,1,0:T(8,128)(2,1)}), bf16[4,4,512,128]{3,2,1,0:T(8,128)(2,1)}, u32[]{:S(2)}, u32[]{:S(2)}) async-start(bf16[4,4,512,128]{3,2,1,0:T(8,128)(2,1)} %get-tuple-element.24), calls=%async_computation.3 | async-start | bytes 4194304 | tf_op jit(solution)/shard_map/all_to_all | solution.py:289
  93.2 5.1 %collective-permute-start.1 = (bf16[4,512,128]{2,1,0:T(8,128)(2,1)S(1)}, bf16[4,512,128]{2,1,0:T(8,128)(2,1)S(1)}, u32[]{:S(2)}, u32[]{:S(2)}) collective-permute-start(bf16[4,512,128]{2,1,0:T(8,128)(2,1)S(1)} %slice.114.xs), channel_id=1, source_target_pairs={{0,12},{1,13},{2,14},{3,15},{4,0},{5,1},{6,2},{7,3},{8,4},{9,5},{1... | collective-permute-start | bytes 1572872 | tf_op jit(solution)/shard_map/ppermute | solution.py:306
  98.3 2.8 %collective-permute-start.2 = (bf16[4,512,128]{2,1,0:T(8,128)(2,1)S(1)}, bf16[4,512,128]{2,1,0:T(8,128)(2,1)S(1)}, u32[]{:S(2)}, u32[]{:S(2)}) collective-permute-start(bf16[4,512,128]{2,1,0:T(8,128)(2,1)S(1)} %slice.114.xs), channel_id=1, source_target_pairs={{0,8},{1,9},{2,10},{3,11},{4,12},{5,13},{6,14},{7,15},{8,0},{9,1},... | collective-permute-start | bytes 1572872 | tf_op jit(solution)/shard_map/ppermute | solution.py:306
  101.0 2.8 %collective-permute-start.3 = (bf16[4,512,128]{2,1,0:T(8,128)(2,1)S(1)}, bf16[4,512,128]{2,1,0:T(8,128)(2,1)S(1)}, u32[]{:S(2)}, u32[]{:S(2)}) collective-permute-start(bf16[4,512,128]{2,1,0:T(8,128)(2,1)S(1)} %slice.114.xs), channel_id=1, source_target_pairs={{0,4},{1,5},{2,6},{3,7},{4,8},{5,9},{6,10},{7,11},{8,12},{9,13},{1... | collective-permute-start | bytes 1572872 | tf_op jit(solution)/shard_map/ppermute | solution.py:306
  103.8 8.9 %collective-permute-done.1.refs_0_ = bf16[4,512,128]{2,1,0:T(8,128)(2,1)S(1)} collective-permute-done((bf16[4,512,128]{2,1,0:T(8,128)(2,1)S(1)}, bf16[4,512,128]{2,1,0:T(8,128)(2,1)S(1)}, u32[]{:S(2)}, u32[]{:S(2)}) %collective-permute-start.1) | collective-permute-done | bytes 524320 | tf_op jit(solution)/shard_map/ppermute | solution.py:306
  112.7 1.6 collective-permute-done.2.refs_1_
  114.3 5.5 %collective-permute-done.3.refs_2_ = bf16[4,512,128]{2,1,0:T(8,128)(2,1)S(1)} collective-permute-done((bf16[4,512,128]{2,1,0:T(8,128)(2,1)S(1)}, bf16[4,512,128]{2,1,0:T(8,128)(2,1)S(1)}, u32[]{:S(2)}, u32[]{:S(2)}) %collective-permute-start.3) | collective-permute-done | bytes 524320 | tf_op jit(solution)/shard_map/ppermute | solution.py:306
  120.6 7.6 %expert_near.1 = (bf16[4,512,128]{2,1,0:T(8,128)(2,1)}, bf16[4,512,128]{2,1,0:T(8,128)(2,1)}, bf16[4,512,128]{2,1,0:T(8,128)(2,1)}, bf16[4,512,128]{2,1,0:T(8,128)(2,1)}) custom-call(s32[1]{0:T(128)} %bitcast.pos.core_ref, s32[1]{0:T(128)} %bitcast.3.y_ref, s32[1]{0:T(128)} %bitcast.4.x_ref, bf16[4,512,128]{2,1,0:T(8,128)(2,1)} %copy-done.1, ...), custom_call_target="tpu_custom_call" | custom-call | tf_op jit(solution)/shard_map/expert_near/pallas_call | solution.py:216
  128.2 3.2 %collective-permute-start.6 = (bf16[4,512,128]{2,1,0:T(8,128)(2,1)}, bf16[4,512,128]{2,1,0:T(8,128)(2,1)S(1)}, u32[]{:S(2)}, u32[]{:S(2)}) collective-permute-start(bf16[4,512,128]{2,1,0:T(8,128)(2,1)} %get-tuple-element.23), channel_id=1, source_target_pairs={{0,3},{1,0},{2,1},{3,2},{4,7},{5,4},{6,5},{7,6},{8,11},{9,8},{10,9... | collective-permute-start | bytes 1572872 | tf_op jit(solution)/shard_map/ppermute | solution.py:306
  131.4 2.8 %collective-permute-start.5 = (bf16[4,512,128]{2,1,0:T(8,128)(2,1)}, bf16[4,512,128]{2,1,0:T(8,128)(2,1)S(1)}, u32[]{:S(2)}, u32[]{:S(2)}) collective-permute-start(bf16[4,512,128]{2,1,0:T(8,128)(2,1)} %get-tuple-element.22), channel_id=1, source_target_pairs={{0,1},{1,2},{2,3},{3,0},{4,5},{5,6},{6,7},{7,4},{8,9},{9,10},{10,1... | collective-permute-start | bytes 1572872 | tf_op jit(solution)/shard_map/ppermute | solution.py:306
  134.2 3.0 %collective-permute-start.4 = (bf16[4,512,128]{2,1,0:T(8,128)(2,1)}, bf16[4,512,128]{2,1,0:T(8,128)(2,1)S(1)}, u32[]{:S(2)}, u32[]{:S(2)}) collective-permute-start(bf16[4,512,128]{2,1,0:T(8,128)(2,1)} %get-tuple-element.21), channel_id=1, source_target_pairs={{0,2},{1,3},{2,0},{3,1},{4,6},{5,7},{6,4},{7,5},{8,10},{9,11},{10,... | collective-permute-start | bytes 1572872 | tf_op jit(solution)/shard_map/ppermute | solution.py:306
  137.2 2.6 %fusion = bf16[4,512,128]{2,1,0:T(8,128)(2,1)} fusion(bf16[4,4,512,128]{3,2,1,0:T(8,128)(2,1)} %all-to-all-done.3), kind=kLoop, calls=%fused_computation.1 | loop fusion | flops 2097152 | bytes 2621440 | tf_op jit(solution)/shard_map/add | solution.py:316
  139.8 3.7 %all-to-all-start.4 = ((bf16[4,512,128]{2,1,0:T(8,128)(2,1)}), bf16[4,512,128]{2,1,0:T(8,128)(2,1)S(1)}, u32[]{:S(2)}, u32[]{:S(2)}) async-start(bf16[4,512,128]{2,1,0:T(8,128)(2,1)} %fusion), calls=%async_computation.4 | async-start | bytes 1048576 | tf_op jit(solution)/shard_map/all_to_all | solution.py:289
  143.5 6.0 %collective-permute-done.5 = bf16[4,512,128]{2,1,0:T(8,128)(2,1)S(1)} collective-permute-done((bf16[4,512,128]{2,1,0:T(8,128)(2,1)}, bf16[4,512,128]{2,1,0:T(8,128)(2,1)S(1)}, u32[]{:S(2)}, u32[]{:S(2)}) %collective-permute-start.5) | collective-permute-done | bytes 524320 | tf_op jit(solution)/shard_map/ppermute | solution.py:306
  149.8 4.0 %collective-permute-start.9 = (bf16[512,128]{1,0:T(8,128)(2,1)S(1)}, bf16[512,128]{1,0:T(8,128)(2,1)S(1)}, u32[]{:S(2)}, u32[]{:S(2)}) collective-permute-start(bf16[512,128]{1,0:T(8,128)(2,1)S(1)} %get-tuple-element.28), channel_id=1, source_target_pairs={{0,12},{1,13},{2,14},{3,15},{4,0},{5,1},{6,2},{7,3},{8,4},{9,5},{1... | collective-permute-start | bytes 393224 | tf_op jit(solution)/shard_map/ppermute | solution.py:306
  153.7 3.4 %collective-permute-start.8 = (bf16[512,128]{1,0:T(8,128)(2,1)S(1)}, bf16[512,128]{1,0:T(8,128)(2,1)S(1)}, u32[]{:S(2)}, u32[]{:S(2)}) collective-permute-start(bf16[512,128]{1,0:T(8,128)(2,1)S(1)} %get-tuple-element.29), channel_id=1, source_target_pairs={{0,8},{1,9},{2,10},{3,11},{4,12},{5,13},{6,14},{7,15},{8,0},{9,1},... | collective-permute-start | bytes 393224 | tf_op jit(solution)/shard_map/ppermute | solution.py:306
  157.1 1.9 collective-permute-start.7
  159.1 1.9 collective-permute-start.10
  162.1 3.1 %collective-permute-done.7 = bf16[512,128]{1,0:T(8,128)(2,1)S(1)} collective-permute-done((bf16[512,128]{1,0:T(8,128)(2,1)S(1)}, bf16[512,128]{1,0:T(8,128)(2,1)S(1)}, u32[]{:S(2)}, u32[]{:S(2)}) %collective-permute-start.7) | collective-permute-done | bytes 131104 | tf_op jit(solution)/shard_map/ppermute | solution.py:306
  165.4 23.2 %all_to_all.37 = bf16[16,2,32,128]{3,2,1,0:T(8,128)(2,1)} all-to-all(bf16[16,2,32,128]{3,2,1,0:T(8,128)(2,1)S(1)} %pad_maximum_fusion.2), channel_id=1, replica_groups=mesh['z'=16,'c'=2,'y'=4,'x'=4] {'z'}, dimensions={0} | all-to-all | bytes 524288 | tf_op jit(solution)/shard_map/all_to_all | solution.py:289
  188.6 2.2 %combine.1 = (f32[256,128]{1,0:T(8,128)}, f32[16,1,256]{2,1,0:T(1,128)}) custom-call(f32[256,8]{1,0:T(8,128)} %get-tuple-element.16.table, bf16[1024,128]{1,0:T(8,128)(2,1)} %bitcast.44), custom_call_target="tpu_custom_call" | custom-call | tf_op jit(solution)/shard_map/combine/pallas_call | solution.py:257
  190.7 4.7 %all-to-all-start.6 = ((f32[16,1,256]{2,1,0:T(1,128)}), f32[16,1,256]{2,1,0:T(1,128)S(1)}, u32[]{:S(2)}, u32[]{:S(2)}) async-start(f32[16,1,256]{2,1,0:T(1,128)} %get-tuple-element.26), calls=%async_computation.6 | async-start | bytes 32768 | tf_op jit(solution)/shard_map/all_to_all | solution.py:289
  195.4 7.6 %all-to-all-done.6 = f32[16,1,256]{2,1,0:T(1,128)S(1)} async-done(((f32[16,1,256]{2,1,0:T(1,128)}), f32[16,1,256]{2,1,0:T(1,128)S(1)}, u32[]{:S(2)}, u32[]{:S(2)}) %all-to-all-start.6) | async-done | bytes 16416 | tf_op jit(solution)/shard_map/all_to_all | solution.py:289
  203.1 1.6 multiply_convert_fusion
  (36 shorter events, 7.8 us)
Async XLA Ops:
  2.1 3.4 %collective-permute-start = (bf16[512,128]{1,0:T(8,128)(2,1)}, bf16[512,128]{1,0:T(8,128)(2,1)S(1)}, u32[]{:S(2)}, u32[]{:S(2)}) collective-permute-start(bf16[512,128]{1,0:T(8,128)(2,1)} %get-tuple-element.18), channel_id=1, source_target_pairs={{0,16},{16,0},{1,17},{17,1},{2,18},{18,2},{3,19},{19,3},{4,20},{20... | collective-permute-start | bytes 393224 | tf_op jit(solution)/shard_map/ppermute | solution.py:310
  55.8 1.0 copy-start
  58.6 21.4 %all-to-all-start.2 = ((bf16[4,4,528,128]{3,2,1,0:T(8,128)(2,1)}), bf16[4,4,528,128]{3,2,1,0:T(8,128)(2,1)}, u32[]{:S(2)}, u32[]{:S(2)}) async-start(bf16[4,4,528,128]{3,2,1,0:T(8,128)(2,1)} %broadcast_in_dim.8), calls=%async_computation.2 | async-start | bytes 4325376 | tf_op jit(solution)/shard_map/all_to_all | solution.py:289
  87.6 49.6 %all-to-all-start.3 = ((bf16[4,4,512,128]{3,2,1,0:T(8,128)(2,1)}), bf16[4,4,512,128]{3,2,1,0:T(8,128)(2,1)}, u32[]{:S(2)}, u32[]{:S(2)}) async-start(bf16[4,4,512,128]{3,2,1,0:T(8,128)(2,1)} %get-tuple-element.24), calls=%async_computation.3 | async-start | bytes 4194304 | tf_op jit(solution)/shard_map/all_to_all | solution.py:289
  93.2 27.5 %copy-start.1 = (bf16[4,512,128]{2,1,0:T(8,128)(2,1)}, bf16[4,512,128]{2,1,0:T(8,128)(2,1)S(1)}, u32[]{:S(2)}) copy-start(bf16[4,512,128]{2,1,0:T(8,128)(2,1)S(1)} %slice.114.xs) | copy-start | bytes 1572868
  93.2 19.5 %collective-permute-start.1 = (bf16[4,512,128]{2,1,0:T(8,128)(2,1)S(1)}, bf16[4,512,128]{2,1,0:T(8,128)(2,1)S(1)}, u32[]{:S(2)}, u32[]{:S(2)}) collective-permute-start(bf16[4,512,128]{2,1,0:T(8,128)(2,1)S(1)} %slice.114.xs), channel_id=1, source_target_pairs={{0,12},{1,13},{2,14},{3,15},{4,0},{5,1},{6,2},{7,3},{8,4},{9,5},{1... | collective-permute-start | bytes 1572872 | tf_op jit(solution)/shard_map/ppermute | solution.py:306
  98.3 16.0 %collective-permute-start.2 = (bf16[4,512,128]{2,1,0:T(8,128)(2,1)S(1)}, bf16[4,512,128]{2,1,0:T(8,128)(2,1)S(1)}, u32[]{:S(2)}, u32[]{:S(2)}) collective-permute-start(bf16[4,512,128]{2,1,0:T(8,128)(2,1)S(1)} %slice.114.xs), channel_id=1, source_target_pairs={{0,8},{1,9},{2,10},{3,11},{4,12},{5,13},{6,14},{7,15},{8,0},{9,1},... | collective-permute-start | bytes 1572872 | tf_op jit(solution)/shard_map/ppermute | solution.py:306
  101.0 18.7 %collective-permute-start.3 = (bf16[4,512,128]{2,1,0:T(8,128)(2,1)S(1)}, bf16[4,512,128]{2,1,0:T(8,128)(2,1)S(1)}, u32[]{:S(2)}, u32[]{:S(2)}) collective-permute-start(bf16[4,512,128]{2,1,0:T(8,128)(2,1)S(1)} %slice.114.xs), channel_id=1, source_target_pairs={{0,4},{1,5},{2,6},{3,7},{4,8},{5,9},{6,10},{7,11},{8,12},{9,13},{1... | collective-permute-start | bytes 1572872 | tf_op jit(solution)/shard_map/ppermute | solution.py:306
  112.7 7.1 %copy-start.2 = (bf16[4,512,128]{2,1,0:T(8,128)(2,1)}, bf16[4,512,128]{2,1,0:T(8,128)(2,1)S(1)}, u32[]{:S(2)}) copy-start(bf16[4,512,128]{2,1,0:T(8,128)(2,1)S(1)} %collective-permute-done.1.refs_0_) | copy-start | bytes 1572868
  114.3 5.5 %copy-start.3 = (bf16[4,512,128]{2,1,0:T(8,128)(2,1)}, bf16[4,512,128]{2,1,0:T(8,128)(2,1)S(1)}, u32[]{:S(2)}) copy-start(bf16[4,512,128]{2,1,0:T(8,128)(2,1)S(1)} %collective-permute-done.2.refs_1_) | copy-start | bytes 1572868
  119.8 0.8 copy-start.4
  128.2 21.3 %copy-start.5 = (bf16[4,512,128]{2,1,0:T(8,128)(2,1)S(1)}, bf16[4,512,128]{2,1,0:T(8,128)(2,1)}, u32[]{:S(2)}) copy-start(bf16[4,512,128]{2,1,0:T(8,128)(2,1)} %get-tuple-element.20) | copy-start | bytes 1572868
  128.2 15.3 %collective-permute-start.6 = (bf16[4,512,128]{2,1,0:T(8,128)(2,1)}, bf16[4,512,128]{2,1,0:T(8,128)(2,1)S(1)}, u32[]{:S(2)}, u32[]{:S(2)}) collective-permute-start(bf16[4,512,128]{2,1,0:T(8,128)(2,1)} %get-tuple-element.23), channel_id=1, source_target_pairs={{0,3},{1,0},{2,1},{3,2},{4,7},{5,4},{6,5},{7,6},{8,11},{9,8},{10,9... | collective-permute-start | bytes 1572872 | tf_op jit(solution)/shard_map/ppermute | solution.py:306
  131.4 18.1 %collective-permute-start.5 = (bf16[4,512,128]{2,1,0:T(8,128)(2,1)}, bf16[4,512,128]{2,1,0:T(8,128)(2,1)S(1)}, u32[]{:S(2)}, u32[]{:S(2)}) collective-permute-start(bf16[4,512,128]{2,1,0:T(8,128)(2,1)} %get-tuple-element.22), channel_id=1, source_target_pairs={{0,1},{1,2},{2,3},{3,0},{4,5},{5,6},{6,7},{7,4},{8,9},{9,10},{10,1... | collective-permute-start | bytes 1572872 | tf_op jit(solution)/shard_map/ppermute | solution.py:306
  134.2 15.3 %collective-permute-start.4 = (bf16[4,512,128]{2,1,0:T(8,128)(2,1)}, bf16[4,512,128]{2,1,0:T(8,128)(2,1)S(1)}, u32[]{:S(2)}, u32[]{:S(2)}) collective-permute-start(bf16[4,512,128]{2,1,0:T(8,128)(2,1)} %get-tuple-element.21), channel_id=1, source_target_pairs={{0,2},{1,3},{2,0},{3,1},{4,6},{5,7},{6,4},{7,5},{8,10},{9,11},{10,... | collective-permute-start | bytes 1572872 | tf_op jit(solution)/shard_map/ppermute | solution.py:306
  139.8 19.2 %all-to-all-start.4 = ((bf16[4,512,128]{2,1,0:T(8,128)(2,1)}), bf16[4,512,128]{2,1,0:T(8,128)(2,1)S(1)}, u32[]{:S(2)}, u32[]{:S(2)}) async-start(bf16[4,512,128]{2,1,0:T(8,128)(2,1)} %fusion), calls=%async_computation.4 | async-start | bytes 1048576 | tf_op jit(solution)/shard_map/all_to_all | solution.py:289
  149.5 45.9 %copy-start.6 = (bf16[128]{0:T(256)(128)(2,1)S(1)}, bf16[128]{0:T(256)(128)(2,1)}, u32[]{:S(2)}) copy-start(bf16[128]{0:T(256)(128)(2,1)} %param.15) | copy-start | bytes 772
  149.8 11.3 %collective-permute-start.9 = (bf16[512,128]{1,0:T(8,128)(2,1)S(1)}, bf16[512,128]{1,0:T(8,128)(2,1)S(1)}, u32[]{:S(2)}, u32[]{:S(2)}) collective-permute-start(bf16[512,128]{1,0:T(8,128)(2,1)S(1)} %get-tuple-element.28), channel_id=1, source_target_pairs={{0,12},{1,13},{2,14},{3,15},{4,0},{5,1},{6,2},{7,3},{8,4},{9,5},{1... | collective-permute-start | bytes 393224 | tf_op jit(solution)/shard_map/ppermute | solution.py:306
  153.7 8.4 %collective-permute-start.8 = (bf16[512,128]{1,0:T(8,128)(2,1)S(1)}, bf16[512,128]{1,0:T(8,128)(2,1)S(1)}, u32[]{:S(2)}, u32[]{:S(2)}) collective-permute-start(bf16[512,128]{1,0:T(8,128)(2,1)S(1)} %get-tuple-element.29), channel_id=1, source_target_pairs={{0,8},{1,9},{2,10},{3,11},{4,12},{5,13},{6,14},{7,15},{8,0},{9,1},... | collective-permute-start | bytes 393224 | tf_op jit(solution)/shard_map/ppermute | solution.py:306
  157.1 8.1 %collective-permute-start.7 = (bf16[512,128]{1,0:T(8,128)(2,1)S(1)}, bf16[512,128]{1,0:T(8,128)(2,1)S(1)}, u32[]{:S(2)}, u32[]{:S(2)}) collective-permute-start(bf16[512,128]{1,0:T(8,128)(2,1)S(1)} %get-tuple-element.27), channel_id=1, source_target_pairs={{0,4},{1,5},{2,6},{3,7},{4,8},{5,9},{6,10},{7,11},{8,12},{9,13},{1... | collective-permute-start | bytes 393224 | tf_op jit(solution)/shard_map/ppermute | solution.py:306
  159.1 6.2 %collective-permute-start.10 = (bf16[512,128]{1,0:T(8,128)(2,1)S(1)}, bf16[512,128]{1,0:T(8,128)(2,1)S(1)}, u32[]{:S(2)}, u32[]{:S(2)}) collective-permute-start(bf16[512,128]{1,0:T(8,128)(2,1)S(1)} %fusion.8), channel_id=1, source_target_pairs={{0,16},{16,0},{1,17},{17,1},{2,18},{18,2},{3,19},{19,3},{4,20},{20... | collective-permute-start | bytes 393224 | tf_op jit(solution)/shard_map/ppermute | solution.py:310
  190.7 12.3 %all-to-all-start.6 = ((f32[16,1,256]{2,1,0:T(1,128)}), f32[16,1,256]{2,1,0:T(1,128)S(1)}, u32[]{:S(2)}, u32[]{:S(2)}) async-start(f32[16,1,256]{2,1,0:T(1,128)} %get-tuple-element.26), calls=%async_computation.6 | async-start | bytes 32768 | tf_op jit(solution)/shard_map/all_to_all | solution.py:289

commit v8 on v6

--- a/solution.py
+++ b/solution.py
@@ -91,12 +91,6 @@
         outer = o if first else jnp.bitwise_and(at_outer + o, 3)
         return jnp.where(core == 0, outer * 4 + i, i * 4 + outer)
 
-    def sent(o, i):
-        if first:
-            return block(o, i)
-        outer = jnp.bitwise_and(jnp.where(core == 0, x_ref[0], y_ref[0]) + o, 3)
-        return jnp.where(core == 0, i * 4 + outer, outer * 4 + i)
-
     def source(o):
         if first:
             return xs.at[o]
@@ -134,7 +128,7 @@
     x_cp.append(fetch_rows(half))
     d_cp = [
         fetch(
-            wd.at[:, pl.ds(pl.multiple_of(sent(o, i) * 128, 128), 128)],
+            wd.at[:, pl.ds(pl.multiple_of(block(o, i) * 128, 128), 128)],
             d_s.at[:, pl.ds((o * 4 + i) * 128, 128)],
         )
         for o in range(4)
@@ -348,10 +342,10 @@
     far, gain = expert(True, place, far, weights, None)
     far = summed(across(far, 1))
     near = expert(False, place, near, weights, gain)
-    two = ahead(near[2], 0, 2)
-    near = total_of([near[0], two, ahead(near[1], 0, 1), ahead(near[3], 0, 3)])
+    two = ahead(near[2], 1, 2)
+    near = total_of([near[0], two, ahead(near[1], 1, 1), ahead(near[3], 1, 3)])
     far = swap(summed(across(far, 0)))
-    near = summed(across(near, 1))
+    near = summed(across(near, 0))
     both = over_z(near, far)
     combined, squares = combine(table, both.reshape(-1, share))
     total = exchange(squares, ("y", "x")).sum(axis=(0, 1))

time: 205 us -> 204 us (level)
    ppermute x6, waiting for transfers between devices: 22 us -> 25.5 us  [ahead(): return lax.ppermute(v, ALL, pairs)]
    all_to_all x5, starting transfers between devices: 21.7 us -> 19.5 us  [exchange(): lax.all_to_all(v, axis, split_axis=0, concat_axis=0, tiled=True, axis_ind...]
  transfers between devices with their start and end apart: 13 -> 13, of which waited for: 9 -> 8; matrix products, arithmetic and copies ran while one was open for 2% -> 2% of each run, Pallas kernels for 4% -> 4%
where the time goes in v8:
time: 204 us; the launch traced here: 203 us
  blocking collectives  70.7 us (35%)
  waiting for transfers between devices  57.5 us (28%)
  starting transfers between devices  43.3 us (21%)
  Pallas kernels  19.5 us (10%)
  other arithmetic  6.48 us (3%)
  local copies, waits for them, and re-layouts  5.46 us (3%)
    all_to_all x3, blocking collectives, exchange(): lax.all_to_all(v, axis, split_axis=0, concat_axis=0, tiled=True, axis_ind...  70.7 us
    all_to_all x5, waiting for transfers between devices, exchange(): lax.all_to_all(v, axis, split_axis=0, concat_axis=0, tiled=True, axis_ind...  30.5 us
    ppermute x6, waiting for transfers between devices, ahead(): return lax.ppermute(v, ALL, pairs)  25.5 us
    ppermute x6, starting transfers between devices, ahead(): return lax.ppermute(v, ALL, pairs)  20 us
    all_to_all x5, starting transfers between devices, exchange(): lax.all_to_all(v, axis, split_axis=0, concat_axis=0, tiled=True, axis_ind...  19.5 us
    pallas_call x2, Pallas kernels, expert(): pl.pallas_call(functools.partial(expert_kernel, first, rows), out_shape=o...  15.2 us
  transfers between devices with their start and end apart: 13, of which 8 were waited for; matrix products, arithmetic and copies ran while one was open for 2% of the time, Pallas kernels for 4%

profile of v8, /device:TPU:32, one launch (start us, length us, event | category | flops | bytes accessed | tf_op | source)
XLA Modules:
  0.0 203.2 jit_solution(12498359383242562552)
XLA Ops:
  0.0 2.1 %pack.1 = (bf16[512,128]{1,0:T(8,128)(2,1)}, bf16[512,128]{1,0:T(8,128)(2,1)}, f32[256,8]{1,0:T(8,128)}) custom-call(s32[1]{0:T(128)} %bitcast.pos.core_ref, s32[2,256]{1,0:T(2,128)} %bitcast.40, f32[2,256]{1,0:T(2,128)} %bitcast.41, bf16[256,128]{1,0:T(8,128)(2,1)} %tokens.1), custom_call_target="tpu_custom_call" | custom-call | tf_op jit(solution)/shard_map/pack/pallas_call | solution.py:63
  2.1 1.9 collective-permute-start
  4.0 1.5 collective-permute-done
  6.5 33.4 %all_to_all.40 = bf16[16,2,32,128]{3,2,1,0:T(8,128)(2,1)S(1)} all-to-all(bf16[16,2,32,128]{3,2,1,0:T(8,128)(2,1)S(1)} %pad_maximum_fusion.1), channel_id=1, replica_groups=mesh['z'=16,'c'=2,'y'=4,'x'=4] {'z'}, dimensions={0} | all-to-all | bytes 524288 | tf_op jit(solution)/shard_map/all_to_all | solution.py:282
  40.7 15.1 %all_to_all.41 = bf16[4,1040,128]{2,1,0:T(8,128)(2,1)S(1)} all-to-all(bf16[4,1040,128]{2,1,0:T(8,128)(2,1)S(1)} %broadcast_in_dim.7), channel_id=1, replica_groups={{0,1,2,3},{4,5,6,7},{8,9,10,11},{12,13,14,15},{16,20,24,28},{17,21,25,2..., dimensions={0} | all-to-all | bytes 2129920 | tf_op jit(solution)/shard_map/all_to_all | solution.py:282
  56.9 1.7 broadcast_in_dim.8
  58.5 4.5 %all-to-all-start.2 = ((bf16[4,4,528,128]{3,2,1,0:T(8,128)(2,1)}), bf16[4,4,528,128]{3,2,1,0:T(8,128)(2,1)}, u32[]{:S(2)}, u32[]{:S(2)}) async-start(bf16[4,4,528,128]{3,2,1,0:T(8,128)(2,1)} %broadcast_in_dim.8), calls=%async_computation.2 | async-start | bytes 4325376 | tf_op jit(solution)/shard_map/all_to_all | solution.py:282
  63.0 17.0 %all-to-all-done.2.xs = bf16[4,4,528,128]{3,2,1,0:T(8,128)(2,1)} async-done(((bf16[4,4,528,128]{3,2,1,0:T(8,128)(2,1)}), bf16[4,4,528,128]{3,2,1,0:T(8,128)(2,1)}, u32[]{:S(2)}, u32[]{:S(2)}) %all-to-all-start.2) | async-done | bytes 2162720 | tf_op jit(solution)/shard_map/all_to_all | solution.py:282
  80.0 7.6 %expert_far.1 = (bf16[4,4,512,128]{3,2,1,0:T(8,128)(2,1)}, bf16[16,16,128]{2,1,0:T(8,128)(2,1)}) custom-call(s32[1]{0:T(128)} %bitcast.pos.core_ref, s32[1]{0:T(128)} %bitcast.3.y_ref, s32[1]{0:T(128)} %bitcast.4.x_ref, bf16[4,4,528,128]{3,2,1,0:T(8,128)(2,1)} %all-to-all-done.2.xs, bf16[2048,384]{1,0:T(8,128)(2,1)} %bitcast.27, bf16[2048,384]{1,0:T(8,128)(2,1)} %bitcast.29, ...), custom_call_target="tpu_custom_call" | custom-call | tf_op jit(solution)/shard_map/expert_far/pallas_call | solution.py:209
  87.6 4.5 %all-to-all-start.4 = ((bf16[4,4,512,128]{3,2,1,0:T(8,128)(2,1)}), bf16[4,4,512,128]{3,2,1,0:T(8,128)(2,1)}, u32[]{:S(2)}, u32[]{:S(2)}) async-start(bf16[4,4,512,128]{3,2,1,0:T(8,128)(2,1)} %get-tuple-element.24), calls=%async_computation.4 | async-start | bytes 4194304 | tf_op jit(solution)/shard_map/all_to_all | solution.py:282
  92.1 1.1 slice.66.xs
  93.2 5.1 %collective-permute-start.1 = (bf16[4,512,128]{2,1,0:T(8,128)(2,1)S(1)}, bf16[4,512,128]{2,1,0:T(8,128)(2,1)S(1)}, u32[]{:S(2)}, u32[]{:S(2)}) collective-permute-start(bf16[4,512,128]{2,1,0:T(8,128)(2,1)S(1)} %slice.66.xs), channel_id=1, source_target_pairs={{0,12},{1,13},{2,14},{3,15},{4,0},{5,1},{6,2},{7,3},{8,4},{9,5},{1... | collective-permute-start | bytes 1572872 | tf_op jit(solution)/shard_map/ppermute | solution.py:299
  98.3 2.8 %collective-permute-start.2 = (bf16[4,512,128]{2,1,0:T(8,128)(2,1)S(1)}, bf16[4,512,128]{2,1,0:T(8,128)(2,1)S(1)}, u32[]{:S(2)}, u32[]{:S(2)}) collective-permute-start(bf16[4,512,128]{2,1,0:T(8,128)(2,1)S(1)} %slice.66.xs), channel_id=1, source_target_pairs={{0,8},{1,9},{2,10},{3,11},{4,12},{5,13},{6,14},{7,15},{8,0},{9,1},... | collective-permute-start | bytes 1572872 | tf_op jit(solution)/shard_map/ppermute | solution.py:299
  101.0 2.8 %collective-permute-start.3 = (bf16[4,512,128]{2,1,0:T(8,128)(2,1)S(1)}, bf16[4,512,128]{2,1,0:T(8,128)(2,1)S(1)}, u32[]{:S(2)}, u32[]{:S(2)}) collective-permute-start(bf16[4,512,128]{2,1,0:T(8,128)(2,1)S(1)} %slice.66.xs), channel_id=1, source_target_pairs={{0,4},{1,5},{2,6},{3,7},{4,8},{5,9},{6,10},{7,11},{8,12},{9,13},{1... | collective-permute-start | bytes 1572872 | tf_op jit(solution)/shard_map/ppermute | solution.py:299
  103.8 8.9 %collective-permute-done.1.refs_0_ = bf16[4,512,128]{2,1,0:T(8,128)(2,1)S(1)} collective-permute-done((bf16[4,512,128]{2,1,0:T(8,128)(2,1)S(1)}, bf16[4,512,128]{2,1,0:T(8,128)(2,1)S(1)}, u32[]{:S(2)}, u32[]{:S(2)}) %collective-permute-start.1) | collective-permute-done | bytes 524320 | tf_op jit(solution)/shard_map/ppermute | solution.py:299
  112.7 1.6 collective-permute-done.2.refs_1_
  114.2 5.5 %collective-permute-done.3.refs_2_ = bf16[4,512,128]{2,1,0:T(8,128)(2,1)S(1)} collective-permute-done((bf16[4,512,128]{2,1,0:T(8,128)(2,1)S(1)}, bf16[4,512,128]{2,1,0:T(8,128)(2,1)S(1)}, u32[]{:S(2)}, u32[]{:S(2)}) %collective-permute-start.3) | collective-permute-done | bytes 524320 | tf_op jit(solution)/shard_map/ppermute | solution.py:299
  120.6 7.6 %expert_near.1 = (bf16[4,512,128]{2,1,0:T(8,128)(2,1)}, bf16[4,512,128]{2,1,0:T(8,128)(2,1)}, bf16[4,512,128]{2,1,0:T(8,128)(2,1)}, bf16[4,512,128]{2,1,0:T(8,128)(2,1)}) custom-call(s32[1]{0:T(128)} %bitcast.pos.core_ref, s32[1]{0:T(128)} %bitcast.3.y_ref, s32[1]{0:T(128)} %bitcast.4.x_ref, bf16[4,512,128]{2,1,0:T(8,128)(2,1)} %copy-done.1, ...), custom_call_target="tpu_custom_call" | custom-call | tf_op jit(solution)/shard_map/expert_near/pallas_call | solution.py:209
  128.2 4.1 %collective-permute-start.6 = (bf16[4,512,128]{2,1,0:T(8,128)(2,1)}, bf16[4,512,128]{2,1,0:T(8,128)(2,1)S(1)}, u32[]{:S(2)}, u32[]{:S(2)}) collective-permute-start(bf16[4,512,128]{2,1,0:T(8,128)(2,1)} %get-tuple-element.23), channel_id=1, source_target_pairs={{0,12},{1,13},{2,14},{3,15},{4,0},{5,1},{6,2},{7,3},{8,4},{9,5},{1... | collective-permute-start | bytes 1572872 | tf_op jit(solution)/shard_map/ppermute | solution.py:299
  132.3 1.9 collective-permute-start.5
  134.2 3.4 %collective-permute-start.4 = (bf16[4,512,128]{2,1,0:T(8,128)(2,1)}, bf16[4,512,128]{2,1,0:T(8,128)(2,1)S(1)}, u32[]{:S(2)}, u32[]{:S(2)}) collective-permute-start(bf16[4,512,128]{2,1,0:T(8,128)(2,1)} %get-tuple-element.21), channel_id=1, source_target_pairs={{0,8},{1,9},{2,10},{3,11},{4,12},{5,13},{6,14},{7,15},{8,0},{9,1},... | collective-permute-start | bytes 1572872 | tf_op jit(solution)/shard_map/ppermute | solution.py:299
  137.6 2.6 %fusion = bf16[4,512,128]{2,1,0:T(8,128)(2,1)} fusion(bf16[4,4,512,128]{3,2,1,0:T(8,128)(2,1)} %all-to-all-done.4), kind=kLoop, calls=%fused_computation.2 | loop fusion | flops 2097152 | bytes 2621440 | tf_op jit(solution)/shard_map/add | solution.py:309
  140.2 3.5 %all-to-all-start.5 = ((bf16[4,512,128]{2,1,0:T(8,128)(2,1)}), bf16[4,512,128]{2,1,0:T(8,128)(2,1)S(1)}, u32[]{:S(2)}, u32[]{:S(2)}) async-start(bf16[4,512,128]{2,1,0:T(8,128)(2,1)} %fusion), calls=%async_computation.5 | async-start | bytes 1048576 | tf_op jit(solution)/shard_map/all_to_all | solution.py:282
  143.7 9.5 %collective-permute-done.5 = bf16[4,512,128]{2,1,0:T(8,128)(2,1)S(1)} collective-permute-done((bf16[4,512,128]{2,1,0:T(8,128)(2,1)}, bf16[4,512,128]{2,1,0:T(8,128)(2,1)S(1)}, u32[]{:S(2)}, u32[]{:S(2)}) %collective-permute-start.5) | collective-permute-done | bytes 524320 | tf_op jit(solution)/shard_map/ppermute | solution.py:299
  154.3 3.6 %all-to-all-start.3 = ((bf16[4,512,128]{2,1,0:T(8,128)(2,1)}), bf16[4,512,128]{2,1,0:T(8,128)(2,1)S(1)}, u32[]{:S(2)}, u32[]{:S(2)}) async-start(bf16[4,512,128]{2,1,0:T(8,128)(2,1)} %add_convert_fusion.1), calls=%async_computation.3 | async-start | bytes 1048576 | tf_op jit(solution)/shard_map/all_to_all | solution.py:282
  158.0 1.9 collective-permute-start.7
  159.9 6.0 %all-to-all-done.3 = bf16[4,512,128]{2,1,0:T(8,128)(2,1)S(1)} async-done(((bf16[4,512,128]{2,1,0:T(8,128)(2,1)}), bf16[4,512,128]{2,1,0:T(8,128)(2,1)S(1)}, u32[]{:S(2)}, u32[]{:S(2)}) %all-to-all-start.3) | async-done | bytes 524320 | tf_op jit(solution)/shard_map/all_to_all | solution.py:282
  166.1 22.2 %all_to_all.42 = bf16[16,2,32,128]{3,2,1,0:T(8,128)(2,1)} all-to-all(bf16[16,2,32,128]{3,2,1,0:T(8,128)(2,1)S(1)} %pad_maximum_fusion.2), channel_id=1, replica_groups=mesh['z'=16,'c'=2,'y'=4,'x'=4] {'z'}, dimensions={0} | all-to-all | bytes 524288 | tf_op jit(solution)/shard_map/all_to_all | solution.py:282
  188.3 2.2 %combine.1 = (f32[256,128]{1,0:T(8,128)}, f32[16,1,256]{2,1,0:T(1,128)}) custom-call(f32[256,8]{1,0:T(8,128)} %get-tuple-element.16.table, bf16[1024,128]{1,0:T(8,128)(2,1)} %bitcast.33), custom_call_target="tpu_custom_call" | custom-call | tf_op jit(solution)/shard_map/combine/pallas_call | solution.py:250
  190.5 3.5 %all-to-all-start.7 = ((f32[16,1,256]{2,1,0:T(1,128)}), f32[16,1,256]{2,1,0:T(1,128)S(1)}, u32[]{:S(2)}, u32[]{:S(2)}) async-start(f32[16,1,256]{2,1,0:T(1,128)} %get-tuple-element.26), calls=%async_computation.7 | async-start | bytes 32768 | tf_op jit(solution)/shard_map/all_to_all | solution.py:282
  194.0 7.5 %all-to-all-done.7 = f32[16,1,256]{2,1,0:T(1,128)S(1)} async-done(((f32[16,1,256]{2,1,0:T(1,128)}), f32[16,1,256]{2,1,0:T(1,128)S(1)}, u32[]{:S(2)}, u32[]{:S(2)}) %all-to-all-start.7) | async-done | bytes 16416 | tf_op jit(solution)/shard_map/all_to_all | solution.py:282
  201.6 1.6 multiply_convert_fusion
  (32 shorter events, 5.0 us)
Async XLA Ops:
  2.1 3.4 %collective-permute-start = (bf16[512,128]{1,0:T(8,128)(2,1)}, bf16[512,128]{1,0:T(8,128)(2,1)S(1)}, u32[]{:S(2)}, u32[]{:S(2)}) collective-permute-start(bf16[512,128]{1,0:T(8,128)(2,1)} %get-tuple-element.18), channel_id=1, source_target_pairs={{0,16},{16,0},{1,17},{17,1},{2,18},{18,2},{3,19},{19,3},{4,20},{20... | collective-permute-start | bytes 393224 | tf_op jit(solution)/shard_map/ppermute | solution.py:303
  55.8 1.0 copy-start
  58.5 21.4 %all-to-all-start.2 = ((bf16[4,4,528,128]{3,2,1,0:T(8,128)(2,1)}), bf16[4,4,528,128]{3,2,1,0:T(8,128)(2,1)}, u32[]{:S(2)}, u32[]{:S(2)}) async-start(bf16[4,4,528,128]{3,2,1,0:T(8,128)(2,1)} %broadcast_in_dim.8), calls=%async_computation.2 | async-start | bytes 4325376 | tf_op jit(solution)/shard_map/all_to_all | solution.py:282
  87.6 50.0 %all-to-all-start.4 = ((bf16[4,4,512,128]{3,2,1,0:T(8,128)(2,1)}), bf16[4,4,512,128]{3,2,1,0:T(8,128)(2,1)}, u32[]{:S(2)}, u32[]{:S(2)}) async-start(bf16[4,4,512,128]{3,2,1,0:T(8,128)(2,1)} %get-tuple-element.24), calls=%async_computation.4 | async-start | bytes 4194304 | tf_op jit(solution)/shard_map/all_to_all | solution.py:282
  93.1 27.5 %copy-start.1 = (bf16[4,512,128]{2,1,0:T(8,128)(2,1)}, bf16[4,512,128]{2,1,0:T(8,128)(2,1)S(1)}, u32[]{:S(2)}) copy-start(bf16[4,512,128]{2,1,0:T(8,128)(2,1)S(1)} %slice.66.xs) | copy-start | bytes 1572868
  93.2 19.5 %collective-permute-start.1 = (bf16[4,512,128]{2,1,0:T(8,128)(2,1)S(1)}, bf16[4,512,128]{2,1,0:T(8,128)(2,1)S(1)}, u32[]{:S(2)}, u32[]{:S(2)}) collective-permute-start(bf16[4,512,128]{2,1,0:T(8,128)(2,1)S(1)} %slice.66.xs), channel_id=1, source_target_pairs={{0,12},{1,13},{2,14},{3,15},{4,0},{5,1},{6,2},{7,3},{8,4},{9,5},{1... | collective-permute-start | bytes 1572872 | tf_op jit(solution)/shard_map/ppermute | solution.py:299
  98.3 16.0 %collective-permute-start.2 = (bf16[4,512,128]{2,1,0:T(8,128)(2,1)S(1)}, bf16[4,512,128]{2,1,0:T(8,128)(2,1)S(1)}, u32[]{:S(2)}, u32[]{:S(2)}) collective-permute-start(bf16[4,512,128]{2,1,0:T(8,128)(2,1)S(1)} %slice.66.xs), channel_id=1, source_target_pairs={{0,8},{1,9},{2,10},{3,11},{4,12},{5,13},{6,14},{7,15},{8,0},{9,1},... | collective-permute-start | bytes 1572872 | tf_op jit(solution)/shard_map/ppermute | solution.py:299
  101.0 18.7 %collective-permute-start.3 = (bf16[4,512,128]{2,1,0:T(8,128)(2,1)S(1)}, bf16[4,512,128]{2,1,0:T(8,128)(2,1)S(1)}, u32[]{:S(2)}, u32[]{:S(2)}) collective-permute-start(bf16[4,512,128]{2,1,0:T(8,128)(2,1)S(1)} %slice.66.xs), channel_id=1, source_target_pairs={{0,4},{1,5},{2,6},{3,7},{4,8},{5,9},{6,10},{7,11},{8,12},{9,13},{1... | collective-permute-start | bytes 1572872 | tf_op jit(solution)/shard_map/ppermute | solution.py:299
  112.7 7.1 %copy-start.3 = (bf16[4,512,128]{2,1,0:T(8,128)(2,1)}, bf16[4,512,128]{2,1,0:T(8,128)(2,1)S(1)}, u32[]{:S(2)}) copy-start(bf16[4,512,128]{2,1,0:T(8,128)(2,1)S(1)} %collective-permute-done.1.refs_0_) | copy-start | bytes 1572868
  114.2 5.5 %copy-start.4 = (bf16[4,512,128]{2,1,0:T(8,128)(2,1)}, bf16[4,512,128]{2,1,0:T(8,128)(2,1)S(1)}, u32[]{:S(2)}) copy-start(bf16[4,512,128]{2,1,0:T(8,128)(2,1)S(1)} %collective-permute-done.2.refs_1_) | copy-start | bytes 1572868
  119.8 0.8 copy-start.5
  128.2 25.0 %copy-start.2 = (bf16[4,512,128]{2,1,0:T(8,128)(2,1)S(1)}, bf16[4,512,128]{2,1,0:T(8,128)(2,1)}, u32[]{:S(2)}) copy-start(bf16[4,512,128]{2,1,0:T(8,128)(2,1)} %get-tuple-element.20) | copy-start | bytes 1572868
  128.2 15.5 %collective-permute-start.6 = (bf16[4,512,128]{2,1,0:T(8,128)(2,1)}, bf16[4,512,128]{2,1,0:T(8,128)(2,1)S(1)}, u32[]{:S(2)}, u32[]{:S(2)}) collective-permute-start(bf16[4,512,128]{2,1,0:T(8,128)(2,1)} %get-tuple-element.23), channel_id=1, source_target_pairs={{0,12},{1,13},{2,14},{3,15},{4,0},{5,1},{6,2},{7,3},{8,4},{9,5},{1... | collective-permute-start | bytes 1572872 | tf_op jit(solution)/shard_map/ppermute | solution.py:299
  132.3 20.9 %collective-permute-start.5 = (bf16[4,512,128]{2,1,0:T(8,128)(2,1)}, bf16[4,512,128]{2,1,0:T(8,128)(2,1)S(1)}, u32[]{:S(2)}, u32[]{:S(2)}) collective-permute-start(bf16[4,512,128]{2,1,0:T(8,128)(2,1)} %get-tuple-element.22), channel_id=1, source_target_pairs={{0,4},{1,5},{2,6},{3,7},{4,8},{5,9},{6,10},{7,11},{8,12},{9,13},{1... | collective-permute-start | bytes 1572872 | tf_op jit(solution)/shard_map/ppermute | solution.py:299
  134.2 19.0 %collective-permute-start.4 = (bf16[4,512,128]{2,1,0:T(8,128)(2,1)}, bf16[4,512,128]{2,1,0:T(8,128)(2,1)S(1)}, u32[]{:S(2)}, u32[]{:S(2)}) collective-permute-start(bf16[4,512,128]{2,1,0:T(8,128)(2,1)} %get-tuple-element.21), channel_id=1, source_target_pairs={{0,8},{1,9},{2,10},{3,11},{4,12},{5,13},{6,14},{7,15},{8,0},{9,1},... | collective-permute-start | bytes 1572872 | tf_op jit(solution)/shard_map/ppermute | solution.py:299
  140.2 14.1 %all-to-all-start.5 = ((bf16[4,512,128]{2,1,0:T(8,128)(2,1)}), bf16[4,512,128]{2,1,0:T(8,128)(2,1)S(1)}, u32[]{:S(2)}, u32[]{:S(2)}) async-start(bf16[4,512,128]{2,1,0:T(8,128)(2,1)} %fusion), calls=%async_computation.5 | async-start | bytes 1048576 | tf_op jit(solution)/shard_map/all_to_all | solution.py:282
  154.3 39.7 %copy-start.6 = (bf16[128]{0:T(256)(128)(2,1)S(1)}, bf16[128]{0:T(256)(128)(2,1)}, u32[]{:S(2)}) copy-start(bf16[128]{0:T(256)(128)(2,1)} %param.15) | copy-start | bytes 772
  154.3 11.7 %all-to-all-start.3 = ((bf16[4,512,128]{2,1,0:T(8,128)(2,1)}), bf16[4,512,128]{2,1,0:T(8,128)(2,1)S(1)}, u32[]{:S(2)}, u32[]{:S(2)}) async-start(bf16[4,512,128]{2,1,0:T(8,128)(2,1)} %add_convert_fusion.1), calls=%async_computation.3 | async-start | bytes 1048576 | tf_op jit(solution)/shard_map/all_to_all | solution.py:282
  158.0 8.0 %collective-permute-start.7 = (bf16[512,128]{1,0:T(8,128)(2,1)S(1)}, bf16[512,128]{1,0:T(8,128)(2,1)S(1)}, u32[]{:S(2)}, u32[]{:S(2)}) collective-permute-start(bf16[512,128]{1,0:T(8,128)(2,1)S(1)} %fusion.1), channel_id=1, source_target_pairs={{0,16},{16,0},{1,17},{17,1},{2,18},{18,2},{3,19},{19,3},{4,20},{20... | collective-permute-start | bytes 393224 | tf_op jit(solution)/shard_map/ppermute | solution.py:303
  190.5 11.0 %all-to-all-start.7 = ((f32[16,1,256]{2,1,0:T(1,128)}), f32[16,1,256]{2,1,0:T(1,128)S(1)}, u32[]{:S(2)}, u32[]{:S(2)}) async-start(f32[16,1,256]{2,1,0:T(1,128)} %get-tuple-element.26), calls=%async_computation.7 | async-start | bytes 32768 | tf_op jit(solution)/shard_map/all_to_all | solution.py:282

commit v9 on v8

--- a/solution.py
+++ b/solution.py
@@ -14,7 +14,7 @@
 GAIN_ROWS = 16
 
 
-def pack_kernel(pos, routes, weights, tokens, near, far, table):
+def pack_kernel(pos, routes, weights, tokens, gain, near, far, table, gain_out):
     tok = tokens.shape[0]
     half = near.shape[0]
     experts = 2 * lax.axis_size("z")
@@ -54,9 +54,10 @@
         [t0.astype(F32), t1.astype(F32), weights[...], jnp.zeros((4, tok), F32)], axis=0
     )
     table[...] = stack.T
-
-
-def pack(c, routes, weights, tokens):
+    gain_out[...] = jnp.broadcast_to(gain[...], gain_out.shape)
+
+
+def pack(c, routes, weights, tokens, gain):
     tok, share = tokens.shape
     half = lax.axis_size("z") * 32
     vmem = pl.BlockSpec(memory_space=pltpu.VMEM)
@@ -66,11 +67,12 @@
             jax.ShapeDtypeStruct((half, share), BF16),
             jax.ShapeDtypeStruct((half, share), BF16),
             jax.ShapeDtypeStruct((tok, 8), F32),
+            jax.ShapeDtypeStruct((GAIN_ROWS, share), BF16),
         ),
-        in_specs=[pl.BlockSpec(memory_space=pltpu.SMEM), vmem, vmem, vmem],
-        out_specs=(vmem, vmem, vmem),
+        in_specs=[pl.BlockSpec(memory_space=pltpu.SMEM)] + [vmem] * 4,
+        out_specs=(vmem,) * 4,
         name="pack",
-    )(c, routes, weights, tokens)
+    )(c, routes, weights, tokens, gain)
 
 
 def expert_kernel(first, rows, core_ref, y_ref, x_ref, xs, *refs):
@@ -230,13 +232,10 @@
     tok = table.shape[0]
     count = rows.shape[0]
     cols = lax.broadcasted_iota(jnp.int32, (tok, count), 1)
-    total = None
-    for k in range(2):
-        target = table[:, k : k + 1].astype(jnp.int32)
-        pick = (cols == target).astype(F32).astype(BF16)
-        got = jnp.dot(pick, rows[...], preferred_element_type=F32)
-        term = got * table[:, 2 + k : 3 + k]
-        total = term if total is None else total + term
+    picks = [(cols == table[:, k : k + 1].astype(jnp.int32)).astype(F32) for k in range(2)]
+    pick = jnp.concatenate(picks, axis=0).astype(BF16)
+    got = jnp.dot(pick, rows[...], preferred_element_type=F32)
+    total = got[:tok] * table[:, 2:3] + got[tok:] * table[:, 3:4]
     combined[...] = total
     mine = jnp.sum((total * total).T, axis=0, keepdims=True)
     for i in range(squares.shape[0]):
@@ -259,6 +258,26 @@
     )(table, rows)
 
 
+def finish_kernel(width, parts, combined, gain, out):
+    total = parts[0]
+    for i in range(1, parts.shape[0]):
+        total = total + parts[i]
+    scale = lax.rsqrt(total / width + EPS)
+    column = jnp.broadcast_to(scale, (8, scale.shape[1])).T[:, 0:1]
+    out[...] = (combined[...] * column * gain[...].astype(F32)).astype(BF16)
+
+
+def finish(width, parts, combined, gain):
+    vmem = pl.BlockSpec(memory_space=pltpu.VMEM)
+    return pl.pallas_call(
+        functools.partial(finish_kernel, width),
+        out_shape=jax.ShapeDtypeStruct(combined.shape, BF16),
+        in_specs=[vmem] * 3,
+        out_specs=vmem,
+        name="finish",
+    )(parts, combined, gain)
+
+
 ALL = ("z", "c", "y", "x")
 
 
@@ -328,11 +347,12 @@
     _, share = tokens.shape
     width = share * 16
     place = tuple(lax.axis_index(a).astype(jnp.int32).reshape(1) for a in ("c", "y", "x"))
-    near, far, table = pack(place[0], routes.T, route_weights.T, tokens)
+    near, far, table, gain_rows = pack(
+        place[0], routes.T, route_weights.T, tokens, norm_gain[None, :]
+    )
     weights = (w_gate[0], w_up[0], w_down[0])
     both = over_z(near, swap(far))
     near, far = (both[:, i].reshape(-1, share) for i in range(2))
-    gain_rows = jnp.broadcast_to(norm_gain[None, :], (GAIN_ROWS, share))
     rows = jnp.concatenate([far, gain_rows, near], axis=0)
     rows = across(copies_of(rows), 0)
     first = far.shape[0] + GAIN_ROWS
@@ -348,9 +368,8 @@
     near = summed(across(near, 0))
     both = over_z(near, far)
     combined, squares = combine(table, both.reshape(-1, share))
-    total = exchange(squares, ("y", "x")).sum(axis=(0, 1))
-    scale = lax.rsqrt(total / width + EPS)
-    return (combined * scale[:, None] * final_gain.astype(F32)[None, :]).astype(BF16)
+    parts = exchange(squares, ("y", "x"))
+    return finish(width, parts, combined, final_gain[None, :])
 
 
 def solution(mesh):

time: 204 us -> 205 us (level)
  blocking collectives: 70.7 us -> 82.8 us
  waiting for transfers between devices: 57.5 us -> 50 us
  starting transfers between devices: 43.3 us -> 39.7 us
    all_to_all x3 -> x4, blocking collectives: 70.7 us -> 82.8 us  [exchange(): lax.all_to_all(v, axis, split_axis=0, concat_axis=0, tiled=True, axis_ind...]
    all_to_all x5 -> x4, waiting for transfers between devices: 30.5 us -> 23 us  [exchange(): lax.all_to_all(v, axis, split_axis=0, concat_axis=0, tiled=True, axis_ind...]
    all_to_all x5 -> x4, starting transfers between devices: 19.5 us -> 15.8 us  [exchange(): lax.all_to_all(v, axis, split_axis=0, concat_axis=0, tiled=True, axis_ind...]
  transfers between devices with their start and end apart: 13 -> 12, of which waited for: 8 -> 7; matrix products, arithmetic and copies ran while one was open for 2% -> 2% of each run, Pallas kernels for 4% -> 4%
where the time goes in v9:
time: 205 us; the launch traced here: 204 us
  blocking collectives  82.8 us (40%)
  waiting for transfers between devices  50 us (24%)
  starting transfers between devices  39.7 us (19%)
  Pallas kernels  21.3 us (10%)
  other arithmetic  5.49 us (3%)
  local copies, waits for them, and re-layouts  4.81 us (2%)
    all_to_all x4, blocking collectives, exchange(): lax.all_to_all(v, axis, split_axis=0, concat_axis=0, tiled=True, axis_ind...  82.8 us
    ppermute x6, waiting for transfers between devices, ahead(): return lax.ppermute(v, ALL, pairs)  25.5 us
    all_to_all x4, waiting for transfers between devices, exchange(): lax.all_to_all(v, axis, split_axis=0, concat_axis=0, tiled=True, axis_ind...  23 us
    ppermute x6, starting transfers between devices, ahead(): return lax.ppermute(v, ALL, pairs)  20 us
    all_to_all x4, starting transfers between devices, exchange(): lax.all_to_all(v, axis, split_axis=0, concat_axis=0, tiled=True, axis_ind...  15.8 us
    pallas_call x2, Pallas kernels, expert(): pl.pallas_call(functools.partial(expert_kernel, first, rows), out_shape=o...  15.2 us
  transfers between devices with their start and end apart: 12, of which 7 were waited for; matrix products, arithmetic and copies ran while one was open for 2% of the time, Pallas kernels for 4%

profile of v9, /device:TPU:32, one launch (start us, length us, event | category | flops | bytes accessed | tf_op | source)
XLA Modules:
  0.0 204.3 jit_solution(14549396859832969456)
XLA Ops:
  0.0 2.1 %pack.1 = (bf16[512,128]{1,0:T(8,128)(2,1)}, bf16[512,128]{1,0:T(8,128)(2,1)}, f32[256,8]{1,0:T(8,128)}, bf16[16,128]{1,0:T(8,128)(2,1)}) custom-call(s32[1]{0:T(128)} %bitcast.pos.core_ref, s32[2,256]{1,0:T(2,128)} %bitcast.42, f32[2,256]{1,0:T(2,128)} %bitcast.43, bf16[256,128]{1,0:T(8,128)(2,1)} %tokens.1, bf16[1,128]{1,0:T(2,128)(2,1)} %bitcast.44), custom_call_target="tpu_custom_call" | custom-call | tf_op jit(solution)/shard_map/pack/pallas_call | solution.py:64
  2.1 1.9 collective-permute-start
  4.0 1.5 collective-permute-done
  6.5 33.4 %all_to_all.40 = bf16[16,2,32,128]{3,2,1,0:T(8,128)(2,1)S(1)} all-to-all(bf16[16,2,32,128]{3,2,1,0:T(8,128)(2,1)S(1)} %pad_maximum_fusion.1), channel_id=1, replica_groups=mesh['z'=16,'c'=2,'y'=4,'x'=4] {'z'}, dimensions={0} | all-to-all | bytes 524288 | tf_op jit(solution)/shard_map/all_to_all | solution.py:301
  40.7 15.1 %all_to_all.41 = bf16[4,1040,128]{2,1,0:T(8,128)(2,1)S(1)} all-to-all(bf16[4,1040,128]{2,1,0:T(8,128)(2,1)S(1)} %broadcast_in_dim.9), channel_id=1, replica_groups={{0,1,2,3},{4,5,6,7},{8,9,10,11},{12,13,14,15},{16,20,24,28},{17,21,25,2..., dimensions={0} | all-to-all | bytes 2129920 | tf_op jit(solution)/shard_map/all_to_all | solution.py:301
  56.9 1.7 broadcast_in_dim.20
  58.5 4.5 %all-to-all-start.2 = ((bf16[4,4,528,128]{3,2,1,0:T(8,128)(2,1)}), bf16[4,4,528,128]{3,2,1,0:T(8,128)(2,1)}, u32[]{:S(2)}, u32[]{:S(2)}) async-start(bf16[4,4,528,128]{3,2,1,0:T(8,128)(2,1)} %broadcast_in_dim.20), calls=%async_computation.2 | async-start | bytes 4325376 | tf_op jit(solution)/shard_map/all_to_all | solution.py:301
  63.0 17.0 %all-to-all-done.2.xs = bf16[4,4,528,128]{3,2,1,0:T(8,128)(2,1)} async-done(((bf16[4,4,528,128]{3,2,1,0:T(8,128)(2,1)}), bf16[4,4,528,128]{3,2,1,0:T(8,128)(2,1)}, u32[]{:S(2)}, u32[]{:S(2)}) %all-to-all-start.2) | async-done | bytes 2162720 | tf_op jit(solution)/shard_map/all_to_all | solution.py:301
  80.0 7.6 %expert_far.1 = (bf16[4,4,512,128]{3,2,1,0:T(8,128)(2,1)}, bf16[16,16,128]{2,1,0:T(8,128)(2,1)}) custom-call(s32[1]{0:T(128)} %bitcast.pos.core_ref, s32[1]{0:T(128)} %bitcast.4.y_ref, s32[1]{0:T(128)} %bitcast.5.x_ref, bf16[4,4,528,128]{3,2,1,0:T(8,128)(2,1)} %all-to-all-done.2.xs, bf16[2048,384]{1,0:T(8,128)(2,1)} %bitcast.29, bf16[2048,384]{1,0:T(8,128)(2,1)} %bitcast.31, ...), custom_call_target="tpu_custom_call" | custom-call | tf_op jit(solution)/shard_map/expert_far/pallas_call | solution.py:211
  87.6 4.4 %all-to-all-start.4 = ((bf16[4,4,512,128]{3,2,1,0:T(8,128)(2,1)}), bf16[4,4,512,128]{3,2,1,0:T(8,128)(2,1)}, u32[]{:S(2)}, u32[]{:S(2)}) async-start(bf16[4,4,512,128]{3,2,1,0:T(8,128)(2,1)} %get-tuple-element.26), calls=%async_computation.4 | async-start | bytes 4194304 | tf_op jit(solution)/shard_map/all_to_all | solution.py:301
  92.0 1.1 slice.66.xs
  93.1 5.1 %collective-permute-start.1 = (bf16[4,512,128]{2,1,0:T(8,128)(2,1)S(1)}, bf16[4,512,128]{2,1,0:T(8,128)(2,1)S(1)}, u32[]{:S(2)}, u32[]{:S(2)}) collective-permute-start(bf16[4,512,128]{2,1,0:T(8,128)(2,1)S(1)} %slice.66.xs), channel_id=1, source_target_pairs={{0,12},{1,13},{2,14},{3,15},{4,0},{5,1},{6,2},{7,3},{8,4},{9,5},{1... | collective-permute-start | bytes 1572872 | tf_op jit(solution)/shard_map/ppermute | solution.py:318
  98.2 2.8 %collective-permute-start.2 = (bf16[4,512,128]{2,1,0:T(8,128)(2,1)S(1)}, bf16[4,512,128]{2,1,0:T(8,128)(2,1)S(1)}, u32[]{:S(2)}, u32[]{:S(2)}) collective-permute-start(bf16[4,512,128]{2,1,0:T(8,128)(2,1)S(1)} %slice.66.xs), channel_id=1, source_target_pairs={{0,8},{1,9},{2,10},{3,11},{4,12},{5,13},{6,14},{7,15},{8,0},{9,1},... | collective-permute-start | bytes 1572872 | tf_op jit(solution)/shard_map/ppermute | solution.py:318
  101.0 2.8 %collective-permute-start.3 = (bf16[4,512,128]{2,1,0:T(8,128)(2,1)S(1)}, bf16[4,512,128]{2,1,0:T(8,128)(2,1)S(1)}, u32[]{:S(2)}, u32[]{:S(2)}) collective-permute-start(bf16[4,512,128]{2,1,0:T(8,128)(2,1)S(1)} %slice.66.xs), channel_id=1, source_target_pairs={{0,4},{1,5},{2,6},{3,7},{4,8},{5,9},{6,10},{7,11},{8,12},{9,13},{1... | collective-permute-start | bytes 1572872 | tf_op jit(solution)/shard_map/ppermute | solution.py:318
  103.8 8.9 %collective-permute-done.1.refs_0_ = bf16[4,512,128]{2,1,0:T(8,128)(2,1)S(1)} collective-permute-done((bf16[4,512,128]{2,1,0:T(8,128)(2,1)S(1)}, bf16[4,512,128]{2,1,0:T(8,128)(2,1)S(1)}, u32[]{:S(2)}, u32[]{:S(2)}) %collective-permute-start.1) | collective-permute-done | bytes 524320 | tf_op jit(solution)/shard_map/ppermute | solution.py:318
  112.7 1.6 collective-permute-done.2.refs_1_
  114.2 5.5 %collective-permute-done.3.refs_2_ = bf16[4,512,128]{2,1,0:T(8,128)(2,1)S(1)} collective-permute-done((bf16[4,512,128]{2,1,0:T(8,128)(2,1)S(1)}, bf16[4,512,128]{2,1,0:T(8,128)(2,1)S(1)}, u32[]{:S(2)}, u32[]{:S(2)}) %collective-permute-start.3) | collective-permute-done | bytes 524320 | tf_op jit(solution)/shard_map/ppermute | solution.py:318
  120.6 7.6 %expert_near.1 = (bf16[4,512,128]{2,1,0:T(8,128)(2,1)}, bf16[4,512,128]{2,1,0:T(8,128)(2,1)}, bf16[4,512,128]{2,1,0:T(8,128)(2,1)}, bf16[4,512,128]{2,1,0:T(8,128)(2,1)}) custom-call(s32[1]{0:T(128)} %bitcast.pos.core_ref, s32[1]{0:T(128)} %bitcast.4.y_ref, s32[1]{0:T(128)} %bitcast.5.x_ref, bf16[4,512,128]{2,1,0:T(8,128)(2,1)} %copy-done.1, ...), custom_call_target="tpu_custom_call" | custom-call | tf_op jit(solution)/shard_map/expert_near/pallas_call | solution.py:211
  128.2 4.1 %collective-permute-start.6 = (bf16[4,512,128]{2,1,0:T(8,128)(2,1)}, bf16[4,512,128]{2,1,0:T(8,128)(2,1)S(1)}, u32[]{:S(2)}, u32[]{:S(2)}) collective-permute-start(bf16[4,512,128]{2,1,0:T(8,128)(2,1)} %get-tuple-element.25), channel_id=1, source_target_pairs={{0,12},{1,13},{2,14},{3,15},{4,0},{5,1},{6,2},{7,3},{8,4},{9,5},{1... | collective-permute-start | bytes 1572872 | tf_op jit(solution)/shard_map/ppermute | solution.py:318
  132.3 1.9 collective-permute-start.5
  134.2 3.4 %collective-permute-start.4 = (bf16[4,512,128]{2,1,0:T(8,128)(2,1)}, bf16[4,512,128]{2,1,0:T(8,128)(2,1)S(1)}, u32[]{:S(2)}, u32[]{:S(2)}) collective-permute-start(bf16[4,512,128]{2,1,0:T(8,128)(2,1)} %get-tuple-element.23), channel_id=1, source_target_pairs={{0,8},{1,9},{2,10},{3,11},{4,12},{5,13},{6,14},{7,15},{8,0},{9,1},... | collective-permute-start | bytes 1572872 | tf_op jit(solution)/shard_map/ppermute | solution.py:318
  137.6 2.6 %fusion = bf16[4,512,128]{2,1,0:T(8,128)(2,1)} fusion(bf16[4,4,512,128]{3,2,1,0:T(8,128)(2,1)} %all-to-all-done.4), kind=kLoop, calls=%fused_computation.2 | loop fusion | flops 2097152 | bytes 2621440 | tf_op jit(solution)/shard_map/add | solution.py:328
  140.2 3.5 %all-to-all-start.5 = ((bf16[4,512,128]{2,1,0:T(8,128)(2,1)}), bf16[4,512,128]{2,1,0:T(8,128)(2,1)S(1)}, u32[]{:S(2)}, u32[]{:S(2)}) async-start(bf16[4,512,128]{2,1,0:T(8,128)(2,1)} %fusion), calls=%async_computation.5 | async-start | bytes 1048576 | tf_op jit(solution)/shard_map/all_to_all | solution.py:301
  143.7 9.5 %collective-permute-done.5 = bf16[4,512,128]{2,1,0:T(8,128)(2,1)S(1)} collective-permute-done((bf16[4,512,128]{2,1,0:T(8,128)(2,1)}, bf16[4,512,128]{2,1,0:T(8,128)(2,1)S(1)}, u32[]{:S(2)}, u32[]{:S(2)}) %collective-permute-start.5) | collective-permute-done | bytes 524320 | tf_op jit(solution)/shard_map/ppermute | solution.py:318
  153.2 1.1 add_convert_fusion.1
  154.3 3.5 %all-to-all-start.3 = ((bf16[4,512,128]{2,1,0:T(8,128)(2,1)}), bf16[4,512,128]{2,1,0:T(8,128)(2,1)S(1)}, u32[]{:S(2)}, u32[]{:S(2)}) async-start(bf16[4,512,128]{2,1,0:T(8,128)(2,1)} %add_convert_fusion.1), calls=%async_computation.3 | async-start | bytes 1048576 | tf_op jit(solution)/shard_map/all_to_all | solution.py:301
  157.8 1.9 collective-permute-start.7
  159.8 6.0 %all-to-all-done.3 = bf16[4,512,128]{2,1,0:T(8,128)(2,1)S(1)} async-done(((bf16[4,512,128]{2,1,0:T(8,128)(2,1)}), bf16[4,512,128]{2,1,0:T(8,128)(2,1)S(1)}, u32[]{:S(2)}, u32[]{:S(2)}) %all-to-all-start.3) | async-done | bytes 524320 | tf_op jit(solution)/shard_map/all_to_all | solution.py:301
  165.9 22.6 %all_to_all.42 = bf16[16,2,32,128]{3,2,1,0:T(8,128)(2,1)} all-to-all(bf16[16,2,32,128]{3,2,1,0:T(8,128)(2,1)S(1)} %pad_maximum_fusion.2), channel_id=1, replica_groups=mesh['z'=16,'c'=2,'y'=4,'x'=4] {'z'}, dimensions={0} | all-to-all | bytes 524288 | tf_op jit(solution)/shard_map/all_to_all | solution.py:301
  188.6 2.2 %combine.1 = (f32[256,128]{1,0:T(8,128)}, f32[16,1,256]{2,1,0:T(1,128)}) custom-call(f32[256,8]{1,0:T(8,128)} %get-tuple-element.17.table, bf16[1024,128]{1,0:T(8,128)(2,1)} %bitcast.35), custom_call_target="tpu_custom_call" | custom-call | tf_op jit(solution)/shard_map/combine/pallas_call | solution.py:249
  190.8 11.7 %all_to_all.43.parts = f32[16,1,256]{2,1,0:T(1,128)} all-to-all(f32[16,1,256]{2,1,0:T(1,128)} %get-tuple-element.27), channel_id=1, replica_groups=mesh['z'=16,'c'=2,'y'=4,'x'=4] {'y','x'}, dimensions={0} | all-to-all | bytes 32768 | tf_op jit(solution)/shard_map/all_to_all | solution.py:301
  202.5 1.8 finish.1
  (25 shorter events, 3.9 us)
Async XLA Ops:
  2.1 3.4 %collective-permute-start = (bf16[512,128]{1,0:T(8,128)(2,1)}, bf16[512,128]{1,0:T(8,128)(2,1)S(1)}, u32[]{:S(2)}, u32[]{:S(2)}) collective-permute-start(bf16[512,128]{1,0:T(8,128)(2,1)} %get-tuple-element.19), channel_id=1, source_target_pairs={{0,16},{16,0},{1,17},{17,1},{2,18},{18,2},{3,19},{19,3},{4,20},{20... | collective-permute-start | bytes 393224 | tf_op jit(solution)/shard_map/ppermute | solution.py:322
  55.8 1.0 copy-start
  58.5 21.4 %all-to-all-start.2 = ((bf16[4,4,528,128]{3,2,1,0:T(8,128)(2,1)}), bf16[4,4,528,128]{3,2,1,0:T(8,128)(2,1)}, u32[]{:S(2)}, u32[]{:S(2)}) async-start(bf16[4,4,528,128]{3,2,1,0:T(8,128)(2,1)} %broadcast_in_dim.20), calls=%async_computation.2 | async-start | bytes 4325376 | tf_op jit(solution)/shard_map/all_to_all | solution.py:301
  87.6 50.0 %all-to-all-start.4 = ((bf16[4,4,512,128]{3,2,1,0:T(8,128)(2,1)}), bf16[4,4,512,128]{3,2,1,0:T(8,128)(2,1)}, u32[]{:S(2)}, u32[]{:S(2)}) async-start(bf16[4,4,512,128]{3,2,1,0:T(8,128)(2,1)} %get-tuple-element.26), calls=%async_computation.4 | async-start | bytes 4194304 | tf_op jit(solution)/shard_map/all_to_all | solution.py:301
  93.1 27.5 %copy-start.1 = (bf16[4,512,128]{2,1,0:T(8,128)(2,1)}, bf16[4,512,128]{2,1,0:T(8,128)(2,1)S(1)}, u32[]{:S(2)}) copy-start(bf16[4,512,128]{2,1,0:T(8,128)(2,1)S(1)} %slice.66.xs) | copy-start | bytes 1572868
  93.1 19.5 %collective-permute-start.1 = (bf16[4,512,128]{2,1,0:T(8,128)(2,1)S(1)}, bf16[4,512,128]{2,1,0:T(8,128)(2,1)S(1)}, u32[]{:S(2)}, u32[]{:S(2)}) collective-permute-start(bf16[4,512,128]{2,1,0:T(8,128)(2,1)S(1)} %slice.66.xs), channel_id=1, source_target_pairs={{0,12},{1,13},{2,14},{3,15},{4,0},{5,1},{6,2},{7,3},{8,4},{9,5},{1... | collective-permute-start | bytes 1572872 | tf_op jit(solution)/shard_map/ppermute | solution.py:318
  98.2 16.0 %collective-permute-start.2 = (bf16[4,512,128]{2,1,0:T(8,128)(2,1)S(1)}, bf16[4,512,128]{2,1,0:T(8,128)(2,1)S(1)}, u32[]{:S(2)}, u32[]{:S(2)}) collective-permute-start(bf16[4,512,128]{2,1,0:T(8,128)(2,1)S(1)} %slice.66.xs), channel_id=1, source_target_pairs={{0,8},{1,9},{2,10},{3,11},{4,12},{5,13},{6,14},{7,15},{8,0},{9,1},... | collective-permute-start | bytes 1572872 | tf_op jit(solution)/shard_map/ppermute | solution.py:318
  101.0 18.7 %collective-permute-start.3 = (bf16[4,512,128]{2,1,0:T(8,128)(2,1)S(1)}, bf16[4,512,128]{2,1,0:T(8,128)(2,1)S(1)}, u32[]{:S(2)}, u32[]{:S(2)}) collective-permute-start(bf16[4,512,128]{2,1,0:T(8,128)(2,1)S(1)} %slice.66.xs), channel_id=1, source_target_pairs={{0,4},{1,5},{2,6},{3,7},{4,8},{5,9},{6,10},{7,11},{8,12},{9,13},{1... | collective-permute-start | bytes 1572872 | tf_op jit(solution)/shard_map/ppermute | solution.py:318
  112.7 7.1 %copy-start.3 = (bf16[4,512,128]{2,1,0:T(8,128)(2,1)}, bf16[4,512,128]{2,1,0:T(8,128)(2,1)S(1)}, u32[]{:S(2)}) copy-start(bf16[4,512,128]{2,1,0:T(8,128)(2,1)S(1)} %collective-permute-done.1.refs_0_) | copy-start | bytes 1572868
  114.2 5.5 %copy-start.4 = (bf16[4,512,128]{2,1,0:T(8,128)(2,1)}, bf16[4,512,128]{2,1,0:T(8,128)(2,1)S(1)}, u32[]{:S(2)}) copy-start(bf16[4,512,128]{2,1,0:T(8,128)(2,1)S(1)} %collective-permute-done.2.refs_1_) | copy-start | bytes 1572868
  119.8 0.8 copy-start.5
  128.2 25.0 %copy-start.2 = (bf16[4,512,128]{2,1,0:T(8,128)(2,1)S(1)}, bf16[4,512,128]{2,1,0:T(8,128)(2,1)}, u32[]{:S(2)}) copy-start(bf16[4,512,128]{2,1,0:T(8,128)(2,1)} %get-tuple-element.22) | copy-start | bytes 1572868
  128.2 15.5 %collective-permute-start.6 = (bf16[4,512,128]{2,1,0:T(8,128)(2,1)}, bf16[4,512,128]{2,1,0:T(8,128)(2,1)S(1)}, u32[]{:S(2)}, u32[]{:S(2)}) collective-permute-start(bf16[4,512,128]{2,1,0:T(8,128)(2,1)} %get-tuple-element.25), channel_id=1, source_target_pairs={{0,12},{1,13},{2,14},{3,15},{4,0},{5,1},{6,2},{7,3},{8,4},{9,5},{1... | collective-permute-start | bytes 1572872 | tf_op jit(solution)/shard_map/ppermute | solution.py:318
  132.3 20.9 %collective-permute-start.5 = (bf16[4,512,128]{2,1,0:T(8,128)(2,1)}, bf16[4,512,128]{2,1,0:T(8,128)(2,1)S(1)}, u32[]{:S(2)}, u32[]{:S(2)}) collective-permute-start(bf16[4,512,128]{2,1,0:T(8,128)(2,1)} %get-tuple-element.24), channel_id=1, source_target_pairs={{0,4},{1,5},{2,6},{3,7},{4,8},{5,9},{6,10},{7,11},{8,12},{9,13},{1... | collective-permute-start | bytes 1572872 | tf_op jit(solution)/shard_map/ppermute | solution.py:318
  134.2 19.0 %collective-permute-start.4 = (bf16[4,512,128]{2,1,0:T(8,128)(2,1)}, bf16[4,512,128]{2,1,0:T(8,128)(2,1)S(1)}, u32[]{:S(2)}, u32[]{:S(2)}) collective-permute-start(bf16[4,512,128]{2,1,0:T(8,128)(2,1)} %get-tuple-element.23), channel_id=1, source_target_pairs={{0,8},{1,9},{2,10},{3,11},{4,12},{5,13},{6,14},{7,15},{8,0},{9,1},... | collective-permute-start | bytes 1572872 | tf_op jit(solution)/shard_map/ppermute | solution.py:318
  140.2 14.1 %all-to-all-start.5 = ((bf16[4,512,128]{2,1,0:T(8,128)(2,1)}), bf16[4,512,128]{2,1,0:T(8,128)(2,1)S(1)}, u32[]{:S(2)}, u32[]{:S(2)}) async-start(bf16[4,512,128]{2,1,0:T(8,128)(2,1)} %fusion), calls=%async_computation.5 | async-start | bytes 1048576 | tf_op jit(solution)/shard_map/all_to_all | solution.py:301
  154.3 11.5 %all-to-all-start.3 = ((bf16[4,512,128]{2,1,0:T(8,128)(2,1)}), bf16[4,512,128]{2,1,0:T(8,128)(2,1)S(1)}, u32[]{:S(2)}, u32[]{:S(2)}) async-start(bf16[4,512,128]{2,1,0:T(8,128)(2,1)} %add_convert_fusion.1), calls=%async_computation.3 | async-start | bytes 1048576 | tf_op jit(solution)/shard_map/all_to_all | solution.py:301
  157.8 8.0 %collective-permute-start.7 = (bf16[512,128]{1,0:T(8,128)(2,1)S(1)}, bf16[512,128]{1,0:T(8,128)(2,1)S(1)}, u32[]{:S(2)}, u32[]{:S(2)}) collective-permute-start(bf16[512,128]{1,0:T(8,128)(2,1)S(1)} %fusion.1), channel_id=1, source_target_pairs={{0,16},{16,0},{1,17},{17,1},{2,18},{18,2},{3,19},{19,3},{4,20},{20... | collective-permute-start | bytes 393224 | tf_op jit(solution)/shard_map/ppermute | solution.py:322

commit v10 on v5

--- a/solution.py
+++ b/solution.py
@@ -73,16 +73,11 @@
         refs = refs[11:]
     raw, gain_s, xn, gu_s, d_s, stage, sems, osems = refs
     core = core_ref[0]
-    role = core if first else 1 - core
-    at_outer = jnp.where(role == 0, y_ref[0], x_ref[0])
-    at_inner = jnp.where(role == 0, x_ref[0], y_ref[0])
+    at_outer = jnp.where(core == 0, y_ref[0], x_ref[0])
 
     def block(o, i):
         outer = o if first else jnp.bitwise_and(at_outer + o, 3)
-        return jnp.where(role == 0, outer * 4 + i, i * 4 + outer)
-
-    def taken(o, i):
-        return block(o, i if first else jnp.bitwise_and(at_inner + i, 3))
+        return jnp.where(core == 0, outer * 4 + i, i * 4 + outer)
 
     def source(o):
         if first:
@@ -103,7 +98,7 @@
 
     def fetch_rows(at):
         return [
-            fetch(source(o).at[i, pl.ds(at, half), :], raw.at[taken(o, i), pl.ds(at, half), :])
+            fetch(source(o).at[i, pl.ds(at, half), :], raw.at[block(o, i), pl.ds(at, half), :])
             for o in range(4)
             for i in range(4)
         ]
@@ -311,6 +306,12 @@
     return jnp.broadcast_to(v[None], (4, *v.shape))
 
 
+def over_z(near, far):
+    share = near.shape[1]
+    both = jnp.stack([near.reshape(16, -1, share), far.reshape(16, -1, share)], axis=1)
+    return exchange(both, "z")
+
+
 def local(tokens, norm_gain, w_gate, w_up, w_down, routes, route_weights, final_gain):
     _, share = tokens.shape
     width = share * 16
@@ -321,19 +322,21 @@
     near, far = (both[:, i].reshape(-1, share) for i in range(2))
     far = swap(far)
     gain_rows = jnp.broadcast_to(norm_gain[None, :], (GAIN_ROWS, share))
-    far = across(copies_of(jnp.concatenate([far, gain_rows], axis=0)), 0)
-    near = jnp.stack([near] + [ahead(near, 1, -s) for s in (1, 2, 3)])
-    far = across(copies_of(far), 1)
-    near = [near] + [ahead(near, 0, -s) for s in (1, 2, 3)]
+    rows = jnp.concatenate([far, gain_rows, near], axis=0)
+    rows = across(copies_of(rows), 0)
+    first = far.shape[0] + GAIN_ROWS
+    far = across(copies_of(rows[:, :first]), 1)
+    near = rows[:, first:]
+    near = [near] + [ahead(near, 1, -s) for s in (1, 2, 3)]
     far, gain = expert(True, place, far, weights, None)
     far = summed(across(far, 1))
     near = expert(False, place, near, weights, gain)
-    two = ahead(near[2], 0, 2)
-    near = total_of([near[0], two, ahead(near[1], 0, 1), ahead(near[3], 0, 3)])
+    two = ahead(near[2], 1, 2)
+    near = total_of([near[0], two, ahead(near[1], 1, 1), ahead(near[3], 1, 3)])
     far = swap(summed(across(far, 0)))
-    near = summed(across(near, 1))
-    both = jnp.stack([near.reshape(16, -1, share), far.reshape(16, -1, share)], axis=1)
-    combined, squares = combine(table, exchange(both, "z").reshape(-1, share))
+    near = summed(across(near, 0))
+    both = over_z(near, far)
+    combined, squares = combine(table, both.reshape(-1, share))
     total = exchange(squares, ("y", "x")).sum(axis=(0, 1))
     scale = lax.rsqrt(total / width + EPS)
     return (combined * scale[:, None] * final_gain.astype(F32)[None, :]).astype(BF16)

time: 210 us -> 203 us (0.967)
  starting transfers between devices: 55.4 us -> 43.3 us
  blocking collectives: 66 us -> 70.6 us
  local copies, waits for them, and re-layouts: 3.26 us -> 5.46 us
    ppermute x9 -> x6, starting transfers between devices: 29.5 us -> 20 us  [ahead(): return lax.ppermute(v, ALL, pairs)]
    all_to_all x3, blocking collectives: 66 us -> 70.6 us  [exchange(): lax.all_to_all(v, axis, split_axis=0, concat_axis=0, tiled=True, axis_ind...]
    all_to_all x5, starting transfers between devices: 22 us -> 19.5 us  [exchange(): lax.all_to_all(v, axis, split_axis=0, concat_axis=0, tiled=True, axis_ind...]
    ppermute x9 -> x6, waiting for transfers between devices: 25.7 us -> 25.5 us  [ahead(): return lax.ppermute(v, ALL, pairs)]
  transfers between devices with their start and end apart: 16 -> 13, of which waited for: 11 -> 8; matrix products, arithmetic and copies ran while one was open for 2% -> 2% of each run, Pallas kernels for 4% -> 4%
where the time goes in v10:
time: 203 us; the launch traced here: 202 us
  blocking collectives  70.6 us (35%)
  waiting for transfers between devices  57.3 us (28%)
  starting transfers between devices  43.3 us (21%)
  Pallas kernels  19.5 us (10%)
  other arithmetic  5.54 us (3%)
  local copies, waits for them, and re-layouts  5.46 us (3%)
    all_to_all x3, blocking collectives, exchange(): lax.all_to_all(v, axis, split_axis=0, concat_axis=0, tiled=True, axis_ind...  70.6 us
    all_to_all x5, waiting for transfers between devices, exchange(): lax.all_to_all(v, axis, split_axis=0, concat_axis=0, tiled=True, axis_ind...  30.5 us
    ppermute x6, waiting for transfers between devices, ahead(): return lax.ppermute(v, ALL, pairs)  25.5 us
    ppermute x6, starting transfers between devices, ahead(): return lax.ppermute(v, ALL, pairs)  20 us
    all_to_all x5, starting transfers between devices, exchange(): lax.all_to_all(v, axis, split_axis=0, concat_axis=0, tiled=True, axis_ind...  19.5 us
    pallas_call x2, Pallas kernels, expert(): pl.pallas_call(functools.partial(expert_kernel, first, rows), out_shape=o...  15.2 us
  transfers between devices with their start and end apart: 13, of which 8 were waited for; matrix products, arithmetic and copies ran while one was open for 2% of the time, Pallas kernels for 4%

profile of v10, /device:TPU:32, one launch (start us, length us, event | category | flops | bytes accessed | tf_op | source)
XLA Modules:
  0.0 201.9 jit_solution(12502086788051705348)
XLA Ops:
  0.0 2.1 %pack.1 = (bf16[1024,128]{1,0:T(8,128)(2,1)}, f32[256,8]{1,0:T(8,128)}) custom-call(s32[1]{0:T(128)} %bitcast.pos.core_ref, s32[2,256]{1,0:T(2,128)} %bitcast.34, f32[2,256]{1,0:T(2,128)} %bitcast.35, bf16[256,128]{1,0:T(8,128)(2,1)} %tokens.1), custom_call_target="tpu_custom_call" | custom-call | tf_op jit(solution)/shard_map/pack/pallas_call | solution.py:52
  2.1 33.1 %all_to_all.40 = bf16[16,2,32,128]{3,2,1,0:T(8,128)(2,1)S(1)} all-to-all(bf16[16,2,32,128]{3,2,1,0:T(8,128)(2,1)} %bitcast.31), channel_id=1, replica_groups=mesh['z'=16,'c'=2,'y'=4,'x'=4] {'z'}, dimensions={0} | all-to-all | bytes 524288 | tf_op jit(solution)/shard_map/all_to_all | solution.py:270
  35.2 1.9 collective-permute-start
  37.2 1.3 collective-permute-done
  39.3 15.1 %all_to_all.41 = bf16[4,1040,128]{2,1,0:T(8,128)(2,1)S(1)} all-to-all(bf16[4,1040,128]{2,1,0:T(8,128)(2,1)S(1)} %broadcast_in_dim.7), channel_id=1, replica_groups={{0,1,2,3},{4,5,6,7},{8,9,10,11},{12,13,14,15},{16,20,24,28},{17,21,25,2..., dimensions={0} | all-to-all | bytes 2129920 | tf_op jit(solution)/shard_map/all_to_all | solution.py:270
  55.4 1.7 broadcast_in_dim.8
  57.1 4.5 %all-to-all-start.2 = ((bf16[4,4,528,128]{3,2,1,0:T(8,128)(2,1)}), bf16[4,4,528,128]{3,2,1,0:T(8,128)(2,1)}, u32[]{:S(2)}, u32[]{:S(2)}) async-start(bf16[4,4,528,128]{3,2,1,0:T(8,128)(2,1)} %broadcast_in_dim.8), calls=%async_computation.2 | async-start | bytes 4325376 | tf_op jit(solution)/shard_map/all_to_all | solution.py:270
  61.5 17.0 %all-to-all-done.2.xs = bf16[4,4,528,128]{3,2,1,0:T(8,128)(2,1)} async-done(((bf16[4,4,528,128]{3,2,1,0:T(8,128)(2,1)}), bf16[4,4,528,128]{3,2,1,0:T(8,128)(2,1)}, u32[]{:S(2)}, u32[]{:S(2)}) %all-to-all-start.2) | async-done | bytes 2162720 | tf_op jit(solution)/shard_map/all_to_all | solution.py:270
  78.5 7.6 %expert_far.1 = (bf16[4,4,512,128]{3,2,1,0:T(8,128)(2,1)}, bf16[16,16,128]{2,1,0:T(8,128)(2,1)}) custom-call(s32[1]{0:T(128)} %bitcast.pos.core_ref, s32[1]{0:T(128)} %bitcast.3.y_ref, s32[1]{0:T(128)} %bitcast.4.x_ref, bf16[4,4,528,128]{3,2,1,0:T(8,128)(2,1)} %all-to-all-done.2.xs, bf16[2048,384]{1,0:T(8,128)(2,1)} %bitcast.22, bf16[2048,384]{1,0:T(8,128)(2,1)} %bitcast.24, ...), custom_call_target="tpu_custom_call" | custom-call | tf_op jit(solution)/shard_map/expert_far/pallas_call | solution.py:197
  86.1 4.5 %all-to-all-start.4 = ((bf16[4,4,512,128]{3,2,1,0:T(8,128)(2,1)}), bf16[4,4,512,128]{3,2,1,0:T(8,128)(2,1)}, u32[]{:S(2)}, u32[]{:S(2)}) async-start(bf16[4,4,512,128]{3,2,1,0:T(8,128)(2,1)} %get-tuple-element.22), calls=%async_computation.4 | async-start | bytes 4194304 | tf_op jit(solution)/shard_map/all_to_all | solution.py:270
  90.6 1.1 slice.66.xs
  91.7 5.1 %collective-permute-start.1 = (bf16[4,512,128]{2,1,0:T(8,128)(2,1)S(1)}, bf16[4,512,128]{2,1,0:T(8,128)(2,1)S(1)}, u32[]{:S(2)}, u32[]{:S(2)}) collective-permute-start(bf16[4,512,128]{2,1,0:T(8,128)(2,1)S(1)} %slice.66.xs), channel_id=1, source_target_pairs={{0,12},{1,13},{2,14},{3,15},{4,0},{5,1},{6,2},{7,3},{8,4},{9,5},{1... | collective-permute-start | bytes 1572872 | tf_op jit(solution)/shard_map/ppermute | solution.py:287
  96.8 2.8 %collective-permute-start.2 = (bf16[4,512,128]{2,1,0:T(8,128)(2,1)S(1)}, bf16[4,512,128]{2,1,0:T(8,128)(2,1)S(1)}, u32[]{:S(2)}, u32[]{:S(2)}) collective-permute-start(bf16[4,512,128]{2,1,0:T(8,128)(2,1)S(1)} %slice.66.xs), channel_id=1, source_target_pairs={{0,8},{1,9},{2,10},{3,11},{4,12},{5,13},{6,14},{7,15},{8,0},{9,1},... | collective-permute-start | bytes 1572872 | tf_op jit(solution)/shard_map/ppermute | solution.py:287
  99.6 2.8 %collective-permute-start.3 = (bf16[4,512,128]{2,1,0:T(8,128)(2,1)S(1)}, bf16[4,512,128]{2,1,0:T(8,128)(2,1)S(1)}, u32[]{:S(2)}, u32[]{:S(2)}) collective-permute-start(bf16[4,512,128]{2,1,0:T(8,128)(2,1)S(1)} %slice.66.xs), channel_id=1, source_target_pairs={{0,4},{1,5},{2,6},{3,7},{4,8},{5,9},{6,10},{7,11},{8,12},{9,13},{1... | collective-permute-start | bytes 1572872 | tf_op jit(solution)/shard_map/ppermute | solution.py:287
  102.4 8.9 %collective-permute-done.1.refs_0_ = bf16[4,512,128]{2,1,0:T(8,128)(2,1)S(1)} collective-permute-done((bf16[4,512,128]{2,1,0:T(8,128)(2,1)S(1)}, bf16[4,512,128]{2,1,0:T(8,128)(2,1)S(1)}, u32[]{:S(2)}, u32[]{:S(2)}) %collective-permute-start.1) | collective-permute-done | bytes 524320 | tf_op jit(solution)/shard_map/ppermute | solution.py:287
  111.2 1.6 collective-permute-done.2.refs_1_
  112.8 5.5 %collective-permute-done.3.refs_2_ = bf16[4,512,128]{2,1,0:T(8,128)(2,1)S(1)} collective-permute-done((bf16[4,512,128]{2,1,0:T(8,128)(2,1)S(1)}, bf16[4,512,128]{2,1,0:T(8,128)(2,1)S(1)}, u32[]{:S(2)}, u32[]{:S(2)}) %collective-permute-start.3) | collective-permute-done | bytes 524320 | tf_op jit(solution)/shard_map/ppermute | solution.py:287
  119.2 7.6 %expert_near.1 = (bf16[4,512,128]{2,1,0:T(8,128)(2,1)}, bf16[4,512,128]{2,1,0:T(8,128)(2,1)}, bf16[4,512,128]{2,1,0:T(8,128)(2,1)}, bf16[4,512,128]{2,1,0:T(8,128)(2,1)}) custom-call(s32[1]{0:T(128)} %bitcast.pos.core_ref, s32[1]{0:T(128)} %bitcast.3.y_ref, s32[1]{0:T(128)} %bitcast.4.x_ref, bf16[4,512,128]{2,1,0:T(8,128)(2,1)} %copy-done.1, ...), custom_call_target="tpu_custom_call" | custom-call | tf_op jit(solution)/shard_map/expert_near/pallas_call | solution.py:197
  126.7 4.1 %collective-permute-start.6 = (bf16[4,512,128]{2,1,0:T(8,128)(2,1)}, bf16[4,512,128]{2,1,0:T(8,128)(2,1)S(1)}, u32[]{:S(2)}, u32[]{:S(2)}) collective-permute-start(bf16[4,512,128]{2,1,0:T(8,128)(2,1)} %get-tuple-element.21), channel_id=1, source_target_pairs={{0,12},{1,13},{2,14},{3,15},{4,0},{5,1},{6,2},{7,3},{8,4},{9,5},{1... | collective-permute-start | bytes 1572872 | tf_op jit(solution)/shard_map/ppermute | solution.py:287
  130.8 1.9 collective-permute-start.5
  132.8 3.4 %collective-permute-start.4 = (bf16[4,512,128]{2,1,0:T(8,128)(2,1)}, bf16[4,512,128]{2,1,0:T(8,128)(2,1)S(1)}, u32[]{:S(2)}, u32[]{:S(2)}) collective-permute-start(bf16[4,512,128]{2,1,0:T(8,128)(2,1)} %get-tuple-element.19), channel_id=1, source_target_pairs={{0,8},{1,9},{2,10},{3,11},{4,12},{5,13},{6,14},{7,15},{8,0},{9,1},... | collective-permute-start | bytes 1572872 | tf_op jit(solution)/shard_map/ppermute | solution.py:287
  136.2 2.6 %fusion = bf16[4,512,128]{2,1,0:T(8,128)(2,1)} fusion(bf16[4,4,512,128]{3,2,1,0:T(8,128)(2,1)} %all-to-all-done.4), kind=kLoop, calls=%fused_computation.2 | loop fusion | flops 2097152 | bytes 2621440 | tf_op jit(solution)/shard_map/add | solution.py:297
  138.8 3.5 %all-to-all-start.5 = ((bf16[4,512,128]{2,1,0:T(8,128)(2,1)}), bf16[4,512,128]{2,1,0:T(8,128)(2,1)S(1)}, u32[]{:S(2)}, u32[]{:S(2)}) async-start(bf16[4,512,128]{2,1,0:T(8,128)(2,1)} %fusion), calls=%async_computation.5 | async-start | bytes 1048576 | tf_op jit(solution)/shard_map/all_to_all | solution.py:270
  142.2 9.5 %collective-permute-done.5 = bf16[4,512,128]{2,1,0:T(8,128)(2,1)S(1)} collective-permute-done((bf16[4,512,128]{2,1,0:T(8,128)(2,1)}, bf16[4,512,128]{2,1,0:T(8,128)(2,1)S(1)}, u32[]{:S(2)}, u32[]{:S(2)}) %collective-permute-start.5) | collective-permute-done | bytes 524320 | tf_op jit(solution)/shard_map/ppermute | solution.py:287
  152.8 3.6 %all-to-all-start.3 = ((bf16[4,512,128]{2,1,0:T(8,128)(2,1)}), bf16[4,512,128]{2,1,0:T(8,128)(2,1)S(1)}, u32[]{:S(2)}, u32[]{:S(2)}) async-start(bf16[4,512,128]{2,1,0:T(8,128)(2,1)} %add_convert_fusion.1), calls=%async_computation.3 | async-start | bytes 1048576 | tf_op jit(solution)/shard_map/all_to_all | solution.py:270
  156.5 1.9 collective-permute-start.7
  158.5 6.0 %all-to-all-done.3 = bf16[4,512,128]{2,1,0:T(8,128)(2,1)S(1)} async-done(((bf16[4,512,128]{2,1,0:T(8,128)(2,1)}), bf16[4,512,128]{2,1,0:T(8,128)(2,1)S(1)}, u32[]{:S(2)}, u32[]{:S(2)}) %all-to-all-start.3) | async-done | bytes 524320 | tf_op jit(solution)/shard_map/all_to_all | solution.py:270
  164.6 22.4 %all_to_all.42 = bf16[16,2,32,128]{3,2,1,0:T(8,128)(2,1)} all-to-all(bf16[16,2,32,128]{3,2,1,0:T(8,128)(2,1)S(1)} %pad_maximum_fusion.1), channel_id=1, replica_groups=mesh['z'=16,'c'=2,'y'=4,'x'=4] {'z'}, dimensions={0} | all-to-all | bytes 524288 | tf_op jit(solution)/shard_map/all_to_all | solution.py:270
  187.0 2.2 %combine.1 = (f32[256,128]{1,0:T(8,128)}, f32[16,1,256]{2,1,0:T(1,128)}) custom-call(f32[256,8]{1,0:T(8,128)} %get-tuple-element.15.table, bf16[1024,128]{1,0:T(8,128)(2,1)} %bitcast.28), custom_call_target="tpu_custom_call" | custom-call | tf_op jit(solution)/shard_map/combine/pallas_call | solution.py:238
  189.2 3.5 %all-to-all-start.7 = ((f32[16,1,256]{2,1,0:T(1,128)}), f32[16,1,256]{2,1,0:T(1,128)S(1)}, u32[]{:S(2)}, u32[]{:S(2)}) async-start(f32[16,1,256]{2,1,0:T(1,128)} %get-tuple-element.24), calls=%async_computation.7 | async-start | bytes 32768 | tf_op jit(solution)/shard_map/all_to_all | solution.py:270
  192.7 7.5 %all-to-all-done.7 = f32[16,1,256]{2,1,0:T(1,128)S(1)} async-done(((f32[16,1,256]{2,1,0:T(1,128)}), f32[16,1,256]{2,1,0:T(1,128)S(1)}, u32[]{:S(2)}, u32[]{:S(2)}) %all-to-all-start.7) | async-done | bytes 16416 | tf_op jit(solution)/shard_map/all_to_all | solution.py:270
  200.3 1.6 multiply_convert_fusion
  (31 shorter events, 4.0 us)
Async XLA Ops:
  35.2 3.2 %collective-permute-start = (bf16[512,128]{1,0:T(8,128)(2,1)S(1)}, bf16[512,128]{1,0:T(8,128)(2,1)S(1)}, u32[]{:S(2)}, u32[]{:S(2)}) collective-permute-start(bf16[512,128]{1,0:T(8,128)(2,1)S(1)} %bitcast.33), channel_id=1, source_target_pairs={{0,16},{16,0},{1,17},{17,1},{2,18},{18,2},{3,19},{19,3},{4,20},{20... | collective-permute-start | bytes 393224 | tf_op jit(solution)/shard_map/ppermute | solution.py:291
  54.4 1.0 copy-start
  57.1 21.4 %all-to-all-start.2 = ((bf16[4,4,528,128]{3,2,1,0:T(8,128)(2,1)}), bf16[4,4,528,128]{3,2,1,0:T(8,128)(2,1)}, u32[]{:S(2)}, u32[]{:S(2)}) async-start(bf16[4,4,528,128]{3,2,1,0:T(8,128)(2,1)} %broadcast_in_dim.8), calls=%async_computation.2 | async-start | bytes 4325376 | tf_op jit(solution)/shard_map/all_to_all | solution.py:270
  86.1 50.0 %all-to-all-start.4 = ((bf16[4,4,512,128]{3,2,1,0:T(8,128)(2,1)}), bf16[4,4,512,128]{3,2,1,0:T(8,128)(2,1)}, u32[]{:S(2)}, u32[]{:S(2)}) async-start(bf16[4,4,512,128]{3,2,1,0:T(8,128)(2,1)} %get-tuple-element.22), calls=%async_computation.4 | async-start | bytes 4194304 | tf_op jit(solution)/shard_map/all_to_all | solution.py:270
  91.7 27.5 %copy-start.1 = (bf16[4,512,128]{2,1,0:T(8,128)(2,1)}, bf16[4,512,128]{2,1,0:T(8,128)(2,1)S(1)}, u32[]{:S(2)}) copy-start(bf16[4,512,128]{2,1,0:T(8,128)(2,1)S(1)} %slice.66.xs) | copy-start | bytes 1572868
  91.7 19.5 %collective-permute-start.1 = (bf16[4,512,128]{2,1,0:T(8,128)(2,1)S(1)}, bf16[4,512,128]{2,1,0:T(8,128)(2,1)S(1)}, u32[]{:S(2)}, u32[]{:S(2)}) collective-permute-start(bf16[4,512,128]{2,1,0:T(8,128)(2,1)S(1)} %slice.66.xs), channel_id=1, source_target_pairs={{0,12},{1,13},{2,14},{3,15},{4,0},{5,1},{6,2},{7,3},{8,4},{9,5},{1... | collective-permute-start | bytes 1572872 | tf_op jit(solution)/shard_map/ppermute | solution.py:287
  96.8 16.0 %collective-permute-start.2 = (bf16[4,512,128]{2,1,0:T(8,128)(2,1)S(1)}, bf16[4,512,128]{2,1,0:T(8,128)(2,1)S(1)}, u32[]{:S(2)}, u32[]{:S(2)}) collective-permute-start(bf16[4,512,128]{2,1,0:T(8,128)(2,1)S(1)} %slice.66.xs), channel_id=1, source_target_pairs={{0,8},{1,9},{2,10},{3,11},{4,12},{5,13},{6,14},{7,15},{8,0},{9,1},... | collective-permute-start | bytes 1572872 | tf_op jit(solution)/shard_map/ppermute | solution.py:287
  99.6 18.7 %collective-permute-start.3 = (bf16[4,512,128]{2,1,0:T(8,128)(2,1)S(1)}, bf16[4,512,128]{2,1,0:T(8,128)(2,1)S(1)}, u32[]{:S(2)}, u32[]{:S(2)}) collective-permute-start(bf16[4,512,128]{2,1,0:T(8,128)(2,1)S(1)} %slice.66.xs), channel_id=1, source_target_pairs={{0,4},{1,5},{2,6},{3,7},{4,8},{5,9},{6,10},{7,11},{8,12},{9,13},{1... | collective-permute-start | bytes 1572872 | tf_op jit(solution)/shard_map/ppermute | solution.py:287
  111.2 7.1 %copy-start.3 = (bf16[4,512,128]{2,1,0:T(8,128)(2,1)}, bf16[4,512,128]{2,1,0:T(8,128)(2,1)S(1)}, u32[]{:S(2)}) copy-start(bf16[4,512,128]{2,1,0:T(8,128)(2,1)S(1)} %collective-permute-done.1.refs_0_) | copy-start | bytes 1572868
  112.8 5.5 %copy-start.4 = (bf16[4,512,128]{2,1,0:T(8,128)(2,1)}, bf16[4,512,128]{2,1,0:T(8,128)(2,1)S(1)}, u32[]{:S(2)}) copy-start(bf16[4,512,128]{2,1,0:T(8,128)(2,1)S(1)} %collective-permute-done.2.refs_1_) | copy-start | bytes 1572868
  118.3 0.8 copy-start.5
  126.7 25.0 %copy-start.2 = (bf16[4,512,128]{2,1,0:T(8,128)(2,1)S(1)}, bf16[4,512,128]{2,1,0:T(8,128)(2,1)}, u32[]{:S(2)}) copy-start(bf16[4,512,128]{2,1,0:T(8,128)(2,1)} %get-tuple-element.18) | copy-start | bytes 1572868
  126.7 15.5 %collective-permute-start.6 = (bf16[4,512,128]{2,1,0:T(8,128)(2,1)}, bf16[4,512,128]{2,1,0:T(8,128)(2,1)S(1)}, u32[]{:S(2)}, u32[]{:S(2)}) collective-permute-start(bf16[4,512,128]{2,1,0:T(8,128)(2,1)} %get-tuple-element.21), channel_id=1, source_target_pairs={{0,12},{1,13},{2,14},{3,15},{4,0},{5,1},{6,2},{7,3},{8,4},{9,5},{1... | collective-permute-start | bytes 1572872 | tf_op jit(solution)/shard_map/ppermute | solution.py:287
  130.8 20.9 %collective-permute-start.5 = (bf16[4,512,128]{2,1,0:T(8,128)(2,1)}, bf16[4,512,128]{2,1,0:T(8,128)(2,1)S(1)}, u32[]{:S(2)}, u32[]{:S(2)}) collective-permute-start(bf16[4,512,128]{2,1,0:T(8,128)(2,1)} %get-tuple-element.20), channel_id=1, source_target_pairs={{0,4},{1,5},{2,6},{3,7},{4,8},{5,9},{6,10},{7,11},{8,12},{9,13},{1... | collective-permute-start | bytes 1572872 | tf_op jit(solution)/shard_map/ppermute | solution.py:287
  132.8 19.0 %collective-permute-start.4 = (bf16[4,512,128]{2,1,0:T(8,128)(2,1)}, bf16[4,512,128]{2,1,0:T(8,128)(2,1)S(1)}, u32[]{:S(2)}, u32[]{:S(2)}) collective-permute-start(bf16[4,512,128]{2,1,0:T(8,128)(2,1)} %get-tuple-element.19), channel_id=1, source_target_pairs={{0,8},{1,9},{2,10},{3,11},{4,12},{5,13},{6,14},{7,15},{8,0},{9,1},... | collective-permute-start | bytes 1572872 | tf_op jit(solution)/shard_map/ppermute | solution.py:287
  138.8 14.1 %all-to-all-start.5 = ((bf16[4,512,128]{2,1,0:T(8,128)(2,1)}), bf16[4,512,128]{2,1,0:T(8,128)(2,1)S(1)}, u32[]{:S(2)}, u32[]{:S(2)}) async-start(bf16[4,512,128]{2,1,0:T(8,128)(2,1)} %fusion), calls=%async_computation.5 | async-start | bytes 1048576 | tf_op jit(solution)/shard_map/all_to_all | solution.py:270
  152.8 39.9 %copy-start.6 = (bf16[128]{0:T(256)(128)(2,1)S(1)}, bf16[128]{0:T(256)(128)(2,1)}, u32[]{:S(2)}) copy-start(bf16[128]{0:T(256)(128)(2,1)} %param.15) | copy-start | bytes 772
  152.8 11.7 %all-to-all-start.3 = ((bf16[4,512,128]{2,1,0:T(8,128)(2,1)}), bf16[4,512,128]{2,1,0:T(8,128)(2,1)S(1)}, u32[]{:S(2)}, u32[]{:S(2)}) async-start(bf16[4,512,128]{2,1,0:T(8,128)(2,1)} %add_convert_fusion.1), calls=%async_computation.3 | async-start | bytes 1048576 | tf_op jit(solution)/shard_map/all_to_all | solution.py:270
  156.5 8.0 %collective-permute-start.7 = (bf16[512,128]{1,0:T(8,128)(2,1)S(1)}, bf16[512,128]{1,0:T(8,128)(2,1)S(1)}, u32[]{:S(2)}, u32[]{:S(2)}) collective-permute-start(bf16[512,128]{1,0:T(8,128)(2,1)S(1)} %fusion.1), channel_id=1, source_target_pairs={{0,16},{16,0},{1,17},{17,1},{2,18},{18,2},{3,19},{19,3},{4,20},{20... | collective-permute-start | bytes 393224 | tf_op jit(solution)/shard_map/ppermute | solution.py:291
  189.2 11.0 %all-to-all-start.7 = ((f32[16,1,256]{2,1,0:T(1,128)}), f32[16,1,256]{2,1,0:T(1,128)S(1)}, u32[]{:S(2)}, u32[]{:S(2)}) async-start(f32[16,1,256]{2,1,0:T(1,128)} %get-tuple-element.24), calls=%async_computation.7 | async-start | bytes 32768 | tf_op jit(solution)/shard_map/all_to_all | solution.py:270
